TPU v7x, 128 devices: a whole 4x4x4 slice. The times are simulated.
128 devices in a mesh: fs: 16 (over z, x), tp: 8 (over y, core).
Axes of the slice: x: 4, y: 4, z: 4, core: 2. Of those that a mesh axis runs over, the one named last changes fastest.
Arguments:
- saved_input: bfloat16 [49152, 2048], P('fs'), may hold values from -24 to 24
- key_cot: bfloat16 [49152, 2048], P('fs', 'tp')
- value_cot: bfloat16 [49152, 2048], P('fs', 'tp')
- weights: float32 [2, 2048, 2048], P(None, 'fs', 'tp'), may hold values from -3 to 3
- left_root: float32 [2, 8, 2048, 2048], P(None, 'tp', 'fs'), may hold values from -1 to 3
- left_stat: float32 [2, 8, 2048, 2048], P(None, 'tp', 'fs'), may hold values from -48 to 48
- right_root: float32 [2, 8, 256, 256], P(None, 'tp'), may hold values from -1 to 3
- right_stat: float32 [2, 8, 256, 256], P(None, 'tp'), may hold values from -48 to 48
Outputs:
- step: float32 [2, 2048, 2048], P(None, 'fs', 'tp')
- new_weights: float32 [2, 2048, 2048], P(None, 'fs', 'tp')
- copies: bfloat16 [2, 2048, 2048], P(None, None, 'tp')
- new_left: float32 [2, 8, 2048, 2048], P(None, 'tp', 'fs')
- new_right: float32 [2, 8, 256, 256], P(None, 'tp')
All inputs are finite; a program needn't handle non-finite values.
Results may differ from a plain program's by a relative error of at most 0.0004.
Values may be sent and summed in bfloat16 or wider, within the bound.
No kernel may reach another device: no remote copies, remote signals or barrier semaphores. Data moves between devices by JAX's collectives and lax.ppermute only.
A program may use at most 128 MiB of HBM per device.

v0:
```python
import functools
import math

import jax
import jax.numpy as jnp
from jax import lax
from jax.experimental import pallas as pl
from jax.experimental.pallas import tpu as pltpu
from jax.sharding import Mesh
from jax.sharding import PartitionSpec as P


FS = ("fs_0", "fs_1")
FS_TP = ("fs_0", "fs_1", "tp_0", "tp_1")
TP = ("tp_0", "tp_1")
Z, X = FS
RING = 4
GROUPS = 8
SPAN = 250.0
FLOOR = 124.0
LN2 = math.log(2.0)
MIB = 1 << 20

decay_stat = 0.9
learn_rate = 0.05
norm_eps = 1e-06


VMEM = pl.BlockSpec(memory_space=pltpu.VMEM)
HBM = pl.BlockSpec(memory_space=pl.ANY)


def call(kernel, out_shape, in_specs, limit, scratch=(), out_specs=None, aliases=None):
    single = not isinstance(out_shape, (list, tuple))
    if out_specs is None:
        out_specs = VMEM if single else [VMEM] * len(out_shape)
    return pl.pallas_call(
        kernel,
        out_shape=out_shape,
        in_specs=in_specs,
        out_specs=out_specs,
        scratch_shapes=list(scratch),
        input_output_aliases=aliases or {},
        compiler_params=pltpu.CompilerParams(vmem_limit_bytes=limit * MIB),
    )


def shift(value, axis, by):
    return lax.ppermute(value, axis, [(i, (i + by) % RING) for i in range(RING)])


def where_am_i():
    return lax.axis_index(Z), lax.axis_index(X)


def turn(index):
    return lax.rem(index, RING)


def lanes(index, width):
    return pl.ds(pl.multiple_of(index * width, width), width)


def encode(block, ref, j):
    columns, width = block.shape
    grouped = block.reshape(columns // GROUPS, GROUPS, width)
    size = jnp.abs(grouped)
    scale = (jnp.max(size, axis=0) * 1.0079 + 1e-30).astype(jnp.bfloat16)
    factor = SPAN / scale.astype(jnp.float32)
    code = jnp.exp2(size * factor[None] - FLOOR)
    code = jnp.where(grouped < 0.0, -code, code)
    ref[j, :columns, :] = code.reshape(columns, width).astype(jnp.bfloat16)
    ref[j, columns:, :] = scale


def decode(ref, j):
    rows, width = ref.shape[1:]
    columns = rows - GROUPS
    code = ref[j, :columns, :].astype(jnp.float32).reshape(columns // GROUPS, GROUPS, width)
    scale = ref[j, columns:, :].astype(jnp.float32) * (1.0 / (SPAN * LN2))
    size = (jnp.log(jnp.abs(code)) + FLOOR * LN2) * scale[None]
    return jnp.where(code < 0.0, -size, size).reshape(columns, width)


def split(value):
    high = value.astype(jnp.bfloat16)
    return high, (value - high.astype(jnp.float32)).astype(jnp.bfloat16)


def dot3(left, right, dims):
    (lh, ll), (rh, rl) = left, right
    dot = functools.partial(
        lax.dot_general, dimension_numbers=(dims, ((), ())), preferred_element_type=jnp.float32
    )
    return dot(lh, rh) + (dot(lh, rl) + dot(ll, rh))


def chunk(turned, x_ref, width, m, by):
    z, x = where_am_i()
    if m == 0:
        at = turn(x + by)
        columns = [x_ref[:, lanes(j * RING + at, width)] for j in range(RING)]
        columns = jnp.concatenate(columns, axis=1)
    else:
        columns = x_ref[:, lanes(turn(z + by), RING * width)]
    return jnp.dot(turned, columns, preferred_element_type=jnp.float32)


def coded_chunk(turned, x_ref, width, m, by, out):
    total = chunk(turned, x_ref, width, m, by)
    for j in range(RING):
        encode(total[:, j * width : (j + 1) * width], out, j)


def columns_of(x_hbm, x_ref, width, down, by):
    z, x = where_am_i()
    at = lanes(turn(z + down) * RING + turn(x + by), width)
    return x_hbm.at[:, at], x_ref.at[:, at]


def started(parts, sems):
    copies = [pltpu.make_async_copy(a, b, sems.at[i]) for i, (a, b) in enumerate(parts)]
    for c in copies:
        c.start()
    return copies


def first_kernel(width, x_hbm, k_hbm, v_hbm, x_ref, kt_ref, vt_ref, out_k, out_v, k_ref, v_ref, sems):
    z, _ = where_am_i()
    at = lanes(turn(z + 2), RING * width)
    parts = [(v_hbm, v_ref), (x_hbm.at[:, at], x_ref.at[:, at]), (k_hbm, k_ref)]
    for by in (2, 1, 3, 0):
        parts += [columns_of(x_hbm, x_ref, width, down, by) for down in (1, 3, 0)]
    copies = started(parts, sems)
    copies[0].wait()
    vt_ref[...] = v_ref[...].T
    copies[1].wait()
    coded_chunk(vt_ref[...], x_ref, width, 1, 2, out_v)
    copies[2].wait()
    kt_ref[...] = k_ref[...].T
    for c in copies[3:6]:
        c.wait()
    coded_chunk(kt_ref[...], x_ref, width, 0, 2, out_k)
    for c in copies[6:]:
        c.wait()


def near_kernel(width, x_ref, kt_ref, vt_ref, *outs):
    for i, (m, by) in enumerate(((0, 1), (1, 1), (0, 3), (1, 3))):
        coded_chunk((kt_ref, vt_ref)[m][...], x_ref, width, m, by, outs[i])


def own_kernel(width, x_ref, kt_ref, vt_ref, *outs):
    for m in range(2):
        total = chunk((kt_ref, vt_ref)[m][...], x_ref, width, m, 0)
        for j in range(RING):
            outs[m][j] = total[:, j * width : (j + 1) * width]


def sum_kernel(own_ref, a_ref, b_ref, c_ref, total_ref, code_ref):
    for j in range(RING):
        total = (own_ref[j] + decode(a_ref, j)) + (decode(b_ref, j) + decode(c_ref, j))
        total_ref[j] = total
        encode(total, code_ref, j)


def exchange(blocks, axis):
    return [shift(blocks, axis, s) for s in (2, 1, 3)]


OFFSETS = (2, 3, 1)


def gather(block, first, second):
    line = jnp.stack([block, *[shift(block, first, s) for s in (1, 2, 3)]])
    return [line, *exchange(line, second)]


def row_block(m, offset, j):
    z, x = where_am_i()
    if m == 0:
        return j * RING + turn(x + offset)
    return turn(z + offset) * RING + j


def raw_kernel(width, m, left_ref, right_ref, before_ref, line_ref, a_ref, b_ref, c_ref, raw_ref, sums_ref, halves_ref):
    pre = None
    for p, (offset, ref) in enumerate(zip((0, *OFFSETS), (line_ref, a_ref, b_ref, c_ref))):
        for pair in range(2):
            lefts, rights = [], []
            for j in (2 * pair, 2 * pair + 1):
                lefts.append(left_ref[m, :, lanes(row_block(m, offset, j), width)])
                rights.append(ref[j] if p == 0 else decode(ref, j))
            both = split(jnp.concatenate(rights, axis=1))
            halves_ref[p * 2 + pair, 0] = both[0]
            halves_ref[p * 2 + pair, 1] = both[1]
            part = dot3(split(jnp.concatenate(lefts, axis=1)), both, ((1,), (1,)))
            pre = part if pre is None else pre + part
    raw = dot3(split(pre), split(right_ref[m]), ((1,), (0,)))
    raw_ref[...] = raw
    own = line_ref[where_am_i()[m]]
    lane = lax.broadcasted_iota(jnp.int32, (1, 128), 1)
    mine = jnp.where(lane < 64, jnp.sum(own * own), jnp.sum(raw * raw))
    sums_ref[...] = jnp.where((lane // 32) % 2 == m, mine, before_ref[...])


def weight_kernel(sums_ref, raw_k, raw_v, weights_ref, step_ref, new_ref, *narrow):
    total = jnp.sum(sums_ref[...], axis=0, keepdims=True)
    for m in range(2):
        grad_sq = total[:, m * 32 : m * 32 + 1]
        raw_sq = total[:, 64 + m * 32 : 64 + m * 32 + 1]
        step = jnp.sqrt(grad_sq / (raw_sq + norm_eps)) * (raw_k, raw_v)[m][...]
        new = weights_ref[m] - learn_rate * step
        step_ref[m] = step
        new_ref[m] = new
        narrow[m][...] = new.astype(jnp.bfloat16)


def stat_kernel(width, left_ref, right_ref, line_k, line_v, halves_k, halves_v, new_left_ref, new_right_ref):
    z, x = where_am_i()
    for m in range(2):
        own = split((line_k, line_v)[m][(z, x)[m]])
        gram = None
        for p, offset in enumerate((0, *OFFSETS)):
            for pair in range(2):
                halves = (halves_k, halves_v)[m]
                both = halves[p * 2 + pair, 0], halves[p * 2 + pair, 1]
                part = dot3(both, both, ((1,), (1,)))
                gram = part if gram is None else gram + part
                left = dot3(own, both, ((0,), (0,)))
                for n in range(2):
                    at = lanes(row_block(m, offset, 2 * pair + n), width)
                    new_left_ref[m, :, at] = (
                        decay_stat * left_ref[m, :, at]
                        + (1.0 - decay_stat) * left[:, n * width : (n + 1) * width]
                    )
        new_right_ref[m] = decay_stat * right_ref[m] + (1.0 - decay_stat) * gram


def place_kernel(width, *refs):
    pieces, out_ref, sems = refs[:-2], refs[-2], refs[-1]
    parts = []
    for m in range(2):
        me = where_am_i()[m]
        for piece, offset in zip(pieces[m * RING :], (0, *OFFSETS)):
            for back in range(RING):
                at = row_block(m, offset, turn(me + RING - back)) * width
                rows = pl.ds(pl.multiple_of(at, width), width)
                parts.append((piece.at[back], out_ref.at[m, rows, :]))
    for c in started(parts, sems):
        c.wait()


def on_device(
    saved_input, key_cot, value_cot, weights, left_root, left_stat, right_root, right_stat
):
    tokens, features = saved_input.shape
    rows, columns = weights.shape[1:]
    f32, bf16 = jnp.float32, jnp.bfloat16
    blocks = (RING, columns, rows)
    coded = (RING, columns + GROUPS, rows)

    x_hbm, k_hbm, v_hbm = [
        pltpu.with_memory_space_constraint(a, pltpu.HBM) for a in (saved_input, key_cot, value_cot)
    ]
    x_here, kt, vt, k2, v2 = call(
        functools.partial(first_kernel, rows),
        [
            pltpu.VMEM((tokens, features), bf16),
            pltpu.VMEM((columns, tokens), bf16),
            pltpu.VMEM((columns, tokens), bf16),
            pltpu.VMEM(coded, bf16),
            pltpu.VMEM(coded, bf16),
        ],
        [HBM] * 3,
        16,
        [
            pltpu.VMEM((tokens, columns), bf16),
            pltpu.VMEM((tokens, columns), bf16),
            pltpu.SemaphoreType.DMA((15,)),
        ],
    )(x_hbm, k_hbm, v_hbm)
    v2, k2 = shift(v2, Z, 2), shift(k2, X, 2)
    k1, v1, k3, v3 = call(
        functools.partial(near_kernel, rows), [pltpu.VMEM(coded, bf16)] * 4, [VMEM] * 3, 12
    )(x_here, kt, vt)
    k1, v1, k3, v3 = shift(k1, X, 1), shift(v1, Z, 1), shift(k3, X, 3), shift(v3, Z, 3)
    k0, v0 = call(
        functools.partial(own_kernel, rows), [pltpu.VMEM(blocks, f32)] * 2, [VMEM] * 3, 12
    )(x_here, kt, vt)

    add = call(sum_kernel, [pltpu.VMEM(blocks, f32), pltpu.VMEM(coded, bf16)], [VMEM] * 4, 16)
    v0, code_v = add(v0, v2, v1, v3)
    got_v = exchange(code_v, X)
    k0, code_k = add(k0, k2, k1, k3)
    got_k = exchange(code_k, Z)
    line_v, code_v = add(v0, *got_v)
    pieces_v = exchange(code_v, Z)
    line_k, code_k = add(k0, *got_k)
    pieces_k = exchange(code_k, X)

    def direction(m, before, line, pieces):
        return call(
            functools.partial(raw_kernel, rows, m),
            [
                pltpu.VMEM((rows, columns), f32),
                pltpu.VMEM((1, 128), f32),
                pltpu.VMEM((2 * RING, 2, columns, 2 * rows), bf16),
            ],
            [VMEM] * 7,
            12,
        )(left_root[:, 0], right_root[:, 0], before, line, *pieces)

    raw_v, sums, halves_v = direction(1, jnp.zeros((1, 128), f32), line_v, pieces_v)
    raw_k, sums, halves_k = direction(0, sums, line_k, pieces_k)

    everyone = lax.axis_size(FS_TP)
    spread = jnp.broadcast_to(sums[None], (everyone, 1, 128))
    sums = lax.all_to_all(spread, FS_TP, 0, 0, tiled=True).reshape(everyone, 128)
    step, new_weights, narrow_k, narrow_v = call(
        weight_kernel,
        [
            jax.ShapeDtypeStruct(weights.shape, f32),
            jax.ShapeDtypeStruct(weights.shape, f32),
            pltpu.VMEM((rows, columns), bf16),
            pltpu.VMEM((rows, columns), bf16),
        ],
        [VMEM] * 4,
        8,
    )(sums, raw_k, raw_v, weights)
    copied = gather(narrow_k, Z, X), gather(narrow_v, X, Z)

    new_left, new_right = call(
        functools.partial(stat_kernel, rows),
        [
            jax.ShapeDtypeStruct((2, rows, features), f32),
            jax.ShapeDtypeStruct((2, columns, columns), f32),
        ],
        [VMEM] * 6,
        20,
    )(left_stat[:, 0], right_stat[:, 0], line_k, line_v, halves_k, halves_v)

    copies = call(
        functools.partial(place_kernel, rows),
        jax.ShapeDtypeStruct((2, features, columns), bf16),
        [VMEM] * 8,
        4,
        [pltpu.SemaphoreType.DMA((32,))],
        out_specs=HBM,
    )(*copied[0], *copied[1])
    return (step, new_weights, copies, new_left[:, None], new_right[:, None])


def solution(mesh):
    rings = Mesh(mesh.devices.reshape(4, 4, 4, 2), ("fs_0", "fs_1", "tp_0", "tp_1"))
    in_specs = (
        P(FS, None),
        P(FS, TP),
        P(FS, TP),
        P(None, FS, TP),
        P(None, TP, FS, None),
        P(None, TP, FS, None),
        P(None, TP, None, None),
        P(None, TP, None, None),
    )
    out_specs = (
        P(None, FS, TP),
        P(None, FS, TP),
        P(None, None, TP),
        P(None, TP, FS, None),
        P(None, TP, None, None),
    )

    return jax.shard_map(
        on_device, mesh=rings, in_specs=in_specs, out_specs=out_specs, check_vma=False
    )
```

profile of v0, /device:TPU:0, one launch (start us, length us, event | category | flops | bytes accessed | tf_op | source)
XLA Modules:
  0.0 124.0 jit_solution(8475927567265732159)
XLA Ops:
  0.6 5.8 %shard_map.119 = (bf16[3072,2048]{1,0:T(8,128)(2,1)S(1)}, bf16[256,3072]{1,0:T(8,128)(2,1)S(1)}, bf16[256,3072]{1,0:T(8,128)(2,1)S(1)}, bf16[4,264,128]{2,1,0:T(8,128)(2,1)S(1)}, bf16[4,264,128]{2,1,0:T(8,128)(2,1)S(1)}) custom-call(bf16[3072,2048]{1,0:T(8,128)(2,1)} %x_hbm.1, bf16[3072,256]{1,0:T(8,128)(2,1)} %k_hbm.1, bf16[3072,256]{1,0:T(8,128)(2,1)} %v_hbm.1), custom_call_target="tpu_custom_call" | custom-call | tf_op jit(solution)/shard_map/pallas_call | solution.py:266
  6.4 4.4 %shard_map.121 = (bf16[4,264,128]{2,1,0:T(8,128)(2,1)S(1)}, bf16[4,264,128]{2,1,0:T(8,128)(2,1)S(1)}, bf16[4,264,128]{2,1,0:T(8,128)(2,1)S(1)}, bf16[4,264,128]{2,1,0:T(8,128)(2,1)S(1)}) custom-call(bf16[3072,2048]{1,0:T(8,128)(2,1)S(1)} %get-tuple-element.36.x_ref, bf16[256,3072]{1,0:T(8,128)(2,1)S(1)} %get-tuple-element.37.kt_ref, ...), custom_call_target="tpu_custom_call" | custom-call | tf_op jit(solution)/shard_map/pallas_call | solution.py:284
  10.9 2.1 %collective-permute-start.1 = (bf16[4,264,128]{2,1,0:T(8,128)(2,1)S(1)}, bf16[4,264,128]{2,1,0:T(8,128)(2,1)S(1)}, u32[]{:S(2)}, u32[]{:S(2)}) collective-permute-start(bf16[4,264,128]{2,1,0:T(8,128)(2,1)S(1)} %get-tuple-element.41), channel_id=1, source_target_pairs={{0,32},{32,64},{64,96},{96,0},{1,33},{33,65},{65,97},{97,1},{2,34}... | collective-permute-start | bytes 811016 | tf_op jit(solution)/shard_map/ppermute | solution.py:49
  12.9 2.2 %collective-permute-start.2 = (bf16[4,264,128]{2,1,0:T(8,128)(2,1)S(1)}, bf16[4,264,128]{2,1,0:T(8,128)(2,1)S(1)}, u32[]{:S(2)}, u32[]{:S(2)}) collective-permute-start(bf16[4,264,128]{2,1,0:T(8,128)(2,1)S(1)} %get-tuple-element.42), channel_id=1, source_target_pairs={{0,96},{32,0},{64,32},{96,64},{1,97},{33,1},{65,33},{97,65},{2,98}... | collective-permute-start | bytes 811016 | tf_op jit(solution)/shard_map/ppermute | solution.py:49
  15.1 1.8 %collective-permute-start = (bf16[4,264,128]{2,1,0:T(8,128)(2,1)S(1)}, bf16[4,264,128]{2,1,0:T(8,128)(2,1)S(1)}, u32[]{:S(2)}, u32[]{:S(2)}) collective-permute-start(bf16[4,264,128]{2,1,0:T(8,128)(2,1)S(1)} %get-tuple-element.40), channel_id=1, source_target_pairs={{0,64},{32,96},{64,0},{96,32},{1,65},{33,97},{65,1},{97,33},{2,66}... | collective-permute-start | bytes 811016 | tf_op jit(solution)/shard_map/ppermute | solution.py:49
  18.5 1.7 %collective-permute-start.11 = (bf16[4,264,128]{2,1,0:T(8,128)(2,1)S(1)}, bf16[4,264,128]{2,1,0:T(8,128)(2,1)S(1)}, u32[]{:S(2)}, u32[]{:S(2)}) collective-permute-start(bf16[4,264,128]{2,1,0:T(8,128)(2,1)S(1)} %get-tuple-element.51), channel_id=1, source_target_pairs={{0,24},{8,0},{16,8},{24,16},{1,25},{9,1},{17,9},{25,17},{2,26},{10... | collective-permute-start | bytes 811016 | tf_op jit(solution)/shard_map/ppermute | solution.py:49
  21.5 3.0 %collective-permute-start.9 = (bf16[4,264,128]{2,1,0:T(8,128)(2,1)S(1)}, bf16[4,264,128]{2,1,0:T(8,128)(2,1)S(1)}, u32[]{:S(2)}, u32[]{:S(2)}) collective-permute-start(bf16[4,264,128]{2,1,0:T(8,128)(2,1)S(1)} %get-tuple-element.49), channel_id=1, source_target_pairs={{0,16},{8,24},{16,0},{24,8},{1,17},{9,25},{17,1},{25,9},{2,18},{10... | collective-permute-start | bytes 811016 | tf_op jit(solution)/shard_map/ppermute | solution.py:49
  24.6 1.9 %shard_map.120 = (f32[4,256,128]{2,1,0:T(8,128)S(1)}, f32[4,256,128]{2,1,0:T(8,128)S(1)}) custom-call(bf16[3072,2048]{1,0:T(8,128)(2,1)S(1)} %get-tuple-element.36.x_ref, bf16[256,3072]{1,0:T(8,128)(2,1)S(1)} %get-tuple-element.37.kt_ref, bf16[256,3072]{1,0:T(8,128)(2,1)S(1)} %get-tuple-element.38.vt_ref), custom_call_target="tpu_custom_call" | custom-call | tf_op jit(solution)/shard_map/pallas_call | solution.py:288
  26.7 1.8 %collective-permute-done.a_ref = bf16[4,264,128]{2,1,0:T(8,128)(2,1)S(1)} collective-permute-done((bf16[4,264,128]{2,1,0:T(8,128)(2,1)S(1)}, bf16[4,264,128]{2,1,0:T(8,128)(2,1)S(1)}, u32[]{:S(2)}, u32[]{:S(2)}) %collective-permute-start) | collective-permute-done | bytes 270368 | tf_op jit(solution)/shard_map/ppermute | solution.py:49
  29.4 3.1 %collective-permute-start.3 = (bf16[4,264,128]{2,1,0:T(8,128)(2,1)S(1)}, bf16[4,264,128]{2,1,0:T(8,128)(2,1)S(1)}, u32[]{:S(2)}, u32[]{:S(2)}) collective-permute-start(bf16[4,264,128]{2,1,0:T(8,128)(2,1)S(1)} %get-tuple-element.44), channel_id=1, source_target_pairs={{0,16},{8,24},{16,0},{24,8},{1,17},{9,25},{17,1},{25,9},{2,18},{10... | collective-permute-start | bytes 811016 | tf_op jit(solution)/shard_map/ppermute | solution.py:49
  33.1 2.7 %collective-permute-start.5 = (bf16[4,264,128]{2,1,0:T(8,128)(2,1)S(1)}, bf16[4,264,128]{2,1,0:T(8,128)(2,1)S(1)}, u32[]{:S(2)}, u32[]{:S(2)}) collective-permute-start(bf16[4,264,128]{2,1,0:T(8,128)(2,1)S(1)} %get-tuple-element.44), channel_id=1, source_target_pairs={{0,24},{8,0},{16,8},{24,16},{1,25},{9,1},{17,9},{25,17},{2,26},{10... | collective-permute-start | bytes 811016 | tf_op jit(solution)/shard_map/ppermute | solution.py:49
  36.7 4.1 %collective-permute-start.12 = (bf16[4,264,128]{2,1,0:T(8,128)(2,1)S(1)}, bf16[4,264,128]{2,1,0:T(8,128)(2,1)S(1)}, u32[]{:S(2)}, u32[]{:S(2)}) collective-permute-start(bf16[4,264,128]{2,1,0:T(8,128)(2,1)S(1)} %get-tuple-element.53), channel_id=1, source_target_pairs={{0,64},{32,96},{64,0},{96,32},{1,65},{33,97},{65,1},{97,33},{2,66}... | collective-permute-start | bytes 811016 | tf_op jit(solution)/shard_map/ppermute | solution.py:49
  40.8 3.2 %collective-permute-start.14 = (bf16[4,264,128]{2,1,0:T(8,128)(2,1)S(1)}, bf16[4,264,128]{2,1,0:T(8,128)(2,1)S(1)}, u32[]{:S(2)}, u32[]{:S(2)}) collective-permute-start(bf16[4,264,128]{2,1,0:T(8,128)(2,1)S(1)} %get-tuple-element.53), channel_id=1, source_target_pairs={{0,96},{32,0},{64,32},{96,64},{1,97},{33,1},{65,33},{97,65},{2,98}... | collective-permute-start | bytes 811016 | tf_op jit(solution)/shard_map/ppermute | solution.py:49
  45.1 3.0 %collective-permute-start.6 = (bf16[4,264,128]{2,1,0:T(8,128)(2,1)S(1)}, bf16[4,264,128]{2,1,0:T(8,128)(2,1)S(1)}, u32[]{:S(2)}, u32[]{:S(2)}) collective-permute-start(bf16[4,264,128]{2,1,0:T(8,128)(2,1)S(1)} %get-tuple-element.46), channel_id=1, source_target_pairs={{0,64},{32,96},{64,0},{96,32},{1,65},{33,97},{65,1},{97,33},{2,66}... | collective-permute-start | bytes 811016 | tf_op jit(solution)/shard_map/ppermute | solution.py:49
  48.2 3.2 %collective-permute-start.8 = (bf16[4,264,128]{2,1,0:T(8,128)(2,1)S(1)}, bf16[4,264,128]{2,1,0:T(8,128)(2,1)S(1)}, u32[]{:S(2)}, u32[]{:S(2)}) collective-permute-start(bf16[4,264,128]{2,1,0:T(8,128)(2,1)S(1)} %get-tuple-element.46), channel_id=1, source_target_pairs={{0,96},{32,0},{64,32},{96,64},{1,97},{33,1},{65,33},{97,65},{2,98}... | collective-permute-start | bytes 811016 | tf_op jit(solution)/shard_map/ppermute | solution.py:49
  51.4 5.5 %collective-permute-done.13.b_ref = bf16[4,264,128]{2,1,0:T(8,128)(2,1)S(1)} collective-permute-done((bf16[4,264,128]{2,1,0:T(8,128)(2,1)S(1)}, bf16[4,264,128]{2,1,0:T(8,128)(2,1)S(1)}, u32[]{:S(2)}, u32[]{:S(2)}) %collective-permute-start.13) | collective-permute-done | bytes 270368 | tf_op jit(solution)/shard_map/ppermute | solution.py:49
  59.6 2.5 %collective-permute-start.17 = (bf16[4,264,128]{2,1,0:T(8,128)(2,1)S(1)}, bf16[4,264,128]{2,1,0:T(8,128)(2,1)S(1)}, u32[]{:S(2)}, u32[]{:S(2)}) collective-permute-start(bf16[4,264,128]{2,1,0:T(8,128)(2,1)S(1)} %get-tuple-element.55), channel_id=1, source_target_pairs={{0,24},{8,0},{16,8},{24,16},{1,25},{9,1},{17,9},{25,17},{2,26},{10... | collective-permute-start | bytes 811016 | tf_op jit(solution)/shard_map/ppermute | solution.py:49
  62.2 1.6 %shard_map.124 = (f32[128,256]{1,0:T(8,128)S(1)}, f32[1,128]{1,0:T(1,128)S(1)}, bf16[8,2,256,256]{3,2,1,0:T(8,128)(2,1)S(1)}) custom-call(f32[2,128,2048]{2,1,0:T(8,128)S(1)} %bitcast.20, f32[2,256,256]{2,1,0:T(8,128)S(1)} %bitcast.22, f32[1,128]{1,0:T(1,128)S(1)} %broadcast_in_dim.17.before_ref, f32[4,256,128]{2,1,0:T(8,128)S(1)} %get-tuple-element.45.line_ref.line_v, ...), custom_call_target="tpu_custom_call" | custom-call | tf_op jit(solution)/shard_map/pallas_call | solution.py:303
  63.8 2.2 %collective-permute-done.15.a_ref = bf16[4,264,128]{2,1,0:T(8,128)(2,1)S(1)} collective-permute-done((bf16[4,264,128]{2,1,0:T(8,128)(2,1)S(1)}, bf16[4,264,128]{2,1,0:T(8,128)(2,1)S(1)}, u32[]{:S(2)}, u32[]{:S(2)}) %collective-permute-start.15) | collective-permute-done | bytes 270368 | tf_op jit(solution)/shard_map/ppermute | solution.py:49
  66.0 2.8 %collective-permute-done.16.b_ref = bf16[4,264,128]{2,1,0:T(8,128)(2,1)S(1)} collective-permute-done((bf16[4,264,128]{2,1,0:T(8,128)(2,1)S(1)}, bf16[4,264,128]{2,1,0:T(8,128)(2,1)S(1)}, u32[]{:S(2)}, u32[]{:S(2)}) %collective-permute-start.16) | collective-permute-done | bytes 270368 | tf_op jit(solution)/shard_map/ppermute | solution.py:49
  68.8 1.6 %shard_map.127 = (f32[128,256]{1,0:T(8,128)S(1)}, f32[1,128]{1,0:T(1,128)S(1)}, bf16[8,2,256,256]{3,2,1,0:T(8,128)(2,1)S(1)}) custom-call(f32[2,128,2048]{2,1,0:T(8,128)S(1)} %bitcast.21, f32[2,256,256]{2,1,0:T(8,128)S(1)} %bitcast.23, f32[1,128]{1,0:T(1,128)S(1)} %get-tuple-element.47.before_ref, f32[4,256,128]{2,1,0:T(8,128)S(1)} %get-tuple-element.54.line_ref.line_k, ...), custom_call_target="tpu_custom_call" | custom-call | tf_op jit(solution)/shard_map/pallas_call | solution.py:303
  70.4 17.8 %all_to_all.5 = f32[128,1,128]{2,1,0:T(1,128)S(1)} all-to-all(f32[128,1,128]{2,1,0:T(1,128)S(1)} %broadcast_in_dim.19), channel_id=1, replica_groups=mesh['fs_0'=4,'fs_1'=4,'tp_0'=4,'tp_1'=2] {'fs_0','fs_1','tp_0','tp_1'}, dimensions={0} | all-to-all | bytes 131072 | tf_op jit(solution)/shard_map/all_to_all | solution.py:319
  90.5 2.1 %collective-permute-start.26 = (bf16[128,256]{1,0:T(8,128)(2,1)S(1)}, bf16[128,256]{1,0:T(8,128)(2,1)S(1)}, u32[]{:S(2)}, u32[]{:S(2)}) collective-permute-start(bf16[128,256]{1,0:T(8,128)(2,1)S(1)} %get-tuple-element.62), channel_id=1, source_target_pairs={{0,24},{8,0},{16,8},{24,16},{1,25},{9,1},{17,9},{25,17},{2,26},{10... | collective-permute-start | bytes 196616 | tf_op jit(solution)/shard_map/ppermute | solution.py:49
  92.5 3.0 %collective-permute-done.25 = bf16[128,256]{1,0:T(8,128)(2,1)S(1)} collective-permute-done((bf16[128,256]{1,0:T(8,128)(2,1)S(1)}, bf16[128,256]{1,0:T(8,128)(2,1)S(1)}, u32[]{:S(2)}, u32[]{:S(2)}) %collective-permute-start.25) | collective-permute-done | bytes 65568 | tf_op jit(solution)/shard_map/ppermute | solution.py:49
  95.5 2.5 %collective-permute-done.24 = bf16[128,256]{1,0:T(8,128)(2,1)S(1)} collective-permute-done((bf16[128,256]{1,0:T(8,128)(2,1)S(1)}, bf16[128,256]{1,0:T(8,128)(2,1)S(1)}, u32[]{:S(2)}, u32[]{:S(2)}) %collective-permute-start.24) | collective-permute-done | bytes 65568 | tf_op jit(solution)/shard_map/ppermute | solution.py:49
  99.9 3.2 %collective-permute-start.19 = (bf16[128,256]{1,0:T(8,128)(2,1)S(1)}, bf16[128,256]{1,0:T(8,128)(2,1)S(1)}, u32[]{:S(2)}, u32[]{:S(2)}) collective-permute-start(bf16[128,256]{1,0:T(8,128)(2,1)S(1)} %get-tuple-element.61), channel_id=1, source_target_pairs={{0,64},{32,96},{64,0},{96,32},{1,65},{33,97},{65,1},{97,33},{2,66}... | collective-permute-start | bytes 196616 | tf_op jit(solution)/shard_map/ppermute | solution.py:49
  105.1 3.3 %collective-permute-done.18 = bf16[128,256]{1,0:T(8,128)(2,1)S(1)} collective-permute-done((bf16[128,256]{1,0:T(8,128)(2,1)S(1)}, bf16[128,256]{1,0:T(8,128)(2,1)S(1)}, u32[]{:S(2)}, u32[]{:S(2)}) %collective-permute-start.18) | collective-permute-done | bytes 65568 | tf_op jit(solution)/shard_map/ppermute | solution.py:49
  108.4 2.3 %collective-permute-start.29 = (bf16[4,128,256]{2,1,0:T(8,128)(2,1)S(1)}, bf16[4,128,256]{2,1,0:T(8,128)(2,1)S(1)}, u32[]{:S(2)}, u32[]{:S(2)}) collective-permute-start(bf16[4,128,256]{2,1,0:T(8,128)(2,1)S(1)} %pad_maximum_fusion.1.refs_4_), channel_id=1, source_target_pairs={{0,96},{32,0},{64,32},{96,64},{1,97},{33,1},{65,33},{97,65},{2,98}... | collective-permute-start | bytes 786440 | tf_op jit(solution)/shard_map/ppermute | solution.py:49
  112.6 2.4 %collective-permute-start.23 = (bf16[4,128,256]{2,1,0:T(8,128)(2,1)S(1)}, bf16[4,128,256]{2,1,0:T(8,128)(2,1)S(1)}, u32[]{:S(2)}, u32[]{:S(2)}) collective-permute-start(bf16[4,128,256]{2,1,0:T(8,128)(2,1)S(1)} %pad_maximum_fusion.refs_0_), channel_id=1, source_target_pairs={{0,24},{8,0},{16,8},{24,16},{1,25},{9,1},{17,9},{25,17},{2,26},{10... | collective-permute-start | bytes 786440 | tf_op jit(solution)/shard_map/ppermute | solution.py:49
  115.1 4.2 %shard_map.130 = (f32[2,128,2048]{2,1,0:T(8,128)}, f32[2,256,256]{2,1,0:T(8,128)}) custom-call(f32[2,128,2048]{2,1,0:T(8,128)S(1)} %bitcast.24, f32[2,256,256]{2,1,0:T(8,128)S(1)} %bitcast.25, f32[4,256,128]{2,1,0:T(8,128)S(1)} %get-tuple-element.54.line_ref.line_k, f32[4,256,128]{2,1,0:T(8,128)S(1)} %get-tuple-element.45.line_ref.line_v, ...), custom_call_target="tpu_custom_call" | custom-call | tf_op jit(solution)/shard_map/pallas_call | solution.py:333
  119.7 2.5 %collective-permute-done.22.refs_2_ = bf16[4,128,256]{2,1,0:T(8,128)(2,1)S(1)} collective-permute-done((bf16[4,128,256]{2,1,0:T(8,128)(2,1)S(1)}, bf16[4,128,256]{2,1,0:T(8,128)(2,1)S(1)}, u32[]{:S(2)}, u32[]{:S(2)}) %collective-permute-start.22) | collective-permute-done | bytes 262176 | tf_op jit(solution)/shard_map/ppermute | solution.py:49
  122.2 1.6 %shard_map.129 = bf16[2,2048,256]{2,1,0:T(8,128)(2,1)} custom-call(bf16[4,128,256]{2,1,0:T(8,128)(2,1)S(1)} %pad_maximum_fusion.refs_0_, bf16[4,128,256]{2,1,0:T(8,128)(2,1)S(1)} %collective-permute-done.21.refs_1_, bf16[4,128,256]{2,1,0:T(8,128)(2,1)S(1)} %collective-permute-done.22.refs_2_, bf16[4,128,256]{2,1,0:T(8,128)(2,1)S(1)} %collective-permute-done.23.refs_3_, ...), custom_call_target="tpu_custom_call" | custom-call | tf_op jit(solution)/shard_map/pallas_call | solution.py:343
  (55 shorter events, 17.7 us)
Async XLA Ops:
  10.9 10.7 %collective-permute-start.1 = (bf16[4,264,128]{2,1,0:T(8,128)(2,1)S(1)}, bf16[4,264,128]{2,1,0:T(8,128)(2,1)S(1)}, u32[]{:S(2)}, u32[]{:S(2)}) collective-permute-start(bf16[4,264,128]{2,1,0:T(8,128)(2,1)S(1)} %get-tuple-element.41), channel_id=1, source_target_pairs={{0,32},{32,64},{64,96},{96,0},{1,33},{33,65},{65,97},{97,1},{2,34}... | collective-permute-start | bytes 811016 | tf_op jit(solution)/shard_map/ppermute | solution.py:49
  12.9 13.8 %collective-permute-start.2 = (bf16[4,264,128]{2,1,0:T(8,128)(2,1)S(1)}, bf16[4,264,128]{2,1,0:T(8,128)(2,1)S(1)}, u32[]{:S(2)}, u32[]{:S(2)}) collective-permute-start(bf16[4,264,128]{2,1,0:T(8,128)(2,1)S(1)} %get-tuple-element.42), channel_id=1, source_target_pairs={{0,96},{32,0},{64,32},{96,64},{1,97},{33,1},{65,33},{97,65},{2,98}... | collective-permute-start | bytes 811016 | tf_op jit(solution)/shard_map/ppermute | solution.py:49
  15.1 13.4 %collective-permute-start = (bf16[4,264,128]{2,1,0:T(8,128)(2,1)S(1)}, bf16[4,264,128]{2,1,0:T(8,128)(2,1)S(1)}, u32[]{:S(2)}, u32[]{:S(2)}) collective-permute-start(bf16[4,264,128]{2,1,0:T(8,128)(2,1)S(1)} %get-tuple-element.40), channel_id=1, source_target_pairs={{0,64},{32,96},{64,0},{96,32},{1,65},{33,97},{65,1},{97,33},{2,66}... | collective-permute-start | bytes 811016 | tf_op jit(solution)/shard_map/ppermute | solution.py:49
  16.9 16.2 %collective-permute-start.10 = (bf16[4,264,128]{2,1,0:T(8,128)(2,1)S(1)}, bf16[4,264,128]{2,1,0:T(8,128)(2,1)S(1)}, u32[]{:S(2)}, u32[]{:S(2)}) collective-permute-start(bf16[4,264,128]{2,1,0:T(8,128)(2,1)S(1)} %get-tuple-element.50), channel_id=1, source_target_pairs={{0,8},{8,16},{16,24},{24,0},{1,9},{9,17},{17,25},{25,1},{2,10},{10... | collective-permute-start | bytes 811016 | tf_op jit(solution)/shard_map/ppermute | solution.py:49
  18.5 17.3 %collective-permute-start.11 = (bf16[4,264,128]{2,1,0:T(8,128)(2,1)S(1)}, bf16[4,264,128]{2,1,0:T(8,128)(2,1)S(1)}, u32[]{:S(2)}, u32[]{:S(2)}) collective-permute-start(bf16[4,264,128]{2,1,0:T(8,128)(2,1)S(1)} %get-tuple-element.51), channel_id=1, source_target_pairs={{0,24},{8,0},{16,8},{24,16},{1,25},{9,1},{17,9},{25,17},{2,26},{10... | collective-permute-start | bytes 811016 | tf_op jit(solution)/shard_map/ppermute | solution.py:49
  21.5 14.3 %collective-permute-start.9 = (bf16[4,264,128]{2,1,0:T(8,128)(2,1)S(1)}, bf16[4,264,128]{2,1,0:T(8,128)(2,1)S(1)}, u32[]{:S(2)}, u32[]{:S(2)}) collective-permute-start(bf16[4,264,128]{2,1,0:T(8,128)(2,1)S(1)} %get-tuple-element.49), channel_id=1, source_target_pairs={{0,16},{8,24},{16,0},{24,8},{1,17},{9,25},{17,1},{25,9},{2,18},{10... | collective-permute-start | bytes 811016 | tf_op jit(solution)/shard_map/ppermute | solution.py:49
  29.4 11.4 %collective-permute-start.3 = (bf16[4,264,128]{2,1,0:T(8,128)(2,1)S(1)}, bf16[4,264,128]{2,1,0:T(8,128)(2,1)S(1)}, u32[]{:S(2)}, u32[]{:S(2)}) collective-permute-start(bf16[4,264,128]{2,1,0:T(8,128)(2,1)S(1)} %get-tuple-element.44), channel_id=1, source_target_pairs={{0,16},{8,24},{16,0},{24,8},{1,17},{9,25},{17,1},{25,9},{2,18},{10... | collective-permute-start | bytes 811016 | tf_op jit(solution)/shard_map/ppermute | solution.py:49
  32.5 11.6 %collective-permute-start.4 = (bf16[4,264,128]{2,1,0:T(8,128)(2,1)S(1)}, bf16[4,264,128]{2,1,0:T(8,128)(2,1)S(1)}, u32[]{:S(2)}, u32[]{:S(2)}) collective-permute-start(bf16[4,264,128]{2,1,0:T(8,128)(2,1)S(1)} %get-tuple-element.44), channel_id=1, source_target_pairs={{0,8},{8,16},{16,24},{24,0},{1,9},{9,17},{17,25},{25,1},{2,10},{10... | collective-permute-start | bytes 811016 | tf_op jit(solution)/shard_map/ppermute | solution.py:49
  33.1 11.1 %collective-permute-start.5 = (bf16[4,264,128]{2,1,0:T(8,128)(2,1)S(1)}, bf16[4,264,128]{2,1,0:T(8,128)(2,1)S(1)}, u32[]{:S(2)}, u32[]{:S(2)}) collective-permute-start(bf16[4,264,128]{2,1,0:T(8,128)(2,1)S(1)} %get-tuple-element.44), channel_id=1, source_target_pairs={{0,24},{8,0},{16,8},{24,16},{1,25},{9,1},{17,9},{25,17},{2,26},{10... | collective-permute-start | bytes 811016 | tf_op jit(solution)/shard_map/ppermute | solution.py:49
  36.7 11.5 %collective-permute-start.12 = (bf16[4,264,128]{2,1,0:T(8,128)(2,1)S(1)}, bf16[4,264,128]{2,1,0:T(8,128)(2,1)S(1)}, u32[]{:S(2)}, u32[]{:S(2)}) collective-permute-start(bf16[4,264,128]{2,1,0:T(8,128)(2,1)S(1)} %get-tuple-element.53), channel_id=1, source_target_pairs={{0,64},{32,96},{64,0},{96,32},{1,65},{33,97},{65,1},{97,33},{2,66}... | collective-permute-start | bytes 811016 | tf_op jit(solution)/shard_map/ppermute | solution.py:49
  40.8 16.1 %collective-permute-start.13 = (bf16[4,264,128]{2,1,0:T(8,128)(2,1)S(1)}, bf16[4,264,128]{2,1,0:T(8,128)(2,1)S(1)}, u32[]{:S(2)}, u32[]{:S(2)}) collective-permute-start(bf16[4,264,128]{2,1,0:T(8,128)(2,1)S(1)} %get-tuple-element.53), channel_id=1, source_target_pairs={{0,32},{32,64},{64,96},{96,0},{1,33},{33,65},{65,97},{97,1},{2,34}... | collective-permute-start | bytes 811016 | tf_op jit(solution)/shard_map/ppermute | solution.py:49
  40.8 16.1 %collective-permute-start.14 = (bf16[4,264,128]{2,1,0:T(8,128)(2,1)S(1)}, bf16[4,264,128]{2,1,0:T(8,128)(2,1)S(1)}, u32[]{:S(2)}, u32[]{:S(2)}) collective-permute-start(bf16[4,264,128]{2,1,0:T(8,128)(2,1)S(1)} %get-tuple-element.53), channel_id=1, source_target_pairs={{0,96},{32,0},{64,32},{96,64},{1,97},{33,1},{65,33},{97,65},{2,98}... | collective-permute-start | bytes 811016 | tf_op jit(solution)/shard_map/ppermute | solution.py:49
  45.1 14.5 %collective-permute-start.6 = (bf16[4,264,128]{2,1,0:T(8,128)(2,1)S(1)}, bf16[4,264,128]{2,1,0:T(8,128)(2,1)S(1)}, u32[]{:S(2)}, u32[]{:S(2)}) collective-permute-start(bf16[4,264,128]{2,1,0:T(8,128)(2,1)S(1)} %get-tuple-element.46), channel_id=1, source_target_pairs={{0,64},{32,96},{64,0},{96,32},{1,65},{33,97},{65,1},{97,33},{2,66}... | collective-permute-start | bytes 811016 | tf_op jit(solution)/shard_map/ppermute | solution.py:49
  48.1 14.0 %collective-permute-start.7 = (bf16[4,264,128]{2,1,0:T(8,128)(2,1)S(1)}, bf16[4,264,128]{2,1,0:T(8,128)(2,1)S(1)}, u32[]{:S(2)}, u32[]{:S(2)}) collective-permute-start(bf16[4,264,128]{2,1,0:T(8,128)(2,1)S(1)} %get-tuple-element.46), channel_id=1, source_target_pairs={{0,32},{32,64},{64,96},{96,0},{1,33},{33,65},{65,97},{97,1},{2,34}... | collective-permute-start | bytes 811016 | tf_op jit(solution)/shard_map/ppermute | solution.py:49
  48.2 14.0 %collective-permute-start.8 = (bf16[4,264,128]{2,1,0:T(8,128)(2,1)S(1)}, bf16[4,264,128]{2,1,0:T(8,128)(2,1)S(1)}, u32[]{:S(2)}, u32[]{:S(2)}) collective-permute-start(bf16[4,264,128]{2,1,0:T(8,128)(2,1)S(1)} %get-tuple-element.46), channel_id=1, source_target_pairs={{0,96},{32,0},{64,32},{96,64},{1,97},{33,1},{65,33},{97,65},{2,98}... | collective-permute-start | bytes 811016 | tf_op jit(solution)/shard_map/ppermute | solution.py:49
  57.8 8.1 %collective-permute-start.15 = (bf16[4,264,128]{2,1,0:T(8,128)(2,1)S(1)}, bf16[4,264,128]{2,1,0:T(8,128)(2,1)S(1)}, u32[]{:S(2)}, u32[]{:S(2)}) collective-permute-start(bf16[4,264,128]{2,1,0:T(8,128)(2,1)S(1)} %get-tuple-element.55), channel_id=1, source_target_pairs={{0,16},{8,24},{16,0},{24,8},{1,17},{9,25},{17,1},{25,9},{2,18},{10... | collective-permute-start | bytes 811016 | tf_op jit(solution)/shard_map/ppermute | solution.py:49
  58.9 9.9 %collective-permute-start.16 = (bf16[4,264,128]{2,1,0:T(8,128)(2,1)S(1)}, bf16[4,264,128]{2,1,0:T(8,128)(2,1)S(1)}, u32[]{:S(2)}, u32[]{:S(2)}) collective-permute-start(bf16[4,264,128]{2,1,0:T(8,128)(2,1)S(1)} %get-tuple-element.55), channel_id=1, source_target_pairs={{0,8},{8,16},{16,24},{24,0},{1,9},{9,17},{17,25},{25,1},{2,10},{10... | collective-permute-start | bytes 811016 | tf_op jit(solution)/shard_map/ppermute | solution.py:49
  59.6 9.2 %collective-permute-start.17 = (bf16[4,264,128]{2,1,0:T(8,128)(2,1)S(1)}, bf16[4,264,128]{2,1,0:T(8,128)(2,1)S(1)}, u32[]{:S(2)}, u32[]{:S(2)}) collective-permute-start(bf16[4,264,128]{2,1,0:T(8,128)(2,1)S(1)} %get-tuple-element.55), channel_id=1, source_target_pairs={{0,24},{8,0},{16,8},{24,16},{1,25},{9,1},{17,9},{25,17},{2,26},{10... | collective-permute-start | bytes 811016 | tf_op jit(solution)/shard_map/ppermute | solution.py:49
  68.8 46.3 %copy-start.2 = (f32[2,1,128,2048]{3,2,1,0:T(8,128)S(1)}, f32[2,1,128,2048]{3,2,1,0:T(8,128)}, u32[]{:S(2)}) copy-start(f32[2,1,128,2048]{3,2,1,0:T(8,128)} %param.13) | copy-start | bytes 6291460
  68.8 46.3 %copy-start.3 = (f32[2,1,256,256]{3,2,1,0:T(8,128)S(1)}, f32[2,1,256,256]{3,2,1,0:T(8,128)}, u32[]{:S(2)}) copy-start(f32[2,1,256,256]{3,2,1,0:T(8,128)} %param.15) | copy-start | bytes 1572868
  89.3 6.2 %collective-permute-start.25 = (bf16[128,256]{1,0:T(8,128)(2,1)S(1)}, bf16[128,256]{1,0:T(8,128)(2,1)S(1)}, u32[]{:S(2)}, u32[]{:S(2)}) collective-permute-start(bf16[128,256]{1,0:T(8,128)(2,1)S(1)} %get-tuple-element.62), channel_id=1, source_target_pairs={{0,16},{8,24},{16,0},{24,8},{1,17},{9,25},{17,1},{25,9},{2,18},{10... | collective-permute-start | bytes 196616 | tf_op jit(solution)/shard_map/ppermute | solution.py:49
  90.5 5.0 %collective-permute-start.26 = (bf16[128,256]{1,0:T(8,128)(2,1)S(1)}, bf16[128,256]{1,0:T(8,128)(2,1)S(1)}, u32[]{:S(2)}, u32[]{:S(2)}) collective-permute-start(bf16[128,256]{1,0:T(8,128)(2,1)S(1)} %get-tuple-element.62), channel_id=1, source_target_pairs={{0,24},{8,0},{16,8},{24,16},{1,25},{9,1},{17,9},{25,17},{2,26},{10... | collective-permute-start | bytes 196616 | tf_op jit(solution)/shard_map/ppermute | solution.py:49
  92.5 5.5 %collective-permute-start.24 = (bf16[128,256]{1,0:T(8,128)(2,1)S(1)}, bf16[128,256]{1,0:T(8,128)(2,1)S(1)}, u32[]{:S(2)}, u32[]{:S(2)}) collective-permute-start(bf16[128,256]{1,0:T(8,128)(2,1)S(1)} %get-tuple-element.62), channel_id=1, source_target_pairs={{0,8},{8,16},{16,24},{24,0},{1,9},{9,17},{17,25},{25,1},{2,10},{10... | collective-permute-start | bytes 196616 | tf_op jit(solution)/shard_map/ppermute | solution.py:49
  98.0 14.6 %collective-permute-start.27 = (bf16[4,128,256]{2,1,0:T(8,128)(2,1)S(1)}, bf16[4,128,256]{2,1,0:T(8,128)(2,1)S(1)}, u32[]{:S(2)}, u32[]{:S(2)}) collective-permute-start(bf16[4,128,256]{2,1,0:T(8,128)(2,1)S(1)} %pad_maximum_fusion.1.refs_4_), channel_id=1, source_target_pairs={{0,64},{32,96},{64,0},{96,32},{1,65},{33,97},{65,1},{97,33},{2,66}... | collective-permute-start | bytes 786440 | tf_op jit(solution)/shard_map/ppermute | solution.py:49
  99.4 9.0 %collective-permute-start.18 = (bf16[128,256]{1,0:T(8,128)(2,1)S(1)}, bf16[128,256]{1,0:T(8,128)(2,1)S(1)}, u32[]{:S(2)}, u32[]{:S(2)}) collective-permute-start(bf16[128,256]{1,0:T(8,128)(2,1)S(1)} %get-tuple-element.61), channel_id=1, source_target_pairs={{0,32},{32,64},{64,96},{96,0},{1,33},{33,65},{65,97},{97,1},{2,34}... | collective-permute-start | bytes 196616 | tf_op jit(solution)/shard_map/ppermute | solution.py:49
  99.9 11.7 %collective-permute-start.19 = (bf16[128,256]{1,0:T(8,128)(2,1)S(1)}, bf16[128,256]{1,0:T(8,128)(2,1)S(1)}, u32[]{:S(2)}, u32[]{:S(2)}) collective-permute-start(bf16[128,256]{1,0:T(8,128)(2,1)S(1)} %get-tuple-element.61), channel_id=1, source_target_pairs={{0,64},{32,96},{64,0},{96,32},{1,65},{33,97},{65,1},{97,33},{2,66}... | collective-permute-start | bytes 196616 | tf_op jit(solution)/shard_map/ppermute | solution.py:49
  103.1 8.5 %collective-permute-start.20 = (bf16[128,256]{1,0:T(8,128)(2,1)S(1)}, bf16[128,256]{1,0:T(8,128)(2,1)S(1)}, u32[]{:S(2)}, u32[]{:S(2)}) collective-permute-start(bf16[128,256]{1,0:T(8,128)(2,1)S(1)} %get-tuple-element.61), channel_id=1, source_target_pairs={{0,96},{32,0},{64,32},{96,64},{1,97},{33,1},{65,33},{97,65},{2,98}... | collective-permute-start | bytes 196616 | tf_op jit(solution)/shard_map/ppermute | solution.py:49
  104.3 15.0 %collective-permute-start.28 = (bf16[4,128,256]{2,1,0:T(8,128)(2,1)S(1)}, bf16[4,128,256]{2,1,0:T(8,128)(2,1)S(1)}, u32[]{:S(2)}, u32[]{:S(2)}) collective-permute-start(bf16[4,128,256]{2,1,0:T(8,128)(2,1)S(1)} %pad_maximum_fusion.1.refs_4_), channel_id=1, source_target_pairs={{0,32},{32,64},{64,96},{96,0},{1,33},{33,65},{65,97},{97,1},{2,34}... | collective-permute-start | bytes 786440 | tf_op jit(solution)/shard_map/ppermute | solution.py:49
  108.4 10.8 %collective-permute-start.29 = (bf16[4,128,256]{2,1,0:T(8,128)(2,1)S(1)}, bf16[4,128,256]{2,1,0:T(8,128)(2,1)S(1)}, u32[]{:S(2)}, u32[]{:S(2)}) collective-permute-start(bf16[4,128,256]{2,1,0:T(8,128)(2,1)S(1)} %pad_maximum_fusion.1.refs_4_), channel_id=1, source_target_pairs={{0,96},{32,0},{64,32},{96,64},{1,97},{33,1},{65,33},{97,65},{2,98}... | collective-permute-start | bytes 786440 | tf_op jit(solution)/shard_map/ppermute | solution.py:49
  111.7 8.1 %collective-permute-start.21 = (bf16[4,128,256]{2,1,0:T(8,128)(2,1)S(1)}, bf16[4,128,256]{2,1,0:T(8,128)(2,1)S(1)}, u32[]{:S(2)}, u32[]{:S(2)}) collective-permute-start(bf16[4,128,256]{2,1,0:T(8,128)(2,1)S(1)} %pad_maximum_fusion.refs_0_), channel_id=1, source_target_pairs={{0,16},{8,24},{16,0},{24,8},{1,17},{9,25},{17,1},{25,9},{2,18},{10... | collective-permute-start | bytes 786440 | tf_op jit(solution)/shard_map/ppermute | solution.py:49
  111.7 10.5 %collective-permute-start.22 = (bf16[4,128,256]{2,1,0:T(8,128)(2,1)S(1)}, bf16[4,128,256]{2,1,0:T(8,128)(2,1)S(1)}, u32[]{:S(2)}, u32[]{:S(2)}) collective-permute-start(bf16[4,128,256]{2,1,0:T(8,128)(2,1)S(1)} %pad_maximum_fusion.refs_0_), channel_id=1, source_target_pairs={{0,8},{8,16},{16,24},{24,0},{1,9},{9,17},{17,25},{25,1},{2,10},{10... | collective-permute-start | bytes 786440 | tf_op jit(solution)/shard_map/ppermute | solution.py:49
  112.6 9.6 %collective-permute-start.23 = (bf16[4,128,256]{2,1,0:T(8,128)(2,1)S(1)}, bf16[4,128,256]{2,1,0:T(8,128)(2,1)S(1)}, u32[]{:S(2)}, u32[]{:S(2)}) collective-permute-start(bf16[4,128,256]{2,1,0:T(8,128)(2,1)S(1)} %pad_maximum_fusion.refs_0_), channel_id=1, source_target_pairs={{0,24},{8,0},{16,8},{24,16},{1,25},{9,1},{17,9},{25,17},{2,26},{10... | collective-permute-start | bytes 786440 | tf_op jit(solution)/shard_map/ppermute | solution.py:49
  (3 other events, 90.1 us)
where the time goes:
time: 124 us
  starting transfers between devices  52.7 us (42%)
  waiting for transfers between devices  26.7 us (22%)
  Pallas kernels  25.6 us (21%)
  blocking collectives  17.8 us (14%)
    ppermute x30, starting transfers between devices, shift(): lax.ppermute(value, axis, [(i, (i + by) % RING) for i in range(RING)])  52.7 us
    ppermute x30, waiting for transfers between devices, shift(): lax.ppermute(value, axis, [(i, (i + by) % RING) for i in range(RING)])  26.7 us
    all_to_all x1, blocking collectives, on_device(): lax.all_to_all(spread, FS_TP, 0, 0, tiled=True).reshape(everyone, 128)  17.8 us
    pallas_call x1, Pallas kernels, on_device(): call(functools.partial(first_kernel, rows), [pltpu.VMEM((tokens, features...  5.81 us
    pallas_call x1, Pallas kernels, on_device(): call(functools.partial(near_kernel, rows), [pltpu.VMEM(coded, bf16)] * 4,...  4.41 us
    pallas_call x1, Pallas kernels, on_device(): call(functools.partial(stat_kernel, rows), [jax.ShapeDtypeStruct((2, rows...  4.17 us
    pallas_call x2, Pallas kernels, direction(): call(functools.partial(raw_kernel, rows, m), [pltpu.VMEM((rows, columns),...  3.12 us
  transfers between devices with their start and end apart: 30, of which 15 were waited for; matrix products, arithmetic and copies ran while one was open for 0% of the time, Pallas kernels for 9%

commit v1 on v0

--- a/solution.py
+++ b/solution.py
@@ -128,16 +128,16 @@
 def first_kernel(width, x_hbm, k_hbm, v_hbm, x_ref, kt_ref, vt_ref, out_k, out_v, k_ref, v_ref, sems):
     z, _ = where_am_i()
     at = lanes(turn(z + 2), RING * width)
-    parts = [(v_hbm, v_ref), (x_hbm.at[:, at], x_ref.at[:, at]), (k_hbm, k_ref)]
+    parts = [(v_hbm, v_ref), (k_hbm, k_ref), (x_hbm.at[:, at], x_ref.at[:, at])]
     for by in (2, 1, 3, 0):
         parts += [columns_of(x_hbm, x_ref, width, down, by) for down in (1, 3, 0)]
     copies = started(parts, sems)
     copies[0].wait()
     vt_ref[...] = v_ref[...].T
     copies[1].wait()
+    kt_ref[...] = k_ref[...].T
+    copies[2].wait()
     coded_chunk(vt_ref[...], x_ref, width, 1, 2, out_v)
-    copies[2].wait()
-    kt_ref[...] = k_ref[...].T
     for c in copies[3:6]:
         c.wait()
     coded_chunk(kt_ref[...], x_ref, width, 0, 2, out_k)
@@ -146,7 +146,7 @@
 
 
 def near_kernel(width, x_ref, kt_ref, vt_ref, *outs):
-    for i, (m, by) in enumerate(((0, 1), (1, 1), (0, 3), (1, 3))):
+    for i, (m, by) in enumerate(((1, 1), (0, 1), (1, 3), (0, 3))):
         coded_chunk((kt_ref, vt_ref)[m][...], x_ref, width, m, by, outs[i])
 
 
@@ -171,11 +171,6 @@
 OFFSETS = (2, 3, 1)
 
 
-def gather(block, first, second):
-    line = jnp.stack([block, *[shift(block, first, s) for s in (1, 2, 3)]])
-    return [line, *exchange(line, second)]
-
-
 def row_block(m, offset, j):
     z, x = where_am_i()
     if m == 0:
@@ -183,7 +178,7 @@
     return turn(z + offset) * RING + j
 
 
-def raw_kernel(width, m, left_ref, right_ref, before_ref, line_ref, a_ref, b_ref, c_ref, raw_ref, sums_ref, halves_ref):
+def raw_kernel(width, m, left_ref, right_ref, before_ref, weights_ref, line_ref, a_ref, b_ref, c_ref, raw_ref, sums_ref, halves_ref):
     pre = None
     for p, (offset, ref) in enumerate(zip((0, *OFFSETS), (line_ref, a_ref, b_ref, c_ref))):
         for pair in range(2):
@@ -197,23 +192,29 @@
             part = dot3(split(jnp.concatenate(lefts, axis=1)), both, ((1,), (1,)))
             pre = part if pre is None else pre + part
     raw = dot3(split(pre), split(right_ref[m]), ((1,), (0,)))
-    raw_ref[...] = raw
+    raw_ref[0] = raw
+    raw_ref[1] = weights_ref[m]
     own = line_ref[where_am_i()[m]]
     lane = lax.broadcasted_iota(jnp.int32, (1, 128), 1)
     mine = jnp.where(lane < 64, jnp.sum(own * own), jnp.sum(raw * raw))
     sums_ref[...] = jnp.where((lane // 32) % 2 == m, mine, before_ref[...])
 
 
-def weight_kernel(sums_ref, raw_k, raw_v, weights_ref, step_ref, new_ref, *narrow):
+def weight_kernel(sums_ref, *refs):
+    ins, (step_ref, new_ref, *lines) = refs[: 2 * RING], refs[2 * RING :]
     total = jnp.sum(sums_ref[...], axis=0, keepdims=True)
     for m in range(2):
         grad_sq = total[:, m * 32 : m * 32 + 1]
         raw_sq = total[:, 64 + m * 32 : 64 + m * 32 + 1]
-        step = jnp.sqrt(grad_sq / (raw_sq + norm_eps)) * (raw_k, raw_v)[m][...]
-        new = weights_ref[m] - learn_rate * step
-        step_ref[m] = step
-        new_ref[m] = new
-        narrow[m][...] = new.astype(jnp.bfloat16)
+        scale = jnp.sqrt(grad_sq / (raw_sq + norm_eps))
+        for back in range(RING):
+            ref = ins[m * RING + back]
+            step = scale * ref[0]
+            new = ref[1] - learn_rate * step
+            if back == 0:
+                step_ref[m] = step
+                new_ref[m] = new
+            lines[m][back] = new.astype(jnp.bfloat16)
 
 
 def stat_kernel(width, left_ref, right_ref, line_k, line_v, halves_k, halves_v, new_left_ref, new_right_ref):
@@ -237,16 +238,15 @@
         new_right_ref[m] = decay_stat * right_ref[m] + (1.0 - decay_stat) * gram
 
 
-def place_kernel(width, *refs):
-    pieces, out_ref, sems = refs[:-2], refs[-2], refs[-1]
+def place_kernel(width, chosen, *refs):
+    out_ref, sems = refs[-2:]
     parts = []
-    for m in range(2):
-        me = where_am_i()[m]
-        for piece, offset in zip(pieces[m * RING :], (0, *OFFSETS)):
-            for back in range(RING):
-                at = row_block(m, offset, turn(me + RING - back)) * width
-                rows = pl.ds(pl.multiple_of(at, width), width)
-                parts.append((piece.at[back], out_ref.at[m, rows, :]))
+    for piece, (m, p) in zip(refs, chosen):
+        me, offset = where_am_i()[1 - m], (0, *OFFSETS)[p]
+        for back in range(RING):
+            at = row_block(1 - m, offset, turn(me + RING - back)) * width
+            rows = pl.ds(pl.multiple_of(at, width), width)
+            parts.append((piece.at[back], out_ref.at[m, rows, :]))
     for c in started(parts, sems):
         c.wait()
 
@@ -281,13 +281,12 @@
         ],
     )(x_hbm, k_hbm, v_hbm)
     v2, k2 = shift(v2, Z, 2), shift(k2, X, 2)
-    k1, v1, k3, v3 = call(
+    v1, k1, v3, k3 = call(
         functools.partial(near_kernel, rows), [pltpu.VMEM(coded, bf16)] * 4, [VMEM] * 3, 12
     )(x_here, kt, vt)
-    k1, v1, k3, v3 = shift(k1, X, 1), shift(v1, Z, 1), shift(k3, X, 3), shift(v3, Z, 3)
-    k0, v0 = call(
-        functools.partial(own_kernel, rows), [pltpu.VMEM(blocks, f32)] * 2, [VMEM] * 3, 12
-    )(x_here, kt, vt)
+    v1, k1 = shift(v1, Z, 1), shift(k1, X, 1)
+    v3, k3 = shift(v3, Z, 3), shift(k3, X, 3)
+    k0, v0 = call(functools.partial(own_kernel, rows), [pltpu.VMEM(blocks, f32)] * 2, [VMEM] * 3, 12)(x_here, kt, vt)
 
     add = call(sum_kernel, [pltpu.VMEM(blocks, f32), pltpu.VMEM(coded, bf16)], [VMEM] * 4, 16)
     v0, code_v = add(v0, v2, v1, v3)
@@ -303,32 +302,35 @@
         return call(
             functools.partial(raw_kernel, rows, m),
             [
-                pltpu.VMEM((rows, columns), f32),
+                pltpu.VMEM((2, rows, columns), f32),
                 pltpu.VMEM((1, 128), f32),
                 pltpu.VMEM((2 * RING, 2, columns, 2 * rows), bf16),
             ],
-            [VMEM] * 7,
+            [VMEM] * 8,
             12,
-        )(left_root[:, 0], right_root[:, 0], before, line, *pieces)
-
-    raw_v, sums, halves_v = direction(1, jnp.zeros((1, 128), f32), line_v, pieces_v)
-    raw_k, sums, halves_k = direction(0, sums, line_k, pieces_k)
+        )(left_root[:, 0], right_root[:, 0], before, weights, line, *pieces)
+
+    value, sums, halves_v = direction(1, jnp.zeros((1, 128), f32), line_v, pieces_v)
+    values = [value, *[shift(value, Z, s) for s in (1, 2, 3)]]
+    key, sums, halves_k = direction(0, sums, line_k, pieces_k)
+    keys = [key, *[shift(key, X, s) for s in (1, 2, 3)]]
 
     everyone = lax.axis_size(FS_TP)
     spread = jnp.broadcast_to(sums[None], (everyone, 1, 128))
     sums = lax.all_to_all(spread, FS_TP, 0, 0, tiled=True).reshape(everyone, 128)
-    step, new_weights, narrow_k, narrow_v = call(
+    step, new_weights, copied_k, copied_v = call(
         weight_kernel,
         [
             jax.ShapeDtypeStruct(weights.shape, f32),
             jax.ShapeDtypeStruct(weights.shape, f32),
-            pltpu.VMEM((rows, columns), bf16),
-            pltpu.VMEM((rows, columns), bf16),
+            pltpu.VMEM((RING, rows, columns), bf16),
+            pltpu.VMEM((RING, rows, columns), bf16),
         ],
-        [VMEM] * 4,
-        8,
-    )(sums, raw_k, raw_v, weights)
-    copied = gather(narrow_k, Z, X), gather(narrow_v, X, Z)
+        [VMEM] * 9,
+        10,
+    )(sums, *keys, *values)
+    copied_v = [copied_v, *exchange(copied_v, X)]
+    copied_k = [copied_k, *exchange(copied_k, Z)]
 
     new_left, new_right = call(
         functools.partial(stat_kernel, rows),
@@ -340,14 +342,20 @@
         20,
     )(left_stat[:, 0], right_stat[:, 0], line_k, line_v, halves_k, halves_v)
 
-    copies = call(
-        functools.partial(place_kernel, rows),
-        jax.ShapeDtypeStruct((2, features, columns), bf16),
-        [VMEM] * 8,
-        4,
-        [pltpu.SemaphoreType.DMA((32,))],
-        out_specs=HBM,
-    )(*copied[0], *copied[1])
+    def placed(chosen, *before):
+        return call(
+            functools.partial(place_kernel, rows, chosen),
+            jax.ShapeDtypeStruct((2, features, columns), bf16),
+            [VMEM] * len(chosen) + [HBM] * len(before),
+            4,
+            [pltpu.SemaphoreType.DMA((RING * len(chosen),))],
+            out_specs=HBM,
+            aliases={len(chosen): 0} if before else None,
+        )(*[(copied_k, copied_v)[m][p] for m, p in chosen], *before)
+
+    copies = placed([(1, 0), (0, 0), (1, 1), (0, 1)])
+    copies = placed([(1, 2), (0, 2)], copies)
+    copies = placed([(1, 3), (0, 3)], copies)
     return (step, new_weights, copies, new_left[:, None], new_right[:, None])
 
 
@@ -371,6 +379,4 @@
         P(None, TP, None, None),
     )
 
-    return jax.shard_map(
-        on_device, mesh=rings, in_specs=in_specs, out_specs=out_specs, check_vma=False
-    )
+    return jax.shard_map(on_device, mesh=rings, in_specs=in_specs, out_specs=out_specs, check_vma=False)

time: 124 us -> 118 us (0.952)
  the two profiles are of different devices: /device:TPU:0 before, /device:TPU:1 now
where the time goes in v1:
time: 118 us
  starting transfers between devices  41.3 us (35%)
  Pallas kernels  26.8 us (23%)
  blocking collectives  25 us (21%)
  waiting for transfers between devices  23.9 us (20%)
    ppermute x30, starting transfers between devices, shift(): lax.ppermute(value, axis, [(i, (i + by) % RING) for i in range(RING)])  41.3 us
    all_to_all x1, blocking collectives, on_device(): lax.all_to_all(spread, FS_TP, 0, 0, tiled=True).reshape(everyone, 128)  25 us
    ppermute x30, waiting for transfers between devices, shift(): lax.ppermute(value, axis, [(i, (i + by) % RING) for i in range(RING)])  23.9 us
    pallas_call x1, Pallas kernels, on_device(): call(functools.partial(first_kernel, rows), [pltpu.VMEM((tokens, features...  5.79 us
    pallas_call x1, Pallas kernels, on_device(): call(functools.partial(near_kernel, rows), [pltpu.VMEM(coded, bf16)] * 4,...  4.4 us
    pallas_call x1, Pallas kernels, on_device(): call(functools.partial(stat_kernel, rows), [jax.ShapeDtypeStruct((2, rows...  4.18 us
    pallas_call x2, Pallas kernels, direction(): call(functools.partial(raw_kernel, rows, m), [pltpu.VMEM((2, rows, column...  3.12 us
    pallas_call x3, Pallas kernels, placed(): call(functools.partial(place_kernel, rows, chosen), jax.ShapeDtypeStruct(...  2.8 us
  transfers between devices with their start and end apart: 30, of which 10 were waited for; matrix products, arithmetic and copies ran while one was open for 0% of the time, Pallas kernels for 11%

profile of v1, /device:TPU:1, one launch (start us, length us, event | category | flops | bytes accessed | tf_op | source)
XLA Modules:
  0.0 118.2 jit_solution(9320480519707342677)
XLA Ops:
  0.6 5.8 %shard_map.119 = (bf16[3072,2048]{1,0:T(8,128)(2,1)S(1)}, bf16[256,3072]{1,0:T(8,128)(2,1)S(1)}, bf16[256,3072]{1,0:T(8,128)(2,1)S(1)}, bf16[4,264,128]{2,1,0:T(8,128)(2,1)S(1)}, bf16[4,264,128]{2,1,0:T(8,128)(2,1)S(1)}) custom-call(bf16[3072,2048]{1,0:T(8,128)(2,1)} %x_hbm.1, bf16[3072,256]{1,0:T(8,128)(2,1)} %k_hbm.1, bf16[3072,256]{1,0:T(8,128)(2,1)} %v_hbm.1), custom_call_target="tpu_custom_call" | custom-call | tf_op jit(solution)/shard_map/pallas_call | solution.py:266
  6.4 4.4 %shard_map.121 = (bf16[4,264,128]{2,1,0:T(8,128)(2,1)S(1)}, bf16[4,264,128]{2,1,0:T(8,128)(2,1)S(1)}, bf16[4,264,128]{2,1,0:T(8,128)(2,1)S(1)}, bf16[4,264,128]{2,1,0:T(8,128)(2,1)S(1)}) custom-call(bf16[3072,2048]{1,0:T(8,128)(2,1)S(1)} %get-tuple-element.36.x_ref, bf16[256,3072]{1,0:T(8,128)(2,1)S(1)} %get-tuple-element.37.kt_ref, ...), custom_call_target="tpu_custom_call" | custom-call | tf_op jit(solution)/shard_map/pallas_call | solution.py:284
  10.8 2.5 %collective-permute-start.1 = (bf16[4,264,128]{2,1,0:T(8,128)(2,1)S(1)}, bf16[4,264,128]{2,1,0:T(8,128)(2,1)S(1)}, u32[]{:S(2)}, u32[]{:S(2)}) collective-permute-start(bf16[4,264,128]{2,1,0:T(8,128)(2,1)S(1)} %get-tuple-element.41), channel_id=1, source_target_pairs={{0,32},{32,64},{64,96},{96,0},{1,33},{33,65},{65,97},{97,1},{2,34}... | collective-permute-start | bytes 811016 | tf_op jit(solution)/shard_map/ppermute | solution.py:49
  13.3 2.2 %collective-permute-start.2 = (bf16[4,264,128]{2,1,0:T(8,128)(2,1)S(1)}, bf16[4,264,128]{2,1,0:T(8,128)(2,1)S(1)}, u32[]{:S(2)}, u32[]{:S(2)}) collective-permute-start(bf16[4,264,128]{2,1,0:T(8,128)(2,1)S(1)} %get-tuple-element.42), channel_id=1, source_target_pairs={{0,96},{32,0},{64,32},{96,64},{1,97},{33,1},{65,33},{97,65},{2,98}... | collective-permute-start | bytes 811016 | tf_op jit(solution)/shard_map/ppermute | solution.py:49
  15.5 1.3 %collective-permute-start = (bf16[4,264,128]{2,1,0:T(8,128)(2,1)S(1)}, bf16[4,264,128]{2,1,0:T(8,128)(2,1)S(1)}, u32[]{:S(2)}, u32[]{:S(2)}) collective-permute-start(bf16[4,264,128]{2,1,0:T(8,128)(2,1)S(1)} %get-tuple-element.40), channel_id=1, source_target_pairs={{0,64},{32,96},{64,0},{96,32},{1,65},{33,97},{65,1},{97,33},{2,66}... | collective-permute-start | bytes 811016 | tf_op jit(solution)/shard_map/ppermute | solution.py:49
  16.8 1.2 %collective-permute-start.10 = (bf16[4,264,128]{2,1,0:T(8,128)(2,1)S(1)}, bf16[4,264,128]{2,1,0:T(8,128)(2,1)S(1)}, u32[]{:S(2)}, u32[]{:S(2)}) collective-permute-start(bf16[4,264,128]{2,1,0:T(8,128)(2,1)S(1)} %get-tuple-element.50), channel_id=1, source_target_pairs={{0,8},{8,16},{16,24},{24,0},{1,9},{9,17},{17,25},{25,1},{2,10},{10... | collective-permute-start | bytes 811016 | tf_op jit(solution)/shard_map/ppermute | solution.py:49
  18.0 1.5 %collective-permute-start.11 = (bf16[4,264,128]{2,1,0:T(8,128)(2,1)S(1)}, bf16[4,264,128]{2,1,0:T(8,128)(2,1)S(1)}, u32[]{:S(2)}, u32[]{:S(2)}) collective-permute-start(bf16[4,264,128]{2,1,0:T(8,128)(2,1)S(1)} %get-tuple-element.51), channel_id=1, source_target_pairs={{0,24},{8,0},{16,8},{24,16},{1,25},{9,1},{17,9},{25,17},{2,26},{10... | collective-permute-start | bytes 811016 | tf_op jit(solution)/shard_map/ppermute | solution.py:49
  19.5 2.2 %collective-permute-done.1.b_ref = bf16[4,264,128]{2,1,0:T(8,128)(2,1)S(1)} collective-permute-done((bf16[4,264,128]{2,1,0:T(8,128)(2,1)S(1)}, bf16[4,264,128]{2,1,0:T(8,128)(2,1)S(1)}, u32[]{:S(2)}, u32[]{:S(2)}) %collective-permute-start.1) | collective-permute-done | bytes 270368 | tf_op jit(solution)/shard_map/ppermute | solution.py:49
  21.6 2.8 %collective-permute-start.9 = (bf16[4,264,128]{2,1,0:T(8,128)(2,1)S(1)}, bf16[4,264,128]{2,1,0:T(8,128)(2,1)S(1)}, u32[]{:S(2)}, u32[]{:S(2)}) collective-permute-start(bf16[4,264,128]{2,1,0:T(8,128)(2,1)S(1)} %get-tuple-element.49), channel_id=1, source_target_pairs={{0,16},{8,24},{16,0},{24,8},{1,17},{9,25},{17,1},{25,9},{2,18},{10... | collective-permute-start | bytes 811016 | tf_op jit(solution)/shard_map/ppermute | solution.py:49
  24.4 1.9 %shard_map.120 = (f32[4,256,128]{2,1,0:T(8,128)S(1)}, f32[4,256,128]{2,1,0:T(8,128)S(1)}) custom-call(bf16[3072,2048]{1,0:T(8,128)(2,1)S(1)} %get-tuple-element.36.x_ref, bf16[256,3072]{1,0:T(8,128)(2,1)S(1)} %get-tuple-element.37.kt_ref, bf16[256,3072]{1,0:T(8,128)(2,1)S(1)} %get-tuple-element.38.vt_ref), custom_call_target="tpu_custom_call" | custom-call | tf_op jit(solution)/shard_map/pallas_call | solution.py:289
  26.3 2.0 %collective-permute-done.a_ref = bf16[4,264,128]{2,1,0:T(8,128)(2,1)S(1)} collective-permute-done((bf16[4,264,128]{2,1,0:T(8,128)(2,1)S(1)}, bf16[4,264,128]{2,1,0:T(8,128)(2,1)S(1)}, u32[]{:S(2)}, u32[]{:S(2)}) %collective-permute-start) | collective-permute-done | bytes 270368 | tf_op jit(solution)/shard_map/ppermute | solution.py:49
  29.2 2.8 %collective-permute-start.3 = (bf16[4,264,128]{2,1,0:T(8,128)(2,1)S(1)}, bf16[4,264,128]{2,1,0:T(8,128)(2,1)S(1)}, u32[]{:S(2)}, u32[]{:S(2)}) collective-permute-start(bf16[4,264,128]{2,1,0:T(8,128)(2,1)S(1)} %get-tuple-element.44), channel_id=1, source_target_pairs={{0,16},{8,24},{16,0},{24,8},{1,17},{9,25},{17,1},{25,9},{2,18},{10... | collective-permute-start | bytes 811016 | tf_op jit(solution)/shard_map/ppermute | solution.py:49
  32.4 2.4 %collective-permute-start.5 = (bf16[4,264,128]{2,1,0:T(8,128)(2,1)S(1)}, bf16[4,264,128]{2,1,0:T(8,128)(2,1)S(1)}, u32[]{:S(2)}, u32[]{:S(2)}) collective-permute-start(bf16[4,264,128]{2,1,0:T(8,128)(2,1)S(1)} %get-tuple-element.44), channel_id=1, source_target_pairs={{0,24},{8,0},{16,8},{24,16},{1,25},{9,1},{17,9},{25,17},{2,26},{10... | collective-permute-start | bytes 811016 | tf_op jit(solution)/shard_map/ppermute | solution.py:49
  35.8 1.3 %collective-permute-start.13 = (bf16[4,264,128]{2,1,0:T(8,128)(2,1)S(1)}, bf16[4,264,128]{2,1,0:T(8,128)(2,1)S(1)}, u32[]{:S(2)}, u32[]{:S(2)}) collective-permute-start(bf16[4,264,128]{2,1,0:T(8,128)(2,1)S(1)} %get-tuple-element.53), channel_id=1, source_target_pairs={{0,32},{32,64},{64,96},{96,0},{1,33},{33,65},{65,97},{97,1},{2,34}... | collective-permute-start | bytes 811016 | tf_op jit(solution)/shard_map/ppermute | solution.py:49
  37.3 1.4 %collective-permute-start.14 = (bf16[4,264,128]{2,1,0:T(8,128)(2,1)S(1)}, bf16[4,264,128]{2,1,0:T(8,128)(2,1)S(1)}, u32[]{:S(2)}, u32[]{:S(2)}) collective-permute-start(bf16[4,264,128]{2,1,0:T(8,128)(2,1)S(1)} %get-tuple-element.53), channel_id=1, source_target_pairs={{0,96},{32,0},{64,32},{96,64},{1,97},{33,1},{65,33},{97,65},{2,98}... | collective-permute-start | bytes 811016 | tf_op jit(solution)/shard_map/ppermute | solution.py:49
  38.7 5.9 %collective-permute-done.4.b_ref = bf16[4,264,128]{2,1,0:T(8,128)(2,1)S(1)} collective-permute-done((bf16[4,264,128]{2,1,0:T(8,128)(2,1)S(1)}, bf16[4,264,128]{2,1,0:T(8,128)(2,1)S(1)}, u32[]{:S(2)}, u32[]{:S(2)}) %collective-permute-start.4) | collective-permute-done | bytes 270368 | tf_op jit(solution)/shard_map/ppermute | solution.py:49
  45.6 1.4 %collective-permute-start.6 = (bf16[4,264,128]{2,1,0:T(8,128)(2,1)S(1)}, bf16[4,264,128]{2,1,0:T(8,128)(2,1)S(1)}, u32[]{:S(2)}, u32[]{:S(2)}) collective-permute-start(bf16[4,264,128]{2,1,0:T(8,128)(2,1)S(1)} %get-tuple-element.46), channel_id=1, source_target_pairs={{0,64},{32,96},{64,0},{96,32},{1,65},{33,97},{65,1},{97,33},{2,66}... | collective-permute-start | bytes 811016 | tf_op jit(solution)/shard_map/ppermute | solution.py:49
  47.0 2.6 %collective-permute-start.8 = (bf16[4,264,128]{2,1,0:T(8,128)(2,1)S(1)}, bf16[4,264,128]{2,1,0:T(8,128)(2,1)S(1)}, u32[]{:S(2)}, u32[]{:S(2)}) collective-permute-start(bf16[4,264,128]{2,1,0:T(8,128)(2,1)S(1)} %get-tuple-element.46), channel_id=1, source_target_pairs={{0,96},{32,0},{64,32},{96,64},{1,97},{33,1},{65,33},{97,65},{2,98}... | collective-permute-start | bytes 811016 | tf_op jit(solution)/shard_map/ppermute | solution.py:49
  50.6 3.1 %collective-permute-start.15 = (bf16[4,264,128]{2,1,0:T(8,128)(2,1)S(1)}, bf16[4,264,128]{2,1,0:T(8,128)(2,1)S(1)}, u32[]{:S(2)}, u32[]{:S(2)}) collective-permute-start(bf16[4,264,128]{2,1,0:T(8,128)(2,1)S(1)} %get-tuple-element.55), channel_id=1, source_target_pairs={{0,16},{8,24},{16,0},{24,8},{1,17},{9,25},{17,1},{25,9},{2,18},{10... | collective-permute-start | bytes 811016 | tf_op jit(solution)/shard_map/ppermute | solution.py:49
  53.9 1.8 %collective-permute-done.6.a_ref = bf16[4,264,128]{2,1,0:T(8,128)(2,1)S(1)} collective-permute-done((bf16[4,264,128]{2,1,0:T(8,128)(2,1)S(1)}, bf16[4,264,128]{2,1,0:T(8,128)(2,1)S(1)}, u32[]{:S(2)}, u32[]{:S(2)}) %collective-permute-start.6) | collective-permute-done | bytes 270368 | tf_op jit(solution)/shard_map/ppermute | solution.py:49
  56.4 5.6 %collective-permute-done.7.b_ref = bf16[4,264,128]{2,1,0:T(8,128)(2,1)S(1)} collective-permute-done((bf16[4,264,128]{2,1,0:T(8,128)(2,1)S(1)}, bf16[4,264,128]{2,1,0:T(8,128)(2,1)S(1)}, u32[]{:S(2)}, u32[]{:S(2)}) %collective-permute-start.7) | collective-permute-done | bytes 270368 | tf_op jit(solution)/shard_map/ppermute | solution.py:49
  62.0 1.6 %shard_map.124 = (f32[2,128,256]{2,1,0:T(8,128)S(1)}, f32[1,128]{1,0:T(1,128)S(1)}, bf16[8,2,256,256]{3,2,1,0:T(8,128)(2,1)S(1)}) custom-call(f32[2,128,2048]{2,1,0:T(8,128)S(1)} %bitcast.12, f32[2,256,256]{2,1,0:T(8,128)S(1)} %bitcast.14, f32[1,128]{1,0:T(1,128)S(1)} %broadcast_in_dim.17.before_ref, f32[2,128,256]{2,1,0:T(8,128)S(1)} %copy-done.3, ...), custom_call_target="tpu_custom_call" | custom-call | tf_op jit(solution)/shard_map/pallas_call | solution.py:302
  63.6 1.6 %shard_map.127 = (f32[2,128,256]{2,1,0:T(8,128)S(1)}, f32[1,128]{1,0:T(1,128)S(1)}, bf16[8,2,256,256]{3,2,1,0:T(8,128)(2,1)S(1)}) custom-call(f32[2,128,2048]{2,1,0:T(8,128)S(1)} %bitcast.13, f32[2,256,256]{2,1,0:T(8,128)S(1)} %bitcast.15, f32[1,128]{1,0:T(1,128)S(1)} %get-tuple-element.47.before_ref, f32[2,128,256]{2,1,0:T(8,128)S(1)} %copy-done.3, ...), custom_call_target="tpu_custom_call" | custom-call | tf_op jit(solution)/shard_map/pallas_call | solution.py:302
  66.2 1.9 %collective-permute-start.19 = (f32[2,128,256]{2,1,0:T(8,128)S(1)}, f32[2,128,256]{2,1,0:T(8,128)S(1)}, u32[]{:S(2)}, u32[]{:S(2)}) collective-permute-start(f32[2,128,256]{2,1,0:T(8,128)S(1)} %get-tuple-element.57.refs_0_), channel_id=1, source_target_pairs={{0,16},{8,24},{16,0},{24,8},{1,17},{9,25},{17,1},{25,9},{2,18},{10... | collective-permute-start | bytes 786440 | tf_op jit(solution)/shard_map/ppermute | solution.py:49
  68.9 2.5 %collective-permute-start.21 = (f32[2,128,256]{2,1,0:T(8,128)S(1)}, f32[2,128,256]{2,1,0:T(8,128)S(1)}, u32[]{:S(2)}, u32[]{:S(2)}) collective-permute-start(f32[2,128,256]{2,1,0:T(8,128)S(1)} %get-tuple-element.58.refs_4_), channel_id=1, source_target_pairs={{0,32},{32,64},{64,96},{96,0},{1,33},{33,65},{65,97},{97,1},{2,34}... | collective-permute-start | bytes 786440 | tf_op jit(solution)/shard_map/ppermute | solution.py:49
  72.3 1.5 %collective-permute-start.23 = (f32[2,128,256]{2,1,0:T(8,128)S(1)}, f32[2,128,256]{2,1,0:T(8,128)S(1)}, u32[]{:S(2)}, u32[]{:S(2)}) collective-permute-start(f32[2,128,256]{2,1,0:T(8,128)S(1)} %get-tuple-element.58.refs_4_), channel_id=1, source_target_pairs={{0,96},{32,0},{64,32},{96,64},{1,97},{33,1},{65,33},{97,65},{2,98}... | collective-permute-start | bytes 786440 | tf_op jit(solution)/shard_map/ppermute | solution.py:49
  73.8 25.0 %all_to_all.5 = f32[128,1,128]{2,1,0:T(1,128)S(1)} all-to-all(f32[128,1,128]{2,1,0:T(1,128)S(1)} %broadcast_in_dim.19), channel_id=1, replica_groups=mesh['fs_0'=4,'fs_1'=4,'tp_0'=4,'tp_1'=2] {'fs_0','fs_1','tp_0','tp_1'}, dimensions={0} | all-to-all | bytes 131072 | tf_op jit(solution)/shard_map/all_to_all | solution.py:320
  102.6 2.2 %collective-permute-start.24 = (bf16[4,128,256]{2,1,0:T(8,128)(2,1)S(1)}, bf16[4,128,256]{2,1,0:T(8,128)(2,1)S(1)}, u32[]{:S(2)}, u32[]{:S(2)}) collective-permute-start(bf16[4,128,256]{2,1,0:T(8,128)(2,1)S(1)} %get-tuple-element.61.refs_0_), channel_id=1, source_target_pairs={{0,24},{8,0},{16,8},{24,16},{1,25},{9,1},{17,9},{25,17},{2,26},{10... | collective-permute-start | bytes 786440 | tf_op jit(solution)/shard_map/ppermute | solution.py:49
  104.8 3.7 %collective-permute-done.28.refs_2_ = bf16[4,128,256]{2,1,0:T(8,128)(2,1)S(1)} collective-permute-done((bf16[4,128,256]{2,1,0:T(8,128)(2,1)S(1)}, bf16[4,128,256]{2,1,0:T(8,128)(2,1)S(1)}, u32[]{:S(2)}, u32[]{:S(2)}) %collective-permute-start.28) | collective-permute-done | bytes 262176 | tf_op jit(solution)/shard_map/ppermute | solution.py:49
  108.5 4.2 %shard_map.132 = (f32[2,128,2048]{2,1,0:T(8,128)}, f32[2,256,256]{2,1,0:T(8,128)}) custom-call(f32[2,128,2048]{2,1,0:T(8,128)S(1)} %bitcast.16, f32[2,256,256]{2,1,0:T(8,128)S(1)} %bitcast.17, f32[4,256,128]{2,1,0:T(8,128)S(1)} %get-tuple-element.54.line_ref.line_k, f32[4,256,128]{2,1,0:T(8,128)S(1)} %get-tuple-element.45.line_ref.line_v, ...), custom_call_target="tpu_custom_call" | custom-call | tf_op jit(solution)/shard_map/pallas_call | solution.py:335
  112.7 1.1 shard_map.129.refs_2_
  113.8 1.4 %collective-permute-done.26.refs_0_ = bf16[4,128,256]{2,1,0:T(8,128)(2,1)S(1)} collective-permute-done((bf16[4,128,256]{2,1,0:T(8,128)(2,1)S(1)}, bf16[4,128,256]{2,1,0:T(8,128)(2,1)S(1)}, u32[]{:S(2)}, u32[]{:S(2)}) %collective-permute-start.26) | collective-permute-done | bytes 262176 | tf_op jit(solution)/shard_map/ppermute | solution.py:49
  (55 shorter events, 14.6 us)
Async XLA Ops:
  10.8 10.8 %collective-permute-start.1 = (bf16[4,264,128]{2,1,0:T(8,128)(2,1)S(1)}, bf16[4,264,128]{2,1,0:T(8,128)(2,1)S(1)}, u32[]{:S(2)}, u32[]{:S(2)}) collective-permute-start(bf16[4,264,128]{2,1,0:T(8,128)(2,1)S(1)} %get-tuple-element.41), channel_id=1, source_target_pairs={{0,32},{32,64},{64,96},{96,0},{1,33},{33,65},{65,97},{97,1},{2,34}... | collective-permute-start | bytes 811016 | tf_op jit(solution)/shard_map/ppermute | solution.py:49
  13.3 13.0 %collective-permute-start.2 = (bf16[4,264,128]{2,1,0:T(8,128)(2,1)S(1)}, bf16[4,264,128]{2,1,0:T(8,128)(2,1)S(1)}, u32[]{:S(2)}, u32[]{:S(2)}) collective-permute-start(bf16[4,264,128]{2,1,0:T(8,128)(2,1)S(1)} %get-tuple-element.42), channel_id=1, source_target_pairs={{0,96},{32,0},{64,32},{96,64},{1,97},{33,1},{65,33},{97,65},{2,98}... | collective-permute-start | bytes 811016 | tf_op jit(solution)/shard_map/ppermute | solution.py:49
  15.5 12.8 %collective-permute-start = (bf16[4,264,128]{2,1,0:T(8,128)(2,1)S(1)}, bf16[4,264,128]{2,1,0:T(8,128)(2,1)S(1)}, u32[]{:S(2)}, u32[]{:S(2)}) collective-permute-start(bf16[4,264,128]{2,1,0:T(8,128)(2,1)S(1)} %get-tuple-element.40), channel_id=1, source_target_pairs={{0,64},{32,96},{64,0},{96,32},{1,65},{33,97},{65,1},{97,33},{2,66}... | collective-permute-start | bytes 811016 | tf_op jit(solution)/shard_map/ppermute | solution.py:49
  16.8 15.6 %collective-permute-start.10 = (bf16[4,264,128]{2,1,0:T(8,128)(2,1)S(1)}, bf16[4,264,128]{2,1,0:T(8,128)(2,1)S(1)}, u32[]{:S(2)}, u32[]{:S(2)}) collective-permute-start(bf16[4,264,128]{2,1,0:T(8,128)(2,1)S(1)} %get-tuple-element.50), channel_id=1, source_target_pairs={{0,8},{8,16},{16,24},{24,0},{1,9},{9,17},{17,25},{25,1},{2,10},{10... | collective-permute-start | bytes 811016 | tf_op jit(solution)/shard_map/ppermute | solution.py:49
  18.0 16.8 %collective-permute-start.11 = (bf16[4,264,128]{2,1,0:T(8,128)(2,1)S(1)}, bf16[4,264,128]{2,1,0:T(8,128)(2,1)S(1)}, u32[]{:S(2)}, u32[]{:S(2)}) collective-permute-start(bf16[4,264,128]{2,1,0:T(8,128)(2,1)S(1)} %get-tuple-element.51), channel_id=1, source_target_pairs={{0,24},{8,0},{16,8},{24,16},{1,25},{9,1},{17,9},{25,17},{2,26},{10... | collective-permute-start | bytes 811016 | tf_op jit(solution)/shard_map/ppermute | solution.py:49
  21.6 13.2 %collective-permute-start.9 = (bf16[4,264,128]{2,1,0:T(8,128)(2,1)S(1)}, bf16[4,264,128]{2,1,0:T(8,128)(2,1)S(1)}, u32[]{:S(2)}, u32[]{:S(2)}) collective-permute-start(bf16[4,264,128]{2,1,0:T(8,128)(2,1)S(1)} %get-tuple-element.49), channel_id=1, source_target_pairs={{0,16},{8,24},{16,0},{24,8},{1,17},{9,25},{17,1},{25,9},{2,18},{10... | collective-permute-start | bytes 811016 | tf_op jit(solution)/shard_map/ppermute | solution.py:49
  29.2 8.1 %collective-permute-start.3 = (bf16[4,264,128]{2,1,0:T(8,128)(2,1)S(1)}, bf16[4,264,128]{2,1,0:T(8,128)(2,1)S(1)}, u32[]{:S(2)}, u32[]{:S(2)}) collective-permute-start(bf16[4,264,128]{2,1,0:T(8,128)(2,1)S(1)} %get-tuple-element.44), channel_id=1, source_target_pairs={{0,16},{8,24},{16,0},{24,8},{1,17},{9,25},{17,1},{25,9},{2,18},{10... | collective-permute-start | bytes 811016 | tf_op jit(solution)/shard_map/ppermute | solution.py:49
  32.1 12.6 %collective-permute-start.4 = (bf16[4,264,128]{2,1,0:T(8,128)(2,1)S(1)}, bf16[4,264,128]{2,1,0:T(8,128)(2,1)S(1)}, u32[]{:S(2)}, u32[]{:S(2)}) collective-permute-start(bf16[4,264,128]{2,1,0:T(8,128)(2,1)S(1)} %get-tuple-element.44), channel_id=1, source_target_pairs={{0,8},{8,16},{16,24},{24,0},{1,9},{9,17},{17,25},{25,1},{2,10},{10... | collective-permute-start | bytes 811016 | tf_op jit(solution)/shard_map/ppermute | solution.py:49
  32.4 12.3 %collective-permute-start.5 = (bf16[4,264,128]{2,1,0:T(8,128)(2,1)S(1)}, bf16[4,264,128]{2,1,0:T(8,128)(2,1)S(1)}, u32[]{:S(2)}, u32[]{:S(2)}) collective-permute-start(bf16[4,264,128]{2,1,0:T(8,128)(2,1)S(1)} %get-tuple-element.44), channel_id=1, source_target_pairs={{0,24},{8,0},{16,8},{24,16},{1,25},{9,1},{17,9},{25,17},{2,26},{10... | collective-permute-start | bytes 811016 | tf_op jit(solution)/shard_map/ppermute | solution.py:49
  35.7 11.3 %collective-permute-start.12 = (bf16[4,264,128]{2,1,0:T(8,128)(2,1)S(1)}, bf16[4,264,128]{2,1,0:T(8,128)(2,1)S(1)}, u32[]{:S(2)}, u32[]{:S(2)}) collective-permute-start(bf16[4,264,128]{2,1,0:T(8,128)(2,1)S(1)} %get-tuple-element.53), channel_id=1, source_target_pairs={{0,64},{32,96},{64,0},{96,32},{1,65},{33,97},{65,1},{97,33},{2,66}... | collective-permute-start | bytes 811016 | tf_op jit(solution)/shard_map/ppermute | solution.py:49
  35.8 13.9 %collective-permute-start.13 = (bf16[4,264,128]{2,1,0:T(8,128)(2,1)S(1)}, bf16[4,264,128]{2,1,0:T(8,128)(2,1)S(1)}, u32[]{:S(2)}, u32[]{:S(2)}) collective-permute-start(bf16[4,264,128]{2,1,0:T(8,128)(2,1)S(1)} %get-tuple-element.53), channel_id=1, source_target_pairs={{0,32},{32,64},{64,96},{96,0},{1,33},{33,65},{65,97},{97,1},{2,34}... | collective-permute-start | bytes 811016 | tf_op jit(solution)/shard_map/ppermute | solution.py:49
  37.3 12.3 %collective-permute-start.14 = (bf16[4,264,128]{2,1,0:T(8,128)(2,1)S(1)}, bf16[4,264,128]{2,1,0:T(8,128)(2,1)S(1)}, u32[]{:S(2)}, u32[]{:S(2)}) collective-permute-start(bf16[4,264,128]{2,1,0:T(8,128)(2,1)S(1)} %get-tuple-element.53), channel_id=1, source_target_pairs={{0,96},{32,0},{64,32},{96,64},{1,97},{33,1},{65,33},{97,65},{2,98}... | collective-permute-start | bytes 811016 | tf_op jit(solution)/shard_map/ppermute | solution.py:49
  45.6 10.1 %collective-permute-start.6 = (bf16[4,264,128]{2,1,0:T(8,128)(2,1)S(1)}, bf16[4,264,128]{2,1,0:T(8,128)(2,1)S(1)}, u32[]{:S(2)}, u32[]{:S(2)}) collective-permute-start(bf16[4,264,128]{2,1,0:T(8,128)(2,1)S(1)} %get-tuple-element.46), channel_id=1, source_target_pairs={{0,64},{32,96},{64,0},{96,32},{1,65},{33,97},{65,1},{97,33},{2,66}... | collective-permute-start | bytes 811016 | tf_op jit(solution)/shard_map/ppermute | solution.py:49
  47.0 15.0 %collective-permute-start.7 = (bf16[4,264,128]{2,1,0:T(8,128)(2,1)S(1)}, bf16[4,264,128]{2,1,0:T(8,128)(2,1)S(1)}, u32[]{:S(2)}, u32[]{:S(2)}) collective-permute-start(bf16[4,264,128]{2,1,0:T(8,128)(2,1)S(1)} %get-tuple-element.46), channel_id=1, source_target_pairs={{0,32},{32,64},{64,96},{96,0},{1,33},{33,65},{65,97},{97,1},{2,34}... | collective-permute-start | bytes 811016 | tf_op jit(solution)/shard_map/ppermute | solution.py:49
  47.0 14.9 %collective-permute-start.8 = (bf16[4,264,128]{2,1,0:T(8,128)(2,1)S(1)}, bf16[4,264,128]{2,1,0:T(8,128)(2,1)S(1)}, u32[]{:S(2)}, u32[]{:S(2)}) collective-permute-start(bf16[4,264,128]{2,1,0:T(8,128)(2,1)S(1)} %get-tuple-element.46), channel_id=1, source_target_pairs={{0,96},{32,0},{64,32},{96,64},{1,97},{33,1},{65,33},{97,65},{2,98}... | collective-permute-start | bytes 811016 | tf_op jit(solution)/shard_map/ppermute | solution.py:49
  50.6 13.0 %collective-permute-start.15 = (bf16[4,264,128]{2,1,0:T(8,128)(2,1)S(1)}, bf16[4,264,128]{2,1,0:T(8,128)(2,1)S(1)}, u32[]{:S(2)}, u32[]{:S(2)}) collective-permute-start(bf16[4,264,128]{2,1,0:T(8,128)(2,1)S(1)} %get-tuple-element.55), channel_id=1, source_target_pairs={{0,16},{8,24},{16,0},{24,8},{1,17},{9,25},{17,1},{25,9},{2,18},{10... | collective-permute-start | bytes 811016 | tf_op jit(solution)/shard_map/ppermute | solution.py:49
  53.7 9.9 %collective-permute-start.16 = (bf16[4,264,128]{2,1,0:T(8,128)(2,1)S(1)}, bf16[4,264,128]{2,1,0:T(8,128)(2,1)S(1)}, u32[]{:S(2)}, u32[]{:S(2)}) collective-permute-start(bf16[4,264,128]{2,1,0:T(8,128)(2,1)S(1)} %get-tuple-element.55), channel_id=1, source_target_pairs={{0,8},{8,16},{16,24},{24,0},{1,9},{9,17},{17,25},{25,1},{2,10},{10... | collective-permute-start | bytes 811016 | tf_op jit(solution)/shard_map/ppermute | solution.py:49
  55.7 7.9 %collective-permute-start.17 = (bf16[4,264,128]{2,1,0:T(8,128)(2,1)S(1)}, bf16[4,264,128]{2,1,0:T(8,128)(2,1)S(1)}, u32[]{:S(2)}, u32[]{:S(2)}) collective-permute-start(bf16[4,264,128]{2,1,0:T(8,128)(2,1)S(1)} %get-tuple-element.55), channel_id=1, source_target_pairs={{0,24},{8,0},{16,8},{24,16},{1,25},{9,1},{17,9},{25,17},{2,26},{10... | collective-permute-start | bytes 811016 | tf_op jit(solution)/shard_map/ppermute | solution.py:49
  63.6 44.9 %copy-start.4 = (f32[2,1,256,256]{3,2,1,0:T(8,128)S(1)}, f32[2,1,256,256]{3,2,1,0:T(8,128)}, u32[]{:S(2)}) copy-start(f32[2,1,256,256]{3,2,1,0:T(8,128)} %param.15) | copy-start | bytes 1572868
  65.2 43.3 %copy-start.2 = (f32[2,1,128,2048]{3,2,1,0:T(8,128)S(1)}, f32[2,1,128,2048]{3,2,1,0:T(8,128)}, u32[]{:S(2)}) copy-start(f32[2,1,128,2048]{3,2,1,0:T(8,128)} %param.13) | copy-start | bytes 6291460
  65.2 7.1 %collective-permute-start.18 = (f32[2,128,256]{2,1,0:T(8,128)S(1)}, f32[2,128,256]{2,1,0:T(8,128)S(1)}, u32[]{:S(2)}, u32[]{:S(2)}) collective-permute-start(f32[2,128,256]{2,1,0:T(8,128)S(1)} %get-tuple-element.57.refs_0_), channel_id=1, source_target_pairs={{0,8},{8,16},{16,24},{24,0},{1,9},{9,17},{17,25},{25,1},{2,10},{10... | collective-permute-start | bytes 786440 | tf_op jit(solution)/shard_map/ppermute | solution.py:49
  66.2 32.6 %collective-permute-start.19 = (f32[2,128,256]{2,1,0:T(8,128)S(1)}, f32[2,128,256]{2,1,0:T(8,128)S(1)}, u32[]{:S(2)}, u32[]{:S(2)}) collective-permute-start(f32[2,128,256]{2,1,0:T(8,128)S(1)} %get-tuple-element.57.refs_0_), channel_id=1, source_target_pairs={{0,16},{8,24},{16,0},{24,8},{1,17},{9,25},{17,1},{25,9},{2,18},{10... | collective-permute-start | bytes 786440 | tf_op jit(solution)/shard_map/ppermute | solution.py:49
  68.1 30.7 %collective-permute-start.20 = (f32[2,128,256]{2,1,0:T(8,128)S(1)}, f32[2,128,256]{2,1,0:T(8,128)S(1)}, u32[]{:S(2)}, u32[]{:S(2)}) collective-permute-start(f32[2,128,256]{2,1,0:T(8,128)S(1)} %get-tuple-element.57.refs_0_), channel_id=1, source_target_pairs={{0,24},{8,0},{16,8},{24,16},{1,25},{9,1},{17,9},{25,17},{2,26},{10... | collective-permute-start | bytes 786440 | tf_op jit(solution)/shard_map/ppermute | solution.py:49
  68.9 29.9 %collective-permute-start.21 = (f32[2,128,256]{2,1,0:T(8,128)S(1)}, f32[2,128,256]{2,1,0:T(8,128)S(1)}, u32[]{:S(2)}, u32[]{:S(2)}) collective-permute-start(f32[2,128,256]{2,1,0:T(8,128)S(1)} %get-tuple-element.58.refs_4_), channel_id=1, source_target_pairs={{0,32},{32,64},{64,96},{96,0},{1,33},{33,65},{65,97},{97,1},{2,34}... | collective-permute-start | bytes 786440 | tf_op jit(solution)/shard_map/ppermute | solution.py:49
  71.4 27.5 %collective-permute-start.22 = (f32[2,128,256]{2,1,0:T(8,128)S(1)}, f32[2,128,256]{2,1,0:T(8,128)S(1)}, u32[]{:S(2)}, u32[]{:S(2)}) collective-permute-start(f32[2,128,256]{2,1,0:T(8,128)S(1)} %get-tuple-element.58.refs_4_), channel_id=1, source_target_pairs={{0,64},{32,96},{64,0},{96,32},{1,65},{33,97},{65,1},{97,33},{2,66}... | collective-permute-start | bytes 786440 | tf_op jit(solution)/shard_map/ppermute | solution.py:49
  72.3 26.6 %collective-permute-start.23 = (f32[2,128,256]{2,1,0:T(8,128)S(1)}, f32[2,128,256]{2,1,0:T(8,128)S(1)}, u32[]{:S(2)}, u32[]{:S(2)}) collective-permute-start(f32[2,128,256]{2,1,0:T(8,128)S(1)} %get-tuple-element.58.refs_4_), channel_id=1, source_target_pairs={{0,96},{32,0},{64,32},{96,64},{1,97},{33,1},{65,33},{97,65},{2,98}... | collective-permute-start | bytes 786440 | tf_op jit(solution)/shard_map/ppermute | solution.py:49
  99.9 8.6 %collective-permute-start.28 = (bf16[4,128,256]{2,1,0:T(8,128)(2,1)S(1)}, bf16[4,128,256]{2,1,0:T(8,128)(2,1)S(1)}, u32[]{:S(2)}, u32[]{:S(2)}) collective-permute-start(bf16[4,128,256]{2,1,0:T(8,128)(2,1)S(1)} %get-tuple-element.61.refs_0_), channel_id=1, source_target_pairs={{0,16},{8,24},{16,0},{24,8},{1,17},{9,25},{17,1},{25,9},{2,18},{10... | collective-permute-start | bytes 786440 | tf_op jit(solution)/shard_map/ppermute | solution.py:49
  100.9 11.8 %collective-permute-start.29 = (bf16[4,128,256]{2,1,0:T(8,128)(2,1)S(1)}, bf16[4,128,256]{2,1,0:T(8,128)(2,1)S(1)}, u32[]{:S(2)}, u32[]{:S(2)}) collective-permute-start(bf16[4,128,256]{2,1,0:T(8,128)(2,1)S(1)} %get-tuple-element.62.refs_1_), channel_id=1, source_target_pairs={{0,64},{32,96},{64,0},{96,32},{1,65},{33,97},{65,1},{97,33},{2,66}... | collective-permute-start | bytes 786440 | tf_op jit(solution)/shard_map/ppermute | solution.py:49
  101.6 13.6 %collective-permute-start.26 = (bf16[4,128,256]{2,1,0:T(8,128)(2,1)S(1)}, bf16[4,128,256]{2,1,0:T(8,128)(2,1)S(1)}, u32[]{:S(2)}, u32[]{:S(2)}) collective-permute-start(bf16[4,128,256]{2,1,0:T(8,128)(2,1)S(1)} %get-tuple-element.61.refs_0_), channel_id=1, source_target_pairs={{0,8},{8,16},{16,24},{24,0},{1,9},{9,17},{17,25},{25,1},{2,10},{10... | collective-permute-start | bytes 786440 | tf_op jit(solution)/shard_map/ppermute | solution.py:49
  102.1 14.2 %collective-permute-start.27 = (bf16[4,128,256]{2,1,0:T(8,128)(2,1)S(1)}, bf16[4,128,256]{2,1,0:T(8,128)(2,1)S(1)}, u32[]{:S(2)}, u32[]{:S(2)}) collective-permute-start(bf16[4,128,256]{2,1,0:T(8,128)(2,1)S(1)} %get-tuple-element.62.refs_1_), channel_id=1, source_target_pairs={{0,32},{32,64},{64,96},{96,0},{1,33},{33,65},{65,97},{97,1},{2,34}... | collective-permute-start | bytes 786440 | tf_op jit(solution)/shard_map/ppermute | solution.py:49
  102.6 14.6 %collective-permute-start.24 = (bf16[4,128,256]{2,1,0:T(8,128)(2,1)S(1)}, bf16[4,128,256]{2,1,0:T(8,128)(2,1)S(1)}, u32[]{:S(2)}, u32[]{:S(2)}) collective-permute-start(bf16[4,128,256]{2,1,0:T(8,128)(2,1)S(1)} %get-tuple-element.61.refs_0_), channel_id=1, source_target_pairs={{0,24},{8,0},{16,8},{24,16},{1,25},{9,1},{17,9},{25,17},{2,26},{10... | collective-permute-start | bytes 786440 | tf_op jit(solution)/shard_map/ppermute | solution.py:49
  108.5 8.7 %collective-permute-start.25 = (bf16[4,128,256]{2,1,0:T(8,128)(2,1)S(1)}, bf16[4,128,256]{2,1,0:T(8,128)(2,1)S(1)}, u32[]{:S(2)}, u32[]{:S(2)}) collective-permute-start(bf16[4,128,256]{2,1,0:T(8,128)(2,1)S(1)} %get-tuple-element.62.refs_1_), channel_id=1, source_target_pairs={{0,96},{32,0},{64,32},{96,64},{1,97},{33,1},{65,33},{97,65},{2,98}... | collective-permute-start | bytes 786440 | tf_op jit(solution)/shard_map/ppermute | solution.py:49
  (3 other events, 98.3 us)

commit v2 on v1

--- a/solution.py
+++ b/solution.py
@@ -157,11 +157,25 @@
             outs[m][j] = total[:, j * width : (j + 1) * width]
 
 
-def sum_kernel(own_ref, a_ref, b_ref, c_ref, total_ref, code_ref):
+def sum_kernel(own_ref, a_ref, b_ref, c_ref, total_ref, *codes):
     for j in range(RING):
         total = (own_ref[j] + decode(a_ref, j)) + (decode(b_ref, j) + decode(c_ref, j))
         total_ref[j] = total
-        encode(total, code_ref, j)
+        encode(total, codes[j // 2], j % 2)
+
+
+def pair_kernel(own_ref, a_ref, b_ref, total_ref, *codes):
+    for j in range(RING):
+        total = own_ref[j] + decode((a_ref, b_ref)[j // 2], j % 2)
+        total_ref[j] = total
+        if len(codes) == 1:
+            encode(total, codes[0], j)
+        else:
+            encode(total, codes[j // 2], j % 2)
+
+
+def swap(value, axis, kind):
+    return lax.ppermute(value, axis, [(i, i ^ 1 if kind == 0 else 3 - i) for i in range(RING)])
 
 
 def exchange(blocks, axis):
@@ -288,14 +302,26 @@
     v3, k3 = shift(v3, Z, 3), shift(k3, X, 3)
     k0, v0 = call(functools.partial(own_kernel, rows), [pltpu.VMEM(blocks, f32)] * 2, [VMEM] * 3, 12)(x_here, kt, vt)
 
-    add = call(sum_kernel, [pltpu.VMEM(blocks, f32), pltpu.VMEM(coded, bf16)], [VMEM] * 4, 16)
-    v0, code_v = add(v0, v2, v1, v3)
-    got_v = exchange(code_v, X)
-    k0, code_k = add(k0, k2, k1, k3)
-    got_k = exchange(code_k, Z)
-    line_v, code_v = add(v0, *got_v)
+    halves = [pltpu.VMEM((2, columns + GROUPS, rows), bf16)] * 2
+    total = pltpu.VMEM(blocks, f32)
+    add = call(sum_kernel, [total, *halves], [VMEM] * 4, 16)
+    pair = call(pair_kernel, [total, *halves], [VMEM] * 3, 16)
+    finish = call(pair_kernel, [total, pltpu.VMEM(coded, bf16)], [VMEM] * 3, 16)
+
+    def swapped(codes, axis, step):
+        return [swap(c, axis, (h + step) % 2) for h, c in enumerate(codes)]
+
+    v0, *codes_v = add(v0, v2, v1, v3)
+    got_v = swapped(codes_v, X, 0)
+    k0, *codes_k = add(k0, k2, k1, k3)
+    got_k = swapped(codes_k, Z, 0)
+    v0, *codes_v = pair(v0, *got_v)
+    got_v = swapped(codes_v, X, 1)
+    k0, *codes_k = pair(k0, *got_k)
+    got_k = swapped(codes_k, Z, 1)
+    line_v, code_v = finish(v0, *got_v)
     pieces_v = exchange(code_v, Z)
-    line_k, code_k = add(k0, *got_k)
+    line_k, code_k = finish(k0, *got_k)
     pieces_k = exchange(code_k, X)
 
     def direction(m, before, line, pieces):

time: 118 us -> 126 us (1.068)
  waiting for transfers between devices: 23.9 us -> 27.4 us
  blocking collectives: 25 us -> 27.6 us
  starting transfers between devices: 41.3 us -> 42.7 us
    ppermute x0 -> x8, waiting for transfers between devices: none -> 10.1 us  [swap(): lax.ppermute(value, axis, [(i, i ^ 1 if kind == 0 else 3 - i) for i in ra...]
    ppermute x0 -> x8, starting transfers between devices: none -> 9.16 us  [swap(): lax.ppermute(value, axis, [(i, i ^ 1 if kind == 0 else 3 - i) for i in ra...]
    ppermute x30 -> x24, starting transfers between devices: 41.3 us -> 33.6 us  [shift(): lax.ppermute(value, axis, [(i, (i + by) % RING) for i in range(RING)])]
    ppermute x30 -> x24, waiting for transfers between devices: 23.9 us -> 17.3 us  [shift(): lax.ppermute(value, axis, [(i, (i + by) % RING) for i in range(RING)])]
    all_to_all x1, blocking collectives: 25 us -> 27.6 us  [on_device(): lax.all_to_all(spread, FS_TP, 0, 0, tiled=True).reshape(everyone, 128)]
    pallas_call x4 -> x6, Pallas kernels: 3.59 us -> 3.51 us  [the longest x1 0.9 us: on_device(): v0, *codes_v = add(v0, v2, v1, v3)]
  transfers between devices with their start and end apart: 30 -> 32, of which waited for: 10 -> 12; matrix products, arithmetic and copies ran while one was open for 0% -> 0% of each run, Pallas kernels for 11% -> 10%
where the time goes in v2:
time: 126 us
  starting transfers between devices  42.7 us (34%)
  blocking collectives  27.6 us (22%)
  waiting for transfers between devices  27.4 us (22%)
  Pallas kernels  26.7 us (21%)
    ppermute x24, starting transfers between devices, shift(): lax.ppermute(value, axis, [(i, (i + by) % RING) for i in range(RING)])  33.6 us
    all_to_all x1, blocking collectives, on_device(): lax.all_to_all(spread, FS_TP, 0, 0, tiled=True).reshape(everyone, 128)  27.6 us
    ppermute x24, waiting for transfers between devices, shift(): lax.ppermute(value, axis, [(i, (i + by) % RING) for i in range(RING)])  17.3 us
    ppermute x8, waiting for transfers between devices, swap(): lax.ppermute(value, axis, [(i, i ^ 1 if kind == 0 else 3 - i) for i in ra...  10.1 us
    ppermute x8, starting transfers between devices, swap(): lax.ppermute(value, axis, [(i, i ^ 1 if kind == 0 else 3 - i) for i in ra...  9.16 us
    pallas_call x1, Pallas kernels, on_device(): call(functools.partial(first_kernel, rows), [pltpu.VMEM((tokens, features...  5.79 us
    pallas_call x1, Pallas kernels, on_device(): call(functools.partial(near_kernel, rows), [pltpu.VMEM(coded, bf16)] * 4,...  4.4 us
    pallas_call x1, Pallas kernels, on_device(): call(functools.partial(stat_kernel, rows), [jax.ShapeDtypeStruct((2, rows...  4.17 us
  transfers between devices with their start and end apart: 32, of which 12 were waited for; matrix products, arithmetic and copies ran while one was open for 0% of the time, Pallas kernels for 10%

profile of v2, /device:TPU:1, one launch (start us, length us, event | category | flops | bytes accessed | tf_op | source)
XLA Modules:
  0.0 125.5 jit_solution(1778349878564331330)
XLA Ops:
  0.6 5.8 %shard_map.119 = (bf16[3072,2048]{1,0:T(8,128)(2,1)S(1)}, bf16[256,3072]{1,0:T(8,128)(2,1)S(1)}, bf16[256,3072]{1,0:T(8,128)(2,1)S(1)}, bf16[4,264,128]{2,1,0:T(8,128)(2,1)S(1)}, bf16[4,264,128]{2,1,0:T(8,128)(2,1)S(1)}) custom-call(bf16[3072,2048]{1,0:T(8,128)(2,1)} %x_hbm.1, bf16[3072,256]{1,0:T(8,128)(2,1)} %k_hbm.1, bf16[3072,256]{1,0:T(8,128)(2,1)} %v_hbm.1), custom_call_target="tpu_custom_call" | custom-call | tf_op jit(solution)/shard_map/pallas_call | solution.py:280
  6.4 4.4 %shard_map.121 = (bf16[4,264,128]{2,1,0:T(8,128)(2,1)S(1)}, bf16[4,264,128]{2,1,0:T(8,128)(2,1)S(1)}, bf16[4,264,128]{2,1,0:T(8,128)(2,1)S(1)}, bf16[4,264,128]{2,1,0:T(8,128)(2,1)S(1)}) custom-call(bf16[3072,2048]{1,0:T(8,128)(2,1)S(1)} %get-tuple-element.44.x_ref, bf16[256,3072]{1,0:T(8,128)(2,1)S(1)} %get-tuple-element.45.kt_ref, ...), custom_call_target="tpu_custom_call" | custom-call | tf_op jit(solution)/shard_map/pallas_call | solution.py:298
  10.8 2.5 %collective-permute-start.1 = (bf16[4,264,128]{2,1,0:T(8,128)(2,1)S(1)}, bf16[4,264,128]{2,1,0:T(8,128)(2,1)S(1)}, u32[]{:S(2)}, u32[]{:S(2)}) collective-permute-start(bf16[4,264,128]{2,1,0:T(8,128)(2,1)S(1)} %get-tuple-element.49), channel_id=1, source_target_pairs={{0,32},{32,64},{64,96},{96,0},{1,33},{33,65},{65,97},{97,1},{2,34}... | collective-permute-start | bytes 811016 | tf_op jit(solution)/shard_map/ppermute | solution.py:49
  13.3 2.2 %collective-permute-start.2 = (bf16[4,264,128]{2,1,0:T(8,128)(2,1)S(1)}, bf16[4,264,128]{2,1,0:T(8,128)(2,1)S(1)}, u32[]{:S(2)}, u32[]{:S(2)}) collective-permute-start(bf16[4,264,128]{2,1,0:T(8,128)(2,1)S(1)} %get-tuple-element.50), channel_id=1, source_target_pairs={{0,96},{32,0},{64,32},{96,64},{1,97},{33,1},{65,33},{97,65},{2,98}... | collective-permute-start | bytes 811016 | tf_op jit(solution)/shard_map/ppermute | solution.py:49
  15.5 1.3 %collective-permute-start = (bf16[4,264,128]{2,1,0:T(8,128)(2,1)S(1)}, bf16[4,264,128]{2,1,0:T(8,128)(2,1)S(1)}, u32[]{:S(2)}, u32[]{:S(2)}) collective-permute-start(bf16[4,264,128]{2,1,0:T(8,128)(2,1)S(1)} %get-tuple-element.48), channel_id=1, source_target_pairs={{0,64},{32,96},{64,0},{96,32},{1,65},{33,97},{65,1},{97,33},{2,66}... | collective-permute-start | bytes 811016 | tf_op jit(solution)/shard_map/ppermute | solution.py:49
  18.0 1.5 %collective-permute-start.12 = (bf16[4,264,128]{2,1,0:T(8,128)(2,1)S(1)}, bf16[4,264,128]{2,1,0:T(8,128)(2,1)S(1)}, u32[]{:S(2)}, u32[]{:S(2)}) collective-permute-start(bf16[4,264,128]{2,1,0:T(8,128)(2,1)S(1)} %get-tuple-element.63), channel_id=1, source_target_pairs={{0,24},{8,0},{16,8},{24,16},{1,25},{9,1},{17,9},{25,17},{2,26},{10... | collective-permute-start | bytes 811016 | tf_op jit(solution)/shard_map/ppermute | solution.py:49
  19.5 1.9 %shard_map.120 = (f32[4,256,128]{2,1,0:T(8,128)S(1)}, f32[4,256,128]{2,1,0:T(8,128)S(1)}) custom-call(bf16[3072,2048]{1,0:T(8,128)(2,1)S(1)} %get-tuple-element.44.x_ref, bf16[256,3072]{1,0:T(8,128)(2,1)S(1)} %get-tuple-element.45.kt_ref, bf16[256,3072]{1,0:T(8,128)(2,1)S(1)} %get-tuple-element.46.vt_ref), custom_call_target="tpu_custom_call" | custom-call | tf_op jit(solution)/shard_map/pallas_call | solution.py:303
  21.6 2.8 %collective-permute-start.10 = (bf16[4,264,128]{2,1,0:T(8,128)(2,1)S(1)}, bf16[4,264,128]{2,1,0:T(8,128)(2,1)S(1)}, u32[]{:S(2)}, u32[]{:S(2)}) collective-permute-start(bf16[4,264,128]{2,1,0:T(8,128)(2,1)S(1)} %get-tuple-element.61), channel_id=1, source_target_pairs={{0,16},{8,24},{16,0},{24,8},{1,17},{9,25},{17,1},{25,9},{2,18},{10... | collective-permute-start | bytes 811016 | tf_op jit(solution)/shard_map/ppermute | solution.py:49
  24.4 3.9 %collective-permute-done.a_ref = bf16[4,264,128]{2,1,0:T(8,128)(2,1)S(1)} collective-permute-done((bf16[4,264,128]{2,1,0:T(8,128)(2,1)S(1)}, bf16[4,264,128]{2,1,0:T(8,128)(2,1)S(1)}, u32[]{:S(2)}, u32[]{:S(2)}) %collective-permute-start) | collective-permute-done | bytes 270368 | tf_op jit(solution)/shard_map/ppermute | solution.py:49
  29.2 1.3 %collective-permute-start.3 = (bf16[2,264,128]{2,1,0:T(8,128)(2,1)S(1)}, bf16[2,264,128]{2,1,0:T(8,128)(2,1)S(1)}, u32[]{:S(2)}, u32[]{:S(2)}) collective-permute-start(bf16[2,264,128]{2,1,0:T(8,128)(2,1)S(1)} %get-tuple-element.52), channel_id=1, source_target_pairs={{0,8},{8,0},{16,24},{24,16},{1,9},{9,1},{17,25},{25,17},{2,10},{10... | collective-permute-start | bytes 405512 | tf_op jit(solution)/shard_map/ppermute | solution.py:178
  30.5 1.8 %collective-permute-start.4 = (bf16[2,264,128]{2,1,0:T(8,128)(2,1)S(1)}, bf16[2,264,128]{2,1,0:T(8,128)(2,1)S(1)}, u32[]{:S(2)}, u32[]{:S(2)}) collective-permute-start(bf16[2,264,128]{2,1,0:T(8,128)(2,1)S(1)} %get-tuple-element.53), channel_id=1, source_target_pairs={{0,24},{8,16},{16,8},{24,0},{1,25},{9,17},{17,9},{25,1},{2,26},{10... | collective-permute-start | bytes 405512 | tf_op jit(solution)/shard_map/ppermute | solution.py:178
  33.5 2.1 %collective-permute-done.4.b_ref = bf16[2,264,128]{2,1,0:T(8,128)(2,1)S(1)} collective-permute-done((bf16[2,264,128]{2,1,0:T(8,128)(2,1)S(1)}, bf16[2,264,128]{2,1,0:T(8,128)(2,1)S(1)}, u32[]{:S(2)}, u32[]{:S(2)}) %collective-permute-start.4) | collective-permute-done | bytes 135200 | tf_op jit(solution)/shard_map/ppermute | solution.py:178
  36.0 1.9 %collective-permute-start.5 = (bf16[2,264,128]{2,1,0:T(8,128)(2,1)S(1)}, bf16[2,264,128]{2,1,0:T(8,128)(2,1)S(1)}, u32[]{:S(2)}, u32[]{:S(2)}) collective-permute-start(bf16[2,264,128]{2,1,0:T(8,128)(2,1)S(1)} %get-tuple-element.55), channel_id=1, source_target_pairs={{0,24},{8,16},{16,8},{24,0},{1,25},{9,17},{17,9},{25,1},{2,26},{10... | collective-permute-start | bytes 405512 | tf_op jit(solution)/shard_map/ppermute | solution.py:178
  38.9 3.2 %collective-permute-start.13 = (bf16[2,264,128]{2,1,0:T(8,128)(2,1)S(1)}, bf16[2,264,128]{2,1,0:T(8,128)(2,1)S(1)}, u32[]{:S(2)}, u32[]{:S(2)}) collective-permute-start(bf16[2,264,128]{2,1,0:T(8,128)(2,1)S(1)} %get-tuple-element.65), channel_id=1, source_target_pairs={{0,32},{32,0},{64,96},{96,64},{1,33},{33,1},{65,97},{97,65},{2,34}... | collective-permute-start | bytes 405512 | tf_op jit(solution)/shard_map/ppermute | solution.py:178
  42.7 2.6 %collective-permute-start.7 = (bf16[4,264,128]{2,1,0:T(8,128)(2,1)S(1)}, bf16[4,264,128]{2,1,0:T(8,128)(2,1)S(1)}, u32[]{:S(2)}, u32[]{:S(2)}) collective-permute-start(bf16[4,264,128]{2,1,0:T(8,128)(2,1)S(1)} %get-tuple-element.58), channel_id=1, source_target_pairs={{0,64},{32,96},{64,0},{96,32},{1,65},{33,97},{65,1},{97,33},{2,66}... | collective-permute-start | bytes 811016 | tf_op jit(solution)/shard_map/ppermute | solution.py:49
  45.4 2.1 %collective-permute-done.14.b_ref = bf16[2,264,128]{2,1,0:T(8,128)(2,1)S(1)} collective-permute-done((bf16[2,264,128]{2,1,0:T(8,128)(2,1)S(1)}, bf16[2,264,128]{2,1,0:T(8,128)(2,1)S(1)}, u32[]{:S(2)}, u32[]{:S(2)}) %collective-permute-start.14) | collective-permute-done | bytes 135200 | tf_op jit(solution)/shard_map/ppermute | solution.py:178
  48.6 1.5 %collective-permute-start.8 = (bf16[4,264,128]{2,1,0:T(8,128)(2,1)S(1)}, bf16[4,264,128]{2,1,0:T(8,128)(2,1)S(1)}, u32[]{:S(2)}, u32[]{:S(2)}) collective-permute-start(bf16[4,264,128]{2,1,0:T(8,128)(2,1)S(1)} %get-tuple-element.58), channel_id=1, source_target_pairs={{0,32},{32,64},{64,96},{96,0},{1,33},{33,65},{65,97},{97,1},{2,34}... | collective-permute-start | bytes 811016 | tf_op jit(solution)/shard_map/ppermute | solution.py:49
  51.3 4.7 %collective-permute-done.15.a_ref = bf16[2,264,128]{2,1,0:T(8,128)(2,1)S(1)} collective-permute-done((bf16[2,264,128]{2,1,0:T(8,128)(2,1)S(1)}, bf16[2,264,128]{2,1,0:T(8,128)(2,1)S(1)}, u32[]{:S(2)}, u32[]{:S(2)}) %collective-permute-start.15) | collective-permute-done | bytes 135200 | tf_op jit(solution)/shard_map/ppermute | solution.py:178
  56.5 1.9 %collective-permute-start.17 = (bf16[4,264,128]{2,1,0:T(8,128)(2,1)S(1)}, bf16[4,264,128]{2,1,0:T(8,128)(2,1)S(1)}, u32[]{:S(2)}, u32[]{:S(2)}) collective-permute-start(bf16[4,264,128]{2,1,0:T(8,128)(2,1)S(1)} %get-tuple-element.71), channel_id=1, source_target_pairs={{0,16},{8,24},{16,0},{24,8},{1,17},{9,25},{17,1},{25,9},{2,18},{10... | collective-permute-start | bytes 811016 | tf_op jit(solution)/shard_map/ppermute | solution.py:49
  58.4 2.7 %collective-permute-start.19 = (bf16[4,264,128]{2,1,0:T(8,128)(2,1)S(1)}, bf16[4,264,128]{2,1,0:T(8,128)(2,1)S(1)}, u32[]{:S(2)}, u32[]{:S(2)}) collective-permute-start(bf16[4,264,128]{2,1,0:T(8,128)(2,1)S(1)} %get-tuple-element.71), channel_id=1, source_target_pairs={{0,24},{8,0},{16,8},{24,16},{1,25},{9,1},{17,9},{25,17},{2,26},{10... | collective-permute-start | bytes 811016 | tf_op jit(solution)/shard_map/ppermute | solution.py:49
  61.1 1.6 %shard_map.125 = (f32[2,128,256]{2,1,0:T(8,128)S(1)}, f32[1,128]{1,0:T(1,128)S(1)}, bf16[8,2,256,256]{3,2,1,0:T(8,128)(2,1)S(1)}) custom-call(f32[2,128,2048]{2,1,0:T(8,128)S(1)} %bitcast.12, f32[2,256,256]{2,1,0:T(8,128)S(1)} %bitcast.14, f32[1,128]{1,0:T(1,128)S(1)} %broadcast_in_dim.17.before_ref, f32[2,128,256]{2,1,0:T(8,128)S(1)} %copy-done.3, ...), custom_call_target="tpu_custom_call" | custom-call | tf_op jit(solution)/shard_map/pallas_call | solution.py:328
  63.5 2.9 %collective-permute-done.18.b_ref = bf16[4,264,128]{2,1,0:T(8,128)(2,1)S(1)} collective-permute-done((bf16[4,264,128]{2,1,0:T(8,128)(2,1)S(1)}, bf16[4,264,128]{2,1,0:T(8,128)(2,1)S(1)}, u32[]{:S(2)}, u32[]{:S(2)}) %collective-permute-start.18) | collective-permute-done | bytes 270368 | tf_op jit(solution)/shard_map/ppermute | solution.py:49
  66.3 1.6 %shard_map.129 = (f32[2,128,256]{2,1,0:T(8,128)S(1)}, f32[1,128]{1,0:T(1,128)S(1)}, bf16[8,2,256,256]{3,2,1,0:T(8,128)(2,1)S(1)}) custom-call(f32[2,128,2048]{2,1,0:T(8,128)S(1)} %bitcast.13, f32[2,256,256]{2,1,0:T(8,128)S(1)} %bitcast.15, f32[1,128]{1,0:T(1,128)S(1)} %get-tuple-element.59.before_ref, f32[2,128,256]{2,1,0:T(8,128)S(1)} %copy-done.3, ...), custom_call_target="tpu_custom_call" | custom-call | tf_op jit(solution)/shard_map/pallas_call | solution.py:328
  67.9 1.9 %collective-permute-start.20 = (f32[2,128,256]{2,1,0:T(8,128)S(1)}, f32[2,128,256]{2,1,0:T(8,128)S(1)}, u32[]{:S(2)}, u32[]{:S(2)}) collective-permute-start(f32[2,128,256]{2,1,0:T(8,128)S(1)} %get-tuple-element.73.refs_0_), channel_id=1, source_target_pairs={{0,8},{8,16},{16,24},{24,0},{1,9},{9,17},{17,25},{25,1},{2,10},{10... | collective-permute-start | bytes 786440 | tf_op jit(solution)/shard_map/ppermute | solution.py:49
  70.5 2.0 %collective-permute-start.22 = (f32[2,128,256]{2,1,0:T(8,128)S(1)}, f32[2,128,256]{2,1,0:T(8,128)S(1)}, u32[]{:S(2)}, u32[]{:S(2)}) collective-permute-start(f32[2,128,256]{2,1,0:T(8,128)S(1)} %get-tuple-element.73.refs_0_), channel_id=1, source_target_pairs={{0,24},{8,0},{16,8},{24,16},{1,25},{9,1},{17,9},{25,17},{2,26},{10... | collective-permute-start | bytes 786440 | tf_op jit(solution)/shard_map/ppermute | solution.py:49
  72.5 2.6 %collective-permute-start.24 = (f32[2,128,256]{2,1,0:T(8,128)S(1)}, f32[2,128,256]{2,1,0:T(8,128)S(1)}, u32[]{:S(2)}, u32[]{:S(2)}) collective-permute-start(f32[2,128,256]{2,1,0:T(8,128)S(1)} %get-tuple-element.74.refs_4_), channel_id=1, source_target_pairs={{0,64},{32,96},{64,0},{96,32},{1,65},{33,97},{65,1},{97,33},{2,66}... | collective-permute-start | bytes 786440 | tf_op jit(solution)/shard_map/ppermute | solution.py:49
  75.1 3.3 %collective-permute-done.20.refs_1_ = f32[2,128,256]{2,1,0:T(8,128)S(1)} collective-permute-done((f32[2,128,256]{2,1,0:T(8,128)S(1)}, f32[2,128,256]{2,1,0:T(8,128)S(1)}, u32[]{:S(2)}, u32[]{:S(2)}) %collective-permute-start.20) | collective-permute-done | bytes 262176 | tf_op jit(solution)/shard_map/ppermute | solution.py:49
  78.5 27.6 %all_to_all.5 = f32[128,1,128]{2,1,0:T(1,128)S(1)} all-to-all(f32[128,1,128]{2,1,0:T(1,128)S(1)} %broadcast_in_dim.19), channel_id=1, replica_groups=mesh['fs_0'=4,'fs_1'=4,'tp_0'=4,'tp_1'=2] {'fs_0','fs_1','tp_0','tp_1'}, dimensions={0} | all-to-all | bytes 131072 | tf_op jit(solution)/shard_map/all_to_all | solution.py:346
  109.9 2.2 %collective-permute-start.26 = (bf16[4,128,256]{2,1,0:T(8,128)(2,1)S(1)}, bf16[4,128,256]{2,1,0:T(8,128)(2,1)S(1)}, u32[]{:S(2)}, u32[]{:S(2)}) collective-permute-start(bf16[4,128,256]{2,1,0:T(8,128)(2,1)S(1)} %get-tuple-element.77.refs_0_), channel_id=1, source_target_pairs={{0,24},{8,0},{16,8},{24,16},{1,25},{9,1},{17,9},{25,17},{2,26},{10... | collective-permute-start | bytes 786440 | tf_op jit(solution)/shard_map/ppermute | solution.py:49
  112.1 3.7 %collective-permute-done.30.refs_2_ = bf16[4,128,256]{2,1,0:T(8,128)(2,1)S(1)} collective-permute-done((bf16[4,128,256]{2,1,0:T(8,128)(2,1)S(1)}, bf16[4,128,256]{2,1,0:T(8,128)(2,1)S(1)}, u32[]{:S(2)}, u32[]{:S(2)}) %collective-permute-start.30) | collective-permute-done | bytes 262176 | tf_op jit(solution)/shard_map/ppermute | solution.py:49
  115.8 4.2 %shard_map.134 = (f32[2,128,2048]{2,1,0:T(8,128)}, f32[2,256,256]{2,1,0:T(8,128)}) custom-call(f32[2,128,2048]{2,1,0:T(8,128)S(1)} %bitcast.16, f32[2,256,256]{2,1,0:T(8,128)S(1)} %bitcast.17, f32[4,256,128]{2,1,0:T(8,128)S(1)} %get-tuple-element.70.line_ref.line_k, f32[4,256,128]{2,1,0:T(8,128)S(1)} %get-tuple-element.57.line_ref.line_v, ...), custom_call_target="tpu_custom_call" | custom-call | tf_op jit(solution)/shard_map/pallas_call | solution.py:361
  121.1 1.4 %collective-permute-done.28.refs_0_ = bf16[4,128,256]{2,1,0:T(8,128)(2,1)S(1)} collective-permute-done((bf16[4,128,256]{2,1,0:T(8,128)(2,1)S(1)}, bf16[4,128,256]{2,1,0:T(8,128)(2,1)S(1)}, u32[]{:S(2)}, u32[]{:S(2)}) %collective-permute-start.28) | collective-permute-done | bytes 262176 | tf_op jit(solution)/shard_map/ppermute | solution.py:49
  (61 shorter events, 17.6 us)
Async XLA Ops:
  10.8 10.8 %collective-permute-start.1 = (bf16[4,264,128]{2,1,0:T(8,128)(2,1)S(1)}, bf16[4,264,128]{2,1,0:T(8,128)(2,1)S(1)}, u32[]{:S(2)}, u32[]{:S(2)}) collective-permute-start(bf16[4,264,128]{2,1,0:T(8,128)(2,1)S(1)} %get-tuple-element.49), channel_id=1, source_target_pairs={{0,32},{32,64},{64,96},{96,0},{1,33},{33,65},{65,97},{97,1},{2,34}... | collective-permute-start | bytes 811016 | tf_op jit(solution)/shard_map/ppermute | solution.py:49
  13.3 11.1 %collective-permute-start.2 = (bf16[4,264,128]{2,1,0:T(8,128)(2,1)S(1)}, bf16[4,264,128]{2,1,0:T(8,128)(2,1)S(1)}, u32[]{:S(2)}, u32[]{:S(2)}) collective-permute-start(bf16[4,264,128]{2,1,0:T(8,128)(2,1)S(1)} %get-tuple-element.50), channel_id=1, source_target_pairs={{0,96},{32,0},{64,32},{96,64},{1,97},{33,1},{65,33},{97,65},{2,98}... | collective-permute-start | bytes 811016 | tf_op jit(solution)/shard_map/ppermute | solution.py:49
  15.5 12.8 %collective-permute-start = (bf16[4,264,128]{2,1,0:T(8,128)(2,1)S(1)}, bf16[4,264,128]{2,1,0:T(8,128)(2,1)S(1)}, u32[]{:S(2)}, u32[]{:S(2)}) collective-permute-start(bf16[4,264,128]{2,1,0:T(8,128)(2,1)S(1)} %get-tuple-element.48), channel_id=1, source_target_pairs={{0,64},{32,96},{64,0},{96,32},{1,65},{33,97},{65,1},{97,33},{2,66}... | collective-permute-start | bytes 811016 | tf_op jit(solution)/shard_map/ppermute | solution.py:49
  16.8 21.2 %collective-permute-start.11 = (bf16[4,264,128]{2,1,0:T(8,128)(2,1)S(1)}, bf16[4,264,128]{2,1,0:T(8,128)(2,1)S(1)}, u32[]{:S(2)}, u32[]{:S(2)}) collective-permute-start(bf16[4,264,128]{2,1,0:T(8,128)(2,1)S(1)} %get-tuple-element.62), channel_id=1, source_target_pairs={{0,8},{8,16},{16,24},{24,0},{1,9},{9,17},{17,25},{25,1},{2,10},{10... | collective-permute-start | bytes 811016 | tf_op jit(solution)/shard_map/ppermute | solution.py:49
  18.0 20.0 %collective-permute-start.12 = (bf16[4,264,128]{2,1,0:T(8,128)(2,1)S(1)}, bf16[4,264,128]{2,1,0:T(8,128)(2,1)S(1)}, u32[]{:S(2)}, u32[]{:S(2)}) collective-permute-start(bf16[4,264,128]{2,1,0:T(8,128)(2,1)S(1)} %get-tuple-element.63), channel_id=1, source_target_pairs={{0,24},{8,0},{16,8},{24,16},{1,25},{9,1},{17,9},{25,17},{2,26},{10... | collective-permute-start | bytes 811016 | tf_op jit(solution)/shard_map/ppermute | solution.py:49
  21.6 16.3 %collective-permute-start.10 = (bf16[4,264,128]{2,1,0:T(8,128)(2,1)S(1)}, bf16[4,264,128]{2,1,0:T(8,128)(2,1)S(1)}, u32[]{:S(2)}, u32[]{:S(2)}) collective-permute-start(bf16[4,264,128]{2,1,0:T(8,128)(2,1)S(1)} %get-tuple-element.61), channel_id=1, source_target_pairs={{0,16},{8,24},{16,0},{24,8},{1,17},{9,25},{17,1},{25,9},{2,18},{10... | collective-permute-start | bytes 811016 | tf_op jit(solution)/shard_map/ppermute | solution.py:49
  29.2 4.3 %collective-permute-start.3 = (bf16[2,264,128]{2,1,0:T(8,128)(2,1)S(1)}, bf16[2,264,128]{2,1,0:T(8,128)(2,1)S(1)}, u32[]{:S(2)}, u32[]{:S(2)}) collective-permute-start(bf16[2,264,128]{2,1,0:T(8,128)(2,1)S(1)} %get-tuple-element.52), channel_id=1, source_target_pairs={{0,8},{8,0},{16,24},{24,16},{1,9},{9,1},{17,25},{25,17},{2,10},{10... | collective-permute-start | bytes 405512 | tf_op jit(solution)/shard_map/ppermute | solution.py:178
  30.5 5.1 %collective-permute-start.4 = (bf16[2,264,128]{2,1,0:T(8,128)(2,1)S(1)}, bf16[2,264,128]{2,1,0:T(8,128)(2,1)S(1)}, u32[]{:S(2)}, u32[]{:S(2)}) collective-permute-start(bf16[2,264,128]{2,1,0:T(8,128)(2,1)S(1)} %get-tuple-element.53), channel_id=1, source_target_pairs={{0,24},{8,16},{16,8},{24,0},{1,25},{9,17},{17,9},{25,1},{2,26},{10... | collective-permute-start | bytes 405512 | tf_op jit(solution)/shard_map/ppermute | solution.py:178
  36.0 6.2 %collective-permute-start.5 = (bf16[2,264,128]{2,1,0:T(8,128)(2,1)S(1)}, bf16[2,264,128]{2,1,0:T(8,128)(2,1)S(1)}, u32[]{:S(2)}, u32[]{:S(2)}) collective-permute-start(bf16[2,264,128]{2,1,0:T(8,128)(2,1)S(1)} %get-tuple-element.55), channel_id=1, source_target_pairs={{0,24},{8,16},{16,8},{24,0},{1,25},{9,17},{17,9},{25,1},{2,26},{10... | collective-permute-start | bytes 405512 | tf_op jit(solution)/shard_map/ppermute | solution.py:178
  37.9 4.3 %collective-permute-start.6 = (bf16[2,264,128]{2,1,0:T(8,128)(2,1)S(1)}, bf16[2,264,128]{2,1,0:T(8,128)(2,1)S(1)}, u32[]{:S(2)}, u32[]{:S(2)}) collective-permute-start(bf16[2,264,128]{2,1,0:T(8,128)(2,1)S(1)} %get-tuple-element.56), channel_id=1, source_target_pairs={{0,8},{8,0},{16,24},{24,16},{1,9},{9,1},{17,25},{25,17},{2,10},{10... | collective-permute-start | bytes 405512 | tf_op jit(solution)/shard_map/ppermute | solution.py:178
  38.9 6.5 %collective-permute-start.13 = (bf16[2,264,128]{2,1,0:T(8,128)(2,1)S(1)}, bf16[2,264,128]{2,1,0:T(8,128)(2,1)S(1)}, u32[]{:S(2)}, u32[]{:S(2)}) collective-permute-start(bf16[2,264,128]{2,1,0:T(8,128)(2,1)S(1)} %get-tuple-element.65), channel_id=1, source_target_pairs={{0,32},{32,0},{64,96},{96,64},{1,33},{33,1},{65,97},{97,65},{2,34}... | collective-permute-start | bytes 405512 | tf_op jit(solution)/shard_map/ppermute | solution.py:178
  42.0 5.4 %collective-permute-start.14 = (bf16[2,264,128]{2,1,0:T(8,128)(2,1)S(1)}, bf16[2,264,128]{2,1,0:T(8,128)(2,1)S(1)}, u32[]{:S(2)}, u32[]{:S(2)}) collective-permute-start(bf16[2,264,128]{2,1,0:T(8,128)(2,1)S(1)} %get-tuple-element.66), channel_id=1, source_target_pairs={{0,96},{32,64},{64,32},{96,0},{1,97},{33,65},{65,33},{97,1},{2,98}... | collective-permute-start | bytes 405512 | tf_op jit(solution)/shard_map/ppermute | solution.py:178
  42.7 15.7 %collective-permute-start.7 = (bf16[4,264,128]{2,1,0:T(8,128)(2,1)S(1)}, bf16[4,264,128]{2,1,0:T(8,128)(2,1)S(1)}, u32[]{:S(2)}, u32[]{:S(2)}) collective-permute-start(bf16[4,264,128]{2,1,0:T(8,128)(2,1)S(1)} %get-tuple-element.58), channel_id=1, source_target_pairs={{0,64},{32,96},{64,0},{96,32},{1,65},{33,97},{65,1},{97,33},{2,66}... | collective-permute-start | bytes 811016 | tf_op jit(solution)/shard_map/ppermute | solution.py:49
  47.9 8.1 %collective-permute-start.15 = (bf16[2,264,128]{2,1,0:T(8,128)(2,1)S(1)}, bf16[2,264,128]{2,1,0:T(8,128)(2,1)S(1)}, u32[]{:S(2)}, u32[]{:S(2)}) collective-permute-start(bf16[2,264,128]{2,1,0:T(8,128)(2,1)S(1)} %get-tuple-element.68), channel_id=1, source_target_pairs={{0,96},{32,64},{64,32},{96,0},{1,97},{33,65},{65,33},{97,1},{2,98}... | collective-permute-start | bytes 405512 | tf_op jit(solution)/shard_map/ppermute | solution.py:178
  48.6 7.4 %collective-permute-start.16 = (bf16[2,264,128]{2,1,0:T(8,128)(2,1)S(1)}, bf16[2,264,128]{2,1,0:T(8,128)(2,1)S(1)}, u32[]{:S(2)}, u32[]{:S(2)}) collective-permute-start(bf16[2,264,128]{2,1,0:T(8,128)(2,1)S(1)} %get-tuple-element.69), channel_id=1, source_target_pairs={{0,32},{32,0},{64,96},{96,64},{1,33},{33,1},{65,97},{97,65},{2,34}... | collective-permute-start | bytes 405512 | tf_op jit(solution)/shard_map/ppermute | solution.py:178
  48.6 12.4 %collective-permute-start.8 = (bf16[4,264,128]{2,1,0:T(8,128)(2,1)S(1)}, bf16[4,264,128]{2,1,0:T(8,128)(2,1)S(1)}, u32[]{:S(2)}, u32[]{:S(2)}) collective-permute-start(bf16[4,264,128]{2,1,0:T(8,128)(2,1)S(1)} %get-tuple-element.58), channel_id=1, source_target_pairs={{0,32},{32,64},{64,96},{96,0},{1,33},{33,65},{65,97},{97,1},{2,34}... | collective-permute-start | bytes 811016 | tf_op jit(solution)/shard_map/ppermute | solution.py:49
  50.1 11.0 %collective-permute-start.9 = (bf16[4,264,128]{2,1,0:T(8,128)(2,1)S(1)}, bf16[4,264,128]{2,1,0:T(8,128)(2,1)S(1)}, u32[]{:S(2)}, u32[]{:S(2)}) collective-permute-start(bf16[4,264,128]{2,1,0:T(8,128)(2,1)S(1)} %get-tuple-element.58), channel_id=1, source_target_pairs={{0,96},{32,0},{64,32},{96,64},{1,97},{33,1},{65,33},{97,65},{2,98}... | collective-permute-start | bytes 811016 | tf_op jit(solution)/shard_map/ppermute | solution.py:49
  56.5 7.0 %collective-permute-start.17 = (bf16[4,264,128]{2,1,0:T(8,128)(2,1)S(1)}, bf16[4,264,128]{2,1,0:T(8,128)(2,1)S(1)}, u32[]{:S(2)}, u32[]{:S(2)}) collective-permute-start(bf16[4,264,128]{2,1,0:T(8,128)(2,1)S(1)} %get-tuple-element.71), channel_id=1, source_target_pairs={{0,16},{8,24},{16,0},{24,8},{1,17},{9,25},{17,1},{25,9},{2,18},{10... | collective-permute-start | bytes 811016 | tf_op jit(solution)/shard_map/ppermute | solution.py:49
  58.4 8.0 %collective-permute-start.18 = (bf16[4,264,128]{2,1,0:T(8,128)(2,1)S(1)}, bf16[4,264,128]{2,1,0:T(8,128)(2,1)S(1)}, u32[]{:S(2)}, u32[]{:S(2)}) collective-permute-start(bf16[4,264,128]{2,1,0:T(8,128)(2,1)S(1)} %get-tuple-element.71), channel_id=1, source_target_pairs={{0,8},{8,16},{16,24},{24,0},{1,9},{9,17},{17,25},{25,1},{2,10},{10... | collective-permute-start | bytes 811016 | tf_op jit(solution)/shard_map/ppermute | solution.py:49
  58.4 8.0 %collective-permute-start.19 = (bf16[4,264,128]{2,1,0:T(8,128)(2,1)S(1)}, bf16[4,264,128]{2,1,0:T(8,128)(2,1)S(1)}, u32[]{:S(2)}, u32[]{:S(2)}) collective-permute-start(bf16[4,264,128]{2,1,0:T(8,128)(2,1)S(1)} %get-tuple-element.71), channel_id=1, source_target_pairs={{0,24},{8,0},{16,8},{24,16},{1,25},{9,1},{17,9},{25,17},{2,26},{10... | collective-permute-start | bytes 811016 | tf_op jit(solution)/shard_map/ppermute | solution.py:49
  67.9 10.4 %collective-permute-start.20 = (f32[2,128,256]{2,1,0:T(8,128)S(1)}, f32[2,128,256]{2,1,0:T(8,128)S(1)}, u32[]{:S(2)}, u32[]{:S(2)}) collective-permute-start(f32[2,128,256]{2,1,0:T(8,128)S(1)} %get-tuple-element.73.refs_0_), channel_id=1, source_target_pairs={{0,8},{8,16},{16,24},{24,0},{1,9},{9,17},{17,25},{25,1},{2,10},{10... | collective-permute-start | bytes 786440 | tf_op jit(solution)/shard_map/ppermute | solution.py:49
  69.8 36.3 %collective-permute-start.21 = (f32[2,128,256]{2,1,0:T(8,128)S(1)}, f32[2,128,256]{2,1,0:T(8,128)S(1)}, u32[]{:S(2)}, u32[]{:S(2)}) collective-permute-start(f32[2,128,256]{2,1,0:T(8,128)S(1)} %get-tuple-element.73.refs_0_), channel_id=1, source_target_pairs={{0,16},{8,24},{16,0},{24,8},{1,17},{9,25},{17,1},{25,9},{2,18},{10... | collective-permute-start | bytes 786440 | tf_op jit(solution)/shard_map/ppermute | solution.py:49
  70.5 35.7 %collective-permute-start.22 = (f32[2,128,256]{2,1,0:T(8,128)S(1)}, f32[2,128,256]{2,1,0:T(8,128)S(1)}, u32[]{:S(2)}, u32[]{:S(2)}) collective-permute-start(f32[2,128,256]{2,1,0:T(8,128)S(1)} %get-tuple-element.73.refs_0_), channel_id=1, source_target_pairs={{0,24},{8,0},{16,8},{24,16},{1,25},{9,1},{17,9},{25,17},{2,26},{10... | collective-permute-start | bytes 786440 | tf_op jit(solution)/shard_map/ppermute | solution.py:49
  72.5 33.7 %collective-permute-start.23 = (f32[2,128,256]{2,1,0:T(8,128)S(1)}, f32[2,128,256]{2,1,0:T(8,128)S(1)}, u32[]{:S(2)}, u32[]{:S(2)}) collective-permute-start(f32[2,128,256]{2,1,0:T(8,128)S(1)} %get-tuple-element.74.refs_4_), channel_id=1, source_target_pairs={{0,32},{32,64},{64,96},{96,0},{1,33},{33,65},{65,97},{97,1},{2,34}... | collective-permute-start | bytes 786440 | tf_op jit(solution)/shard_map/ppermute | solution.py:49
  72.5 33.7 %collective-permute-start.24 = (f32[2,128,256]{2,1,0:T(8,128)S(1)}, f32[2,128,256]{2,1,0:T(8,128)S(1)}, u32[]{:S(2)}, u32[]{:S(2)}) collective-permute-start(f32[2,128,256]{2,1,0:T(8,128)S(1)} %get-tuple-element.74.refs_4_), channel_id=1, source_target_pairs={{0,64},{32,96},{64,0},{96,32},{1,65},{33,97},{65,1},{97,33},{2,66}... | collective-permute-start | bytes 786440 | tf_op jit(solution)/shard_map/ppermute | solution.py:49
  78.4 27.8 %collective-permute-start.25 = (f32[2,128,256]{2,1,0:T(8,128)S(1)}, f32[2,128,256]{2,1,0:T(8,128)S(1)}, u32[]{:S(2)}, u32[]{:S(2)}) collective-permute-start(f32[2,128,256]{2,1,0:T(8,128)S(1)} %get-tuple-element.74.refs_4_), channel_id=1, source_target_pairs={{0,96},{32,0},{64,32},{96,64},{1,97},{33,1},{65,33},{97,65},{2,98}... | collective-permute-start | bytes 786440 | tf_op jit(solution)/shard_map/ppermute | solution.py:49
  107.2 8.6 %collective-permute-start.30 = (bf16[4,128,256]{2,1,0:T(8,128)(2,1)S(1)}, bf16[4,128,256]{2,1,0:T(8,128)(2,1)S(1)}, u32[]{:S(2)}, u32[]{:S(2)}) collective-permute-start(bf16[4,128,256]{2,1,0:T(8,128)(2,1)S(1)} %get-tuple-element.77.refs_0_), channel_id=1, source_target_pairs={{0,16},{8,24},{16,0},{24,8},{1,17},{9,25},{17,1},{25,9},{2,18},{10... | collective-permute-start | bytes 786440 | tf_op jit(solution)/shard_map/ppermute | solution.py:49
  108.3 11.7 %collective-permute-start.31 = (bf16[4,128,256]{2,1,0:T(8,128)(2,1)S(1)}, bf16[4,128,256]{2,1,0:T(8,128)(2,1)S(1)}, u32[]{:S(2)}, u32[]{:S(2)}) collective-permute-start(bf16[4,128,256]{2,1,0:T(8,128)(2,1)S(1)} %get-tuple-element.78.refs_1_), channel_id=1, source_target_pairs={{0,64},{32,96},{64,0},{96,32},{1,65},{33,97},{65,1},{97,33},{2,66}... | collective-permute-start | bytes 786440 | tf_op jit(solution)/shard_map/ppermute | solution.py:49
  109.0 13.6 %collective-permute-start.28 = (bf16[4,128,256]{2,1,0:T(8,128)(2,1)S(1)}, bf16[4,128,256]{2,1,0:T(8,128)(2,1)S(1)}, u32[]{:S(2)}, u32[]{:S(2)}) collective-permute-start(bf16[4,128,256]{2,1,0:T(8,128)(2,1)S(1)} %get-tuple-element.77.refs_0_), channel_id=1, source_target_pairs={{0,8},{8,16},{16,24},{24,0},{1,9},{9,17},{17,25},{25,1},{2,10},{10... | collective-permute-start | bytes 786440 | tf_op jit(solution)/shard_map/ppermute | solution.py:49
  109.4 14.2 %collective-permute-start.29 = (bf16[4,128,256]{2,1,0:T(8,128)(2,1)S(1)}, bf16[4,128,256]{2,1,0:T(8,128)(2,1)S(1)}, u32[]{:S(2)}, u32[]{:S(2)}) collective-permute-start(bf16[4,128,256]{2,1,0:T(8,128)(2,1)S(1)} %get-tuple-element.78.refs_1_), channel_id=1, source_target_pairs={{0,32},{32,64},{64,96},{96,0},{1,33},{33,65},{65,97},{97,1},{2,34}... | collective-permute-start | bytes 786440 | tf_op jit(solution)/shard_map/ppermute | solution.py:49
  109.9 14.6 %collective-permute-start.26 = (bf16[4,128,256]{2,1,0:T(8,128)(2,1)S(1)}, bf16[4,128,256]{2,1,0:T(8,128)(2,1)S(1)}, u32[]{:S(2)}, u32[]{:S(2)}) collective-permute-start(bf16[4,128,256]{2,1,0:T(8,128)(2,1)S(1)} %get-tuple-element.77.refs_0_), channel_id=1, source_target_pairs={{0,24},{8,0},{16,8},{24,16},{1,25},{9,1},{17,9},{25,17},{2,26},{10... | collective-permute-start | bytes 786440 | tf_op jit(solution)/shard_map/ppermute | solution.py:49
  115.8 8.7 %collective-permute-start.27 = (bf16[4,128,256]{2,1,0:T(8,128)(2,1)S(1)}, bf16[4,128,256]{2,1,0:T(8,128)(2,1)S(1)}, u32[]{:S(2)}, u32[]{:S(2)}) collective-permute-start(bf16[4,128,256]{2,1,0:T(8,128)(2,1)S(1)} %get-tuple-element.78.refs_1_), channel_id=1, source_target_pairs={{0,96},{32,0},{64,32},{96,64},{1,97},{33,1},{65,33},{97,65},{2,98}... | collective-permute-start | bytes 786440 | tf_op jit(solution)/shard_map/ppermute | solution.py:49
  (5 other events, 173.9 us)

commit v3 on v2

--- a/solution.py
+++ b/solution.py
@@ -214,21 +214,19 @@
     sums_ref[...] = jnp.where((lane // 32) % 2 == m, mine, before_ref[...])
 
 
-def weight_kernel(sums_ref, *refs):
-    ins, (step_ref, new_ref, *lines) = refs[: 2 * RING], refs[2 * RING :]
+def weight_kernel(m, sums_ref, *refs):
+    ins, (step_ref, new_ref, line_ref) = refs[:RING], refs[RING:]
     total = jnp.sum(sums_ref[...], axis=0, keepdims=True)
-    for m in range(2):
-        grad_sq = total[:, m * 32 : m * 32 + 1]
-        raw_sq = total[:, 64 + m * 32 : 64 + m * 32 + 1]
-        scale = jnp.sqrt(grad_sq / (raw_sq + norm_eps))
-        for back in range(RING):
-            ref = ins[m * RING + back]
-            step = scale * ref[0]
-            new = ref[1] - learn_rate * step
-            if back == 0:
-                step_ref[m] = step
-                new_ref[m] = new
-            lines[m][back] = new.astype(jnp.bfloat16)
+    grad_sq = total[:, m * 32 : m * 32 + 1]
+    raw_sq = total[:, 64 + m * 32 : 64 + m * 32 + 1]
+    scale = jnp.sqrt(grad_sq / (raw_sq + norm_eps))
+    for back in range(RING):
+        step = scale * ins[back][0]
+        new = ins[back][1] - learn_rate * step
+        if back == 0:
+            step_ref[...] = step
+            new_ref[...] = new
+        line_ref[back] = new.astype(jnp.bfloat16)
 
 
 def stat_kernel(width, left_ref, right_ref, line_k, line_v, halves_k, halves_v, new_left_ref, new_right_ref):
@@ -344,17 +342,16 @@
     everyone = lax.axis_size(FS_TP)
     spread = jnp.broadcast_to(sums[None], (everyone, 1, 128))
     sums = lax.all_to_all(spread, FS_TP, 0, 0, tiled=True).reshape(everyone, 128)
-    step, new_weights, copied_k, copied_v = call(
-        weight_kernel,
-        [
-            jax.ShapeDtypeStruct(weights.shape, f32),
-            jax.ShapeDtypeStruct(weights.shape, f32),
-            pltpu.VMEM((RING, rows, columns), bf16),
-            pltpu.VMEM((RING, rows, columns), bf16),
-        ],
-        [VMEM] * 9,
-        10,
-    )(sums, *keys, *values)
+
+    def updated(m, line):
+        one = jax.ShapeDtypeStruct((rows, columns), f32)
+        return call(
+            functools.partial(weight_kernel, m), [one, one, pltpu.VMEM((RING, rows, columns), bf16)], [VMEM] * 5, 6
+        )(sums, *line)
+
+    step_v, new_v, copied_v = updated(1, values)
+    step_k, new_k, copied_k = updated(0, keys)
+    step, new_weights = jnp.stack([step_k, step_v]), jnp.stack([new_k, new_v])
     copied_v = [copied_v, *exchange(copied_v, X)]
     copied_k = [copied_k, *exchange(copied_k, Z)]
 
@@ -380,8 +377,7 @@
         )(*[(copied_k, copied_v)[m][p] for m, p in chosen], *before)
 
     copies = placed([(1, 0), (0, 0), (1, 1), (0, 1)])
-    copies = placed([(1, 2), (0, 2)], copies)
-    copies = placed([(1, 3), (0, 3)], copies)
+    copies = placed([(1, 2), (0, 2), (1, 3), (0, 3)], copies)
     return (step, new_weights, copies, new_left[:, None], new_right[:, None])
 
 

time: 126 us -> 132 us (1.048); the launches traced: 126 us -> 130 us
  blocking collectives: 27.6 us -> 0 us
  starting transfers between devices: 42.7 us -> 66.7 us
  local copies, waits for them, and re-layouts: 0.06 us -> 7.53 us
  waiting for transfers between devices: 27.4 us -> 25.2 us
  Pallas kernels: 26.7 us -> 28.5 us
    all_to_all x1 -> x0, blocking collectives: 27.6 us -> none  [on_device(): lax.all_to_all(spread, FS_TP, 0, 0, tiled=True).reshape(everyone, 128)]
    all_to_all x0 -> x1, starting transfers between devices: none -> 16.7 us  [on_device(): lax.all_to_all(spread, FS_TP, 0, 0, tiled=True).reshape(everyone, 128)]
    ppermute x24, starting transfers between devices: 33.6 us -> 40.8 us  [shift(): lax.ppermute(value, axis, [(i, (i + by) % RING) for i in range(RING)])]
    unnamed x10 -> x18, local copies, waits for them, and re-layouts: 0.02 us -> 6.87 us
    ppermute x24, waiting for transfers between devices: 17.3 us -> 10.9 us  [shift(): lax.ppermute(value, axis, [(i, (i + by) % RING) for i in range(RING)])]
    all_to_all x0 -> x1, waiting for transfers between devices: none -> 4.16 us  [on_device(): lax.all_to_all(spread, FS_TP, 0, 0, tiled=True).reshape(everyone, 128)]
    pallas_call x1 -> x2, Pallas kernels: 1.02 us -> 2.79 us  [updated(): call(functools.partial(weight_kernel, m), [one, one, pltpu.VMEM((RING, ro...]
    pallas_call x3 -> x2, Pallas kernels: 2.8 us -> 2.2 us  [placed(): call(functools.partial(place_kernel, rows, chosen), jax.ShapeDtypeStruct(...]
  transfers between devices with their start and end apart: 32 -> 33, of which waited for: 12 -> 9; matrix products, arithmetic and copies ran while one was open for 0% -> 1% of each run, Pallas kernels for 10% -> 12%
where the time goes in v3:
time: 132 us; the launch traced here: 130 us
  starting transfers between devices  66.7 us (51%)
  Pallas kernels  28.5 us (22%)
  waiting for transfers between devices  25.2 us (19%)
  local copies, waits for them, and re-layouts  7.53 us (6%)
    ppermute x24, starting transfers between devices, shift(): lax.ppermute(value, axis, [(i, (i + by) % RING) for i in range(RING)])  40.8 us
    all_to_all x1, starting transfers between devices, on_device(): lax.all_to_all(spread, FS_TP, 0, 0, tiled=True).reshape(everyone, 128)  16.7 us
    ppermute x24, waiting for transfers between devices, shift(): lax.ppermute(value, axis, [(i, (i + by) % RING) for i in range(RING)])  10.9 us
    ppermute x8, waiting for transfers between devices, swap(): lax.ppermute(value, axis, [(i, i ^ 1 if kind == 0 else 3 - i) for i in ra...  10.1 us
    ppermute x8, starting transfers between devices, swap(): lax.ppermute(value, axis, [(i, i ^ 1 if kind == 0 else 3 - i) for i in ra...  9.16 us
    unnamed x18, local copies, waits for them, and re-layouts  6.87 us
    pallas_call x1, Pallas kernels, on_device(): call(functools.partial(first_kernel, rows), [pltpu.VMEM((tokens, features...  5.79 us
    pallas_call x1, Pallas kernels, on_device(): call(functools.partial(near_kernel, rows), [pltpu.VMEM(coded, bf16)] * 4,...  4.4 us
  transfers between devices with their start and end apart: 33, of which 9 were waited for; matrix products, arithmetic and copies ran while one was open for 1% of the time, Pallas kernels for 12%

profile of v3, /device:TPU:1, one launch (start us, length us, event | category | flops | bytes accessed | tf_op | source)
XLA Modules:
  0.0 129.8 jit_solution(4445797687610934655)
XLA Ops:
  0.6 5.8 %shard_map.119 = (bf16[3072,2048]{1,0:T(8,128)(2,1)S(1)}, bf16[256,3072]{1,0:T(8,128)(2,1)S(1)}, bf16[256,3072]{1,0:T(8,128)(2,1)S(1)}, bf16[4,264,128]{2,1,0:T(8,128)(2,1)S(1)}, bf16[4,264,128]{2,1,0:T(8,128)(2,1)S(1)}) custom-call(bf16[3072,2048]{1,0:T(8,128)(2,1)} %x_hbm.1, bf16[3072,256]{1,0:T(8,128)(2,1)} %k_hbm.1, bf16[3072,256]{1,0:T(8,128)(2,1)} %v_hbm.1), custom_call_target="tpu_custom_call" | custom-call | tf_op jit(solution)/shard_map/pallas_call | solution.py:278
  6.4 4.4 %shard_map.121 = (bf16[4,264,128]{2,1,0:T(8,128)(2,1)S(1)}, bf16[4,264,128]{2,1,0:T(8,128)(2,1)S(1)}, bf16[4,264,128]{2,1,0:T(8,128)(2,1)S(1)}, bf16[4,264,128]{2,1,0:T(8,128)(2,1)S(1)}) custom-call(bf16[3072,2048]{1,0:T(8,128)(2,1)S(1)} %get-tuple-element.46.x_ref, bf16[256,3072]{1,0:T(8,128)(2,1)S(1)} %get-tuple-element.47.kt_ref, ...), custom_call_target="tpu_custom_call" | custom-call | tf_op jit(solution)/shard_map/pallas_call | solution.py:296
  10.8 2.5 %collective-permute-start.1 = (bf16[4,264,128]{2,1,0:T(8,128)(2,1)S(1)}, bf16[4,264,128]{2,1,0:T(8,128)(2,1)S(1)}, u32[]{:S(2)}, u32[]{:S(2)}) collective-permute-start(bf16[4,264,128]{2,1,0:T(8,128)(2,1)S(1)} %get-tuple-element.51), channel_id=1, source_target_pairs={{0,32},{32,64},{64,96},{96,0},{1,33},{33,65},{65,97},{97,1},{2,34}... | collective-permute-start | bytes 811016 | tf_op jit(solution)/shard_map/ppermute | solution.py:49
  13.3 2.2 %collective-permute-start.2 = (bf16[4,264,128]{2,1,0:T(8,128)(2,1)S(1)}, bf16[4,264,128]{2,1,0:T(8,128)(2,1)S(1)}, u32[]{:S(2)}, u32[]{:S(2)}) collective-permute-start(bf16[4,264,128]{2,1,0:T(8,128)(2,1)S(1)} %get-tuple-element.52), channel_id=1, source_target_pairs={{0,96},{32,0},{64,32},{96,64},{1,97},{33,1},{65,33},{97,65},{2,98}... | collective-permute-start | bytes 811016 | tf_op jit(solution)/shard_map/ppermute | solution.py:49
  19.5 1.9 %shard_map.120 = (f32[4,256,128]{2,1,0:T(8,128)S(1)}, f32[4,256,128]{2,1,0:T(8,128)S(1)}) custom-call(bf16[3072,2048]{1,0:T(8,128)(2,1)S(1)} %get-tuple-element.46.x_ref, bf16[256,3072]{1,0:T(8,128)(2,1)S(1)} %get-tuple-element.47.kt_ref, bf16[256,3072]{1,0:T(8,128)(2,1)S(1)} %get-tuple-element.48.vt_ref), custom_call_target="tpu_custom_call" | custom-call | tf_op jit(solution)/shard_map/pallas_call | solution.py:301
  21.6 2.8 %collective-permute-start.10 = (bf16[4,264,128]{2,1,0:T(8,128)(2,1)S(1)}, bf16[4,264,128]{2,1,0:T(8,128)(2,1)S(1)}, u32[]{:S(2)}, u32[]{:S(2)}) collective-permute-start(bf16[4,264,128]{2,1,0:T(8,128)(2,1)S(1)} %get-tuple-element.63), channel_id=1, source_target_pairs={{0,16},{8,24},{16,0},{24,8},{1,17},{9,25},{17,1},{25,9},{2,18},{10... | collective-permute-start | bytes 811016 | tf_op jit(solution)/shard_map/ppermute | solution.py:49
  24.4 3.9 %collective-permute-done.a_ref = bf16[4,264,128]{2,1,0:T(8,128)(2,1)S(1)} collective-permute-done((bf16[4,264,128]{2,1,0:T(8,128)(2,1)S(1)}, bf16[4,264,128]{2,1,0:T(8,128)(2,1)S(1)}, u32[]{:S(2)}, u32[]{:S(2)}) %collective-permute-start) | collective-permute-done | bytes 270368 | tf_op jit(solution)/shard_map/ppermute | solution.py:49
  30.5 1.8 %collective-permute-start.4 = (bf16[2,264,128]{2,1,0:T(8,128)(2,1)S(1)}, bf16[2,264,128]{2,1,0:T(8,128)(2,1)S(1)}, u32[]{:S(2)}, u32[]{:S(2)}) collective-permute-start(bf16[2,264,128]{2,1,0:T(8,128)(2,1)S(1)} %get-tuple-element.55), channel_id=1, source_target_pairs={{0,24},{8,16},{16,8},{24,0},{1,25},{9,17},{17,9},{25,1},{2,26},{10... | collective-permute-start | bytes 405512 | tf_op jit(solution)/shard_map/ppermute | solution.py:178
  33.5 2.1 %collective-permute-done.4.b_ref = bf16[2,264,128]{2,1,0:T(8,128)(2,1)S(1)} collective-permute-done((bf16[2,264,128]{2,1,0:T(8,128)(2,1)S(1)}, bf16[2,264,128]{2,1,0:T(8,128)(2,1)S(1)}, u32[]{:S(2)}, u32[]{:S(2)}) %collective-permute-start.4) | collective-permute-done | bytes 135200 | tf_op jit(solution)/shard_map/ppermute | solution.py:178
  36.0 1.9 %collective-permute-start.5 = (bf16[2,264,128]{2,1,0:T(8,128)(2,1)S(1)}, bf16[2,264,128]{2,1,0:T(8,128)(2,1)S(1)}, u32[]{:S(2)}, u32[]{:S(2)}) collective-permute-start(bf16[2,264,128]{2,1,0:T(8,128)(2,1)S(1)} %get-tuple-element.57), channel_id=1, source_target_pairs={{0,24},{8,16},{16,8},{24,0},{1,25},{9,17},{17,9},{25,1},{2,26},{10... | collective-permute-start | bytes 405512 | tf_op jit(solution)/shard_map/ppermute | solution.py:178
  38.9 3.2 %collective-permute-start.13 = (bf16[2,264,128]{2,1,0:T(8,128)(2,1)S(1)}, bf16[2,264,128]{2,1,0:T(8,128)(2,1)S(1)}, u32[]{:S(2)}, u32[]{:S(2)}) collective-permute-start(bf16[2,264,128]{2,1,0:T(8,128)(2,1)S(1)} %get-tuple-element.67), channel_id=1, source_target_pairs={{0,32},{32,0},{64,96},{96,64},{1,33},{33,1},{65,97},{97,65},{2,34}... | collective-permute-start | bytes 405512 | tf_op jit(solution)/shard_map/ppermute | solution.py:178
  42.7 2.6 %collective-permute-start.7 = (bf16[4,264,128]{2,1,0:T(8,128)(2,1)S(1)}, bf16[4,264,128]{2,1,0:T(8,128)(2,1)S(1)}, u32[]{:S(2)}, u32[]{:S(2)}) collective-permute-start(bf16[4,264,128]{2,1,0:T(8,128)(2,1)S(1)} %get-tuple-element.60), channel_id=1, source_target_pairs={{0,64},{32,96},{64,0},{96,32},{1,65},{33,97},{65,1},{97,33},{2,66}... | collective-permute-start | bytes 811016 | tf_op jit(solution)/shard_map/ppermute | solution.py:49
  45.4 2.1 %collective-permute-done.14.b_ref = bf16[2,264,128]{2,1,0:T(8,128)(2,1)S(1)} collective-permute-done((bf16[2,264,128]{2,1,0:T(8,128)(2,1)S(1)}, bf16[2,264,128]{2,1,0:T(8,128)(2,1)S(1)}, u32[]{:S(2)}, u32[]{:S(2)}) %collective-permute-start.14) | collective-permute-done | bytes 135200 | tf_op jit(solution)/shard_map/ppermute | solution.py:178
  51.3 4.7 %collective-permute-done.15.a_ref = bf16[2,264,128]{2,1,0:T(8,128)(2,1)S(1)} collective-permute-done((bf16[2,264,128]{2,1,0:T(8,128)(2,1)S(1)}, bf16[2,264,128]{2,1,0:T(8,128)(2,1)S(1)}, u32[]{:S(2)}, u32[]{:S(2)}) %collective-permute-start.15) | collective-permute-done | bytes 135200 | tf_op jit(solution)/shard_map/ppermute | solution.py:178
  56.5 1.9 %collective-permute-start.17 = (bf16[4,264,128]{2,1,0:T(8,128)(2,1)S(1)}, bf16[4,264,128]{2,1,0:T(8,128)(2,1)S(1)}, u32[]{:S(2)}, u32[]{:S(2)}) collective-permute-start(bf16[4,264,128]{2,1,0:T(8,128)(2,1)S(1)} %get-tuple-element.73), channel_id=1, source_target_pairs={{0,16},{8,24},{16,0},{24,8},{1,17},{9,25},{17,1},{25,9},{2,18},{10... | collective-permute-start | bytes 811016 | tf_op jit(solution)/shard_map/ppermute | solution.py:49
  58.4 2.7 %collective-permute-start.19 = (bf16[4,264,128]{2,1,0:T(8,128)(2,1)S(1)}, bf16[4,264,128]{2,1,0:T(8,128)(2,1)S(1)}, u32[]{:S(2)}, u32[]{:S(2)}) collective-permute-start(bf16[4,264,128]{2,1,0:T(8,128)(2,1)S(1)} %get-tuple-element.73), channel_id=1, source_target_pairs={{0,24},{8,0},{16,8},{24,16},{1,25},{9,1},{17,9},{25,17},{2,26},{10... | collective-permute-start | bytes 811016 | tf_op jit(solution)/shard_map/ppermute | solution.py:49
  61.1 1.6 %shard_map.125 = (f32[2,128,256]{2,1,0:T(8,128)S(1)}, f32[1,128]{1,0:T(1,128)S(1)}, bf16[8,2,256,256]{3,2,1,0:T(8,128)(2,1)S(1)}) custom-call(f32[2,128,2048]{2,1,0:T(8,128)S(1)} %bitcast.16, f32[2,256,256]{2,1,0:T(8,128)S(1)} %bitcast.18, f32[1,128]{1,0:T(1,128)S(1)} %broadcast_in_dim.17.before_ref, f32[2,128,256]{2,1,0:T(8,128)S(1)} %copy-done.7, ...), custom_call_target="tpu_custom_call" | custom-call | tf_op jit(solution)/shard_map/pallas_call | solution.py:326
  64.0 2.4 %collective-permute-done.18.b_ref = bf16[4,264,128]{2,1,0:T(8,128)(2,1)S(1)} collective-permute-done((bf16[4,264,128]{2,1,0:T(8,128)(2,1)S(1)}, bf16[4,264,128]{2,1,0:T(8,128)(2,1)S(1)}, u32[]{:S(2)}, u32[]{:S(2)}) %collective-permute-start.18) | collective-permute-done | bytes 270368 | tf_op jit(solution)/shard_map/ppermute | solution.py:49
  66.3 2.1 %shard_map.129 = (f32[2,128,256]{2,1,0:T(8,128)}, f32[1,128]{1,0:T(1,128)S(1)}, bf16[8,2,256,256]{3,2,1,0:T(8,128)(2,1)S(1)}) custom-call(f32[2,128,2048]{2,1,0:T(8,128)S(1)} %bitcast.17, f32[2,256,256]{2,1,0:T(8,128)S(1)} %bitcast.19, f32[1,128]{1,0:T(1,128)S(1)} %get-tuple-element.61.before_ref, f32[2,128,256]{2,1,0:T(8,128)S(1)} %copy-done.7, ...), custom_call_target="tpu_custom_call" | custom-call | tf_op jit(solution)/shard_map/pallas_call | solution.py:326
  69.8 1.8 %collective-permute-start.20 = (f32[2,128,256]{2,1,0:T(8,128)}, f32[2,128,256]{2,1,0:T(8,128)}, u32[]{:S(2)}, u32[]{:S(2)}) collective-permute-start(f32[2,128,256]{2,1,0:T(8,128)} %get-tuple-element.75.refs_0_), channel_id=1, source_target_pairs={{0,8},{8,16},{16,24},{24,0},{1,9},{9,17},{17,25},{25,1},{2,10},{10... | collective-permute-start | bytes 786440 | tf_op jit(solution)/shard_map/ppermute | solution.py:49
  72.2 2.1 %collective-permute-start.22 = (f32[2,128,256]{2,1,0:T(8,128)}, f32[2,128,256]{2,1,0:T(8,128)}, u32[]{:S(2)}, u32[]{:S(2)}) collective-permute-start(f32[2,128,256]{2,1,0:T(8,128)} %get-tuple-element.75.refs_0_), channel_id=1, source_target_pairs={{0,24},{8,0},{16,8},{24,16},{1,25},{9,1},{17,9},{25,17},{2,26},{10... | collective-permute-start | bytes 786440 | tf_op jit(solution)/shard_map/ppermute | solution.py:49
  74.9 16.7 %all-to-all-start = ((f32[128,1,128]{2,1,0:T(1,128)}), f32[128,1,128]{2,1,0:T(1,128)S(1)}, u32[]{:S(2)}, u32[]{:S(2)}) async-start(f32[128,1,128]{2,1,0:T(1,128)} %broadcast_in_dim.19), calls=%async_computation | async-start | bytes 131072 | tf_op jit(solution)/shard_map/all_to_all | solution.py:344
  91.7 1.6 %collective-permute-start.23 = (f32[2,128,256]{2,1,0:T(8,128)S(1)}, f32[2,128,256]{2,1,0:T(8,128)}, u32[]{:S(2)}, u32[]{:S(2)}) collective-permute-start(f32[2,128,256]{2,1,0:T(8,128)S(1)} %get-tuple-element.77.refs_0_), channel_id=1, source_target_pairs={{0,32},{32,64},{64,96},{96,0},{1,33},{33,65},{65,97},{97,1},{2,34}... | collective-permute-start | bytes 786440 | tf_op jit(solution)/shard_map/ppermute | solution.py:49
  93.2 2.9 %collective-permute-start.24 = (f32[2,128,256]{2,1,0:T(8,128)S(1)}, f32[2,128,256]{2,1,0:T(8,128)}, u32[]{:S(2)}, u32[]{:S(2)}) collective-permute-start(f32[2,128,256]{2,1,0:T(8,128)S(1)} %get-tuple-element.77.refs_0_), channel_id=1, source_target_pairs={{0,64},{32,96},{64,0},{96,32},{1,65},{33,97},{65,1},{97,33},{2,66}... | collective-permute-start | bytes 786440 | tf_op jit(solution)/shard_map/ppermute | solution.py:49
  97.1 4.2 %all-to-all-done = f32[128,1,128]{2,1,0:T(1,128)S(1)} async-done(((f32[128,1,128]{2,1,0:T(1,128)}), f32[128,1,128]{2,1,0:T(1,128)S(1)}, u32[]{:S(2)}, u32[]{:S(2)}) %all-to-all-start) | async-done | bytes 65568 | tf_op jit(solution)/shard_map/all_to_all | solution.py:344
  104.2 4.4 %collective-permute-done.24.refs_2_ = f32[2,128,256]{2,1,0:T(8,128)} collective-permute-done((f32[2,128,256]{2,1,0:T(8,128)S(1)}, f32[2,128,256]{2,1,0:T(8,128)}, u32[]{:S(2)}, u32[]{:S(2)}) %collective-permute-start.24) | collective-permute-done | bytes 262176 | tf_op jit(solution)/shard_map/ppermute | solution.py:49
  110.0 2.7 %collective-permute-start.30 = (bf16[4,128,256]{2,1,0:T(8,128)(2,1)S(1)}, bf16[4,128,256]{2,1,0:T(8,128)(2,1)S(1)}, u32[]{:S(2)}, u32[]{:S(2)}) collective-permute-start(bf16[4,128,256]{2,1,0:T(8,128)(2,1)S(1)} %get-tuple-element.81.refs_0_), channel_id=1, source_target_pairs={{0,16},{8,24},{16,0},{24,8},{1,17},{9,25},{17,1},{25,9},{2,18},{10... | collective-permute-start | bytes 786440 | tf_op jit(solution)/shard_map/ppermute | solution.py:49
  113.6 1.8 %collective-permute-start.29 = (bf16[4,128,256]{2,1,0:T(8,128)(2,1)S(1)}, bf16[4,128,256]{2,1,0:T(8,128)(2,1)S(1)}, u32[]{:S(2)}, u32[]{:S(2)}) collective-permute-start(bf16[4,128,256]{2,1,0:T(8,128)(2,1)S(1)} %get-tuple-element.82.refs_1_), channel_id=1, source_target_pairs={{0,96},{32,0},{64,32},{96,64},{1,97},{33,1},{65,33},{97,65},{2,98}... | collective-permute-start | bytes 786440 | tf_op jit(solution)/shard_map/ppermute | solution.py:49
  115.8 2.4 %collective-permute-start.28 = (bf16[4,128,256]{2,1,0:T(8,128)(2,1)S(1)}, bf16[4,128,256]{2,1,0:T(8,128)(2,1)S(1)}, u32[]{:S(2)}, u32[]{:S(2)}) collective-permute-start(bf16[4,128,256]{2,1,0:T(8,128)(2,1)S(1)} %get-tuple-element.81.refs_0_), channel_id=1, source_target_pairs={{0,24},{8,0},{16,8},{24,16},{1,25},{9,1},{17,9},{25,17},{2,26},{10... | collective-permute-start | bytes 786440 | tf_op jit(solution)/shard_map/ppermute | solution.py:49
  118.1 1.6 %copy-done.4 = bf16[8,2,256,256]{3,2,1,0:T(8,128)(2,1)S(1)} copy-done((bf16[8,2,256,256]{3,2,1,0:T(8,128)(2,1)S(1)}, bf16[8,2,256,256]{3,2,1,0:T(8,128)(2,1)}, u32[]{:S(2)}) %copy-start.4) | copy-done | bytes 2097176
  119.7 1.6 %copy-done.6 = bf16[8,2,256,256]{3,2,1,0:T(8,128)(2,1)S(1)} copy-done((bf16[8,2,256,256]{3,2,1,0:T(8,128)(2,1)S(1)}, bf16[8,2,256,256]{3,2,1,0:T(8,128)(2,1)}, u32[]{:S(2)}) %copy-start.6) | copy-done | bytes 2097176
  122.3 4.2 %shard_map.134 = (f32[2,128,2048]{2,1,0:T(8,128)}, f32[2,256,256]{2,1,0:T(8,128)}) custom-call(f32[2,128,2048]{2,1,0:T(8,128)S(1)} %bitcast.20, f32[2,256,256]{2,1,0:T(8,128)S(1)} %bitcast.23, f32[4,256,128]{2,1,0:T(8,128)S(1)} %get-tuple-element.72.line_ref.line_k, f32[4,256,128]{2,1,0:T(8,128)S(1)} %get-tuple-element.59.line_ref.line_v, ...), custom_call_target="tpu_custom_call" | custom-call | tf_op jit(solution)/shard_map/pallas_call | solution.py:358
  (71 shorter events, 28.4 us)
Async XLA Ops:
  10.8 10.8 %collective-permute-start.1 = (bf16[4,264,128]{2,1,0:T(8,128)(2,1)S(1)}, bf16[4,264,128]{2,1,0:T(8,128)(2,1)S(1)}, u32[]{:S(2)}, u32[]{:S(2)}) collective-permute-start(bf16[4,264,128]{2,1,0:T(8,128)(2,1)S(1)} %get-tuple-element.51), channel_id=1, source_target_pairs={{0,32},{32,64},{64,96},{96,0},{1,33},{33,65},{65,97},{97,1},{2,34}... | collective-permute-start | bytes 811016 | tf_op jit(solution)/shard_map/ppermute | solution.py:49
  13.3 11.1 %collective-permute-start.2 = (bf16[4,264,128]{2,1,0:T(8,128)(2,1)S(1)}, bf16[4,264,128]{2,1,0:T(8,128)(2,1)S(1)}, u32[]{:S(2)}, u32[]{:S(2)}) collective-permute-start(bf16[4,264,128]{2,1,0:T(8,128)(2,1)S(1)} %get-tuple-element.52), channel_id=1, source_target_pairs={{0,96},{32,0},{64,32},{96,64},{1,97},{33,1},{65,33},{97,65},{2,98}... | collective-permute-start | bytes 811016 | tf_op jit(solution)/shard_map/ppermute | solution.py:49
  15.5 12.8 %collective-permute-start = (bf16[4,264,128]{2,1,0:T(8,128)(2,1)S(1)}, bf16[4,264,128]{2,1,0:T(8,128)(2,1)S(1)}, u32[]{:S(2)}, u32[]{:S(2)}) collective-permute-start(bf16[4,264,128]{2,1,0:T(8,128)(2,1)S(1)} %get-tuple-element.50), channel_id=1, source_target_pairs={{0,64},{32,96},{64,0},{96,32},{1,65},{33,97},{65,1},{97,33},{2,66}... | collective-permute-start | bytes 811016 | tf_op jit(solution)/shard_map/ppermute | solution.py:49
  16.8 21.2 %collective-permute-start.11 = (bf16[4,264,128]{2,1,0:T(8,128)(2,1)S(1)}, bf16[4,264,128]{2,1,0:T(8,128)(2,1)S(1)}, u32[]{:S(2)}, u32[]{:S(2)}) collective-permute-start(bf16[4,264,128]{2,1,0:T(8,128)(2,1)S(1)} %get-tuple-element.64), channel_id=1, source_target_pairs={{0,8},{8,16},{16,24},{24,0},{1,9},{9,17},{17,25},{25,1},{2,10},{10... | collective-permute-start | bytes 811016 | tf_op jit(solution)/shard_map/ppermute | solution.py:49
  18.0 20.0 %collective-permute-start.12 = (bf16[4,264,128]{2,1,0:T(8,128)(2,1)S(1)}, bf16[4,264,128]{2,1,0:T(8,128)(2,1)S(1)}, u32[]{:S(2)}, u32[]{:S(2)}) collective-permute-start(bf16[4,264,128]{2,1,0:T(8,128)(2,1)S(1)} %get-tuple-element.65), channel_id=1, source_target_pairs={{0,24},{8,0},{16,8},{24,16},{1,25},{9,1},{17,9},{25,17},{2,26},{10... | collective-permute-start | bytes 811016 | tf_op jit(solution)/shard_map/ppermute | solution.py:49
  21.6 16.3 %collective-permute-start.10 = (bf16[4,264,128]{2,1,0:T(8,128)(2,1)S(1)}, bf16[4,264,128]{2,1,0:T(8,128)(2,1)S(1)}, u32[]{:S(2)}, u32[]{:S(2)}) collective-permute-start(bf16[4,264,128]{2,1,0:T(8,128)(2,1)S(1)} %get-tuple-element.63), channel_id=1, source_target_pairs={{0,16},{8,24},{16,0},{24,8},{1,17},{9,25},{17,1},{25,9},{2,18},{10... | collective-permute-start | bytes 811016 | tf_op jit(solution)/shard_map/ppermute | solution.py:49
  30.5 5.1 %collective-permute-start.4 = (bf16[2,264,128]{2,1,0:T(8,128)(2,1)S(1)}, bf16[2,264,128]{2,1,0:T(8,128)(2,1)S(1)}, u32[]{:S(2)}, u32[]{:S(2)}) collective-permute-start(bf16[2,264,128]{2,1,0:T(8,128)(2,1)S(1)} %get-tuple-element.55), channel_id=1, source_target_pairs={{0,24},{8,16},{16,8},{24,0},{1,25},{9,17},{17,9},{25,1},{2,26},{10... | collective-permute-start | bytes 405512 | tf_op jit(solution)/shard_map/ppermute | solution.py:178
  36.0 6.2 %collective-permute-start.5 = (bf16[2,264,128]{2,1,0:T(8,128)(2,1)S(1)}, bf16[2,264,128]{2,1,0:T(8,128)(2,1)S(1)}, u32[]{:S(2)}, u32[]{:S(2)}) collective-permute-start(bf16[2,264,128]{2,1,0:T(8,128)(2,1)S(1)} %get-tuple-element.57), channel_id=1, source_target_pairs={{0,24},{8,16},{16,8},{24,0},{1,25},{9,17},{17,9},{25,1},{2,26},{10... | collective-permute-start | bytes 405512 | tf_op jit(solution)/shard_map/ppermute | solution.py:178
  37.9 4.3 %collective-permute-start.6 = (bf16[2,264,128]{2,1,0:T(8,128)(2,1)S(1)}, bf16[2,264,128]{2,1,0:T(8,128)(2,1)S(1)}, u32[]{:S(2)}, u32[]{:S(2)}) collective-permute-start(bf16[2,264,128]{2,1,0:T(8,128)(2,1)S(1)} %get-tuple-element.58), channel_id=1, source_target_pairs={{0,8},{8,0},{16,24},{24,16},{1,9},{9,1},{17,25},{25,17},{2,10},{10... | collective-permute-start | bytes 405512 | tf_op jit(solution)/shard_map/ppermute | solution.py:178
  38.9 6.5 %collective-permute-start.13 = (bf16[2,264,128]{2,1,0:T(8,128)(2,1)S(1)}, bf16[2,264,128]{2,1,0:T(8,128)(2,1)S(1)}, u32[]{:S(2)}, u32[]{:S(2)}) collective-permute-start(bf16[2,264,128]{2,1,0:T(8,128)(2,1)S(1)} %get-tuple-element.67), channel_id=1, source_target_pairs={{0,32},{32,0},{64,96},{96,64},{1,33},{33,1},{65,97},{97,65},{2,34}... | collective-permute-start | bytes 405512 | tf_op jit(solution)/shard_map/ppermute | solution.py:178
  42.0 5.4 %collective-permute-start.14 = (bf16[2,264,128]{2,1,0:T(8,128)(2,1)S(1)}, bf16[2,264,128]{2,1,0:T(8,128)(2,1)S(1)}, u32[]{:S(2)}, u32[]{:S(2)}) collective-permute-start(bf16[2,264,128]{2,1,0:T(8,128)(2,1)S(1)} %get-tuple-element.68), channel_id=1, source_target_pairs={{0,96},{32,64},{64,32},{96,0},{1,97},{33,65},{65,33},{97,1},{2,98}... | collective-permute-start | bytes 405512 | tf_op jit(solution)/shard_map/ppermute | solution.py:178
  42.7 15.7 %collective-permute-start.7 = (bf16[4,264,128]{2,1,0:T(8,128)(2,1)S(1)}, bf16[4,264,128]{2,1,0:T(8,128)(2,1)S(1)}, u32[]{:S(2)}, u32[]{:S(2)}) collective-permute-start(bf16[4,264,128]{2,1,0:T(8,128)(2,1)S(1)} %get-tuple-element.60), channel_id=1, source_target_pairs={{0,64},{32,96},{64,0},{96,32},{1,65},{33,97},{65,1},{97,33},{2,66}... | collective-permute-start | bytes 811016 | tf_op jit(solution)/shard_map/ppermute | solution.py:49
  47.9 8.1 %collective-permute-start.15 = (bf16[2,264,128]{2,1,0:T(8,128)(2,1)S(1)}, bf16[2,264,128]{2,1,0:T(8,128)(2,1)S(1)}, u32[]{:S(2)}, u32[]{:S(2)}) collective-permute-start(bf16[2,264,128]{2,1,0:T(8,128)(2,1)S(1)} %get-tuple-element.70), channel_id=1, source_target_pairs={{0,96},{32,64},{64,32},{96,0},{1,97},{33,65},{65,33},{97,1},{2,98}... | collective-permute-start | bytes 405512 | tf_op jit(solution)/shard_map/ppermute | solution.py:178
  48.6 7.4 %collective-permute-start.16 = (bf16[2,264,128]{2,1,0:T(8,128)(2,1)S(1)}, bf16[2,264,128]{2,1,0:T(8,128)(2,1)S(1)}, u32[]{:S(2)}, u32[]{:S(2)}) collective-permute-start(bf16[2,264,128]{2,1,0:T(8,128)(2,1)S(1)} %get-tuple-element.71), channel_id=1, source_target_pairs={{0,32},{32,0},{64,96},{96,64},{1,33},{33,1},{65,97},{97,65},{2,34}... | collective-permute-start | bytes 405512 | tf_op jit(solution)/shard_map/ppermute | solution.py:178
  48.6 12.4 %collective-permute-start.8 = (bf16[4,264,128]{2,1,0:T(8,128)(2,1)S(1)}, bf16[4,264,128]{2,1,0:T(8,128)(2,1)S(1)}, u32[]{:S(2)}, u32[]{:S(2)}) collective-permute-start(bf16[4,264,128]{2,1,0:T(8,128)(2,1)S(1)} %get-tuple-element.60), channel_id=1, source_target_pairs={{0,32},{32,64},{64,96},{96,0},{1,33},{33,65},{65,97},{97,1},{2,34}... | collective-permute-start | bytes 811016 | tf_op jit(solution)/shard_map/ppermute | solution.py:49
  50.1 11.0 %collective-permute-start.9 = (bf16[4,264,128]{2,1,0:T(8,128)(2,1)S(1)}, bf16[4,264,128]{2,1,0:T(8,128)(2,1)S(1)}, u32[]{:S(2)}, u32[]{:S(2)}) collective-permute-start(bf16[4,264,128]{2,1,0:T(8,128)(2,1)S(1)} %get-tuple-element.60), channel_id=1, source_target_pairs={{0,96},{32,0},{64,32},{96,64},{1,97},{33,1},{65,33},{97,65},{2,98}... | collective-permute-start | bytes 811016 | tf_op jit(solution)/shard_map/ppermute | solution.py:49
  56.5 7.5 %collective-permute-start.17 = (bf16[4,264,128]{2,1,0:T(8,128)(2,1)S(1)}, bf16[4,264,128]{2,1,0:T(8,128)(2,1)S(1)}, u32[]{:S(2)}, u32[]{:S(2)}) collective-permute-start(bf16[4,264,128]{2,1,0:T(8,128)(2,1)S(1)} %get-tuple-element.73), channel_id=1, source_target_pairs={{0,16},{8,24},{16,0},{24,8},{1,17},{9,25},{17,1},{25,9},{2,18},{10... | collective-permute-start | bytes 811016 | tf_op jit(solution)/shard_map/ppermute | solution.py:49
  58.4 8.0 %collective-permute-start.18 = (bf16[4,264,128]{2,1,0:T(8,128)(2,1)S(1)}, bf16[4,264,128]{2,1,0:T(8,128)(2,1)S(1)}, u32[]{:S(2)}, u32[]{:S(2)}) collective-permute-start(bf16[4,264,128]{2,1,0:T(8,128)(2,1)S(1)} %get-tuple-element.73), channel_id=1, source_target_pairs={{0,8},{8,16},{16,24},{24,0},{1,9},{9,17},{17,25},{25,1},{2,10},{10... | collective-permute-start | bytes 811016 | tf_op jit(solution)/shard_map/ppermute | solution.py:49
  58.4 8.0 %collective-permute-start.19 = (bf16[4,264,128]{2,1,0:T(8,128)(2,1)S(1)}, bf16[4,264,128]{2,1,0:T(8,128)(2,1)S(1)}, u32[]{:S(2)}, u32[]{:S(2)}) collective-permute-start(bf16[4,264,128]{2,1,0:T(8,128)(2,1)S(1)} %get-tuple-element.73), channel_id=1, source_target_pairs={{0,24},{8,0},{16,8},{24,16},{1,25},{9,1},{17,9},{25,17},{2,26},{10... | collective-permute-start | bytes 811016 | tf_op jit(solution)/shard_map/ppermute | solution.py:49
  69.8 26.3 %collective-permute-start.20 = (f32[2,128,256]{2,1,0:T(8,128)}, f32[2,128,256]{2,1,0:T(8,128)}, u32[]{:S(2)}, u32[]{:S(2)}) collective-permute-start(f32[2,128,256]{2,1,0:T(8,128)} %get-tuple-element.75.refs_0_), channel_id=1, source_target_pairs={{0,8},{8,16},{16,24},{24,0},{1,9},{9,17},{17,25},{25,1},{2,10},{10... | collective-permute-start | bytes 786440 | tf_op jit(solution)/shard_map/ppermute | solution.py:49
  71.6 29.6 %collective-permute-start.21 = (f32[2,128,256]{2,1,0:T(8,128)}, f32[2,128,256]{2,1,0:T(8,128)}, u32[]{:S(2)}, u32[]{:S(2)}) collective-permute-start(f32[2,128,256]{2,1,0:T(8,128)} %get-tuple-element.75.refs_0_), channel_id=1, source_target_pairs={{0,16},{8,24},{16,0},{24,8},{1,17},{9,25},{17,1},{25,9},{2,18},{10... | collective-permute-start | bytes 786440 | tf_op jit(solution)/shard_map/ppermute | solution.py:49
  72.2 29.0 %collective-permute-start.22 = (f32[2,128,256]{2,1,0:T(8,128)}, f32[2,128,256]{2,1,0:T(8,128)}, u32[]{:S(2)}, u32[]{:S(2)}) collective-permute-start(f32[2,128,256]{2,1,0:T(8,128)} %get-tuple-element.75.refs_0_), channel_id=1, source_target_pairs={{0,24},{8,0},{16,8},{24,16},{1,25},{9,1},{17,9},{25,17},{2,26},{10... | collective-permute-start | bytes 786440 | tf_op jit(solution)/shard_map/ppermute | solution.py:49
  74.9 26.3 %all-to-all-start = ((f32[128,1,128]{2,1,0:T(1,128)}), f32[128,1,128]{2,1,0:T(1,128)S(1)}, u32[]{:S(2)}, u32[]{:S(2)}) async-start(f32[128,1,128]{2,1,0:T(1,128)} %broadcast_in_dim.19), calls=%async_computation | async-start | bytes 131072 | tf_op jit(solution)/shard_map/all_to_all | solution.py:344
  91.7 12.5 %collective-permute-start.23 = (f32[2,128,256]{2,1,0:T(8,128)S(1)}, f32[2,128,256]{2,1,0:T(8,128)}, u32[]{:S(2)}, u32[]{:S(2)}) collective-permute-start(f32[2,128,256]{2,1,0:T(8,128)S(1)} %get-tuple-element.77.refs_0_), channel_id=1, source_target_pairs={{0,32},{32,64},{64,96},{96,0},{1,33},{33,65},{65,97},{97,1},{2,34}... | collective-permute-start | bytes 786440 | tf_op jit(solution)/shard_map/ppermute | solution.py:49
  93.2 15.3 %collective-permute-start.24 = (f32[2,128,256]{2,1,0:T(8,128)S(1)}, f32[2,128,256]{2,1,0:T(8,128)}, u32[]{:S(2)}, u32[]{:S(2)}) collective-permute-start(f32[2,128,256]{2,1,0:T(8,128)S(1)} %get-tuple-element.77.refs_0_), channel_id=1, source_target_pairs={{0,64},{32,96},{64,0},{96,32},{1,65},{33,97},{65,1},{97,33},{2,66}... | collective-permute-start | bytes 786440 | tf_op jit(solution)/shard_map/ppermute | solution.py:49
  96.2 12.4 %collective-permute-start.25 = (f32[2,128,256]{2,1,0:T(8,128)S(1)}, f32[2,128,256]{2,1,0:T(8,128)}, u32[]{:S(2)}, u32[]{:S(2)}) collective-permute-start(f32[2,128,256]{2,1,0:T(8,128)S(1)} %get-tuple-element.77.refs_0_), channel_id=1, source_target_pairs={{0,96},{32,0},{64,32},{96,64},{1,97},{33,1},{65,33},{97,65},{2,98}... | collective-permute-start | bytes 786440 | tf_op jit(solution)/shard_map/ppermute | solution.py:49
  102.6 13.1 %collective-permute-start.31 = (bf16[4,128,256]{2,1,0:T(8,128)(2,1)S(1)}, bf16[4,128,256]{2,1,0:T(8,128)(2,1)S(1)}, u32[]{:S(2)}, u32[]{:S(2)}) collective-permute-start(bf16[4,128,256]{2,1,0:T(8,128)(2,1)S(1)} %get-tuple-element.82.refs_1_), channel_id=1, source_target_pairs={{0,64},{32,96},{64,0},{96,32},{1,65},{33,97},{65,1},{97,33},{2,66}... | collective-permute-start | bytes 786440 | tf_op jit(solution)/shard_map/ppermute | solution.py:49
  110.0 17.4 %collective-permute-start.30 = (bf16[4,128,256]{2,1,0:T(8,128)(2,1)S(1)}, bf16[4,128,256]{2,1,0:T(8,128)(2,1)S(1)}, u32[]{:S(2)}, u32[]{:S(2)}) collective-permute-start(bf16[4,128,256]{2,1,0:T(8,128)(2,1)S(1)} %get-tuple-element.81.refs_0_), channel_id=1, source_target_pairs={{0,16},{8,24},{16,0},{24,8},{1,17},{9,25},{17,1},{25,9},{2,18},{10... | collective-permute-start | bytes 786440 | tf_op jit(solution)/shard_map/ppermute | solution.py:49
  112.6 15.8 %collective-permute-start.27 = (bf16[4,128,256]{2,1,0:T(8,128)(2,1)S(1)}, bf16[4,128,256]{2,1,0:T(8,128)(2,1)S(1)}, u32[]{:S(2)}, u32[]{:S(2)}) collective-permute-start(bf16[4,128,256]{2,1,0:T(8,128)(2,1)S(1)} %get-tuple-element.82.refs_1_), channel_id=1, source_target_pairs={{0,32},{32,64},{64,96},{96,0},{1,33},{33,65},{65,97},{97,1},{2,34}... | collective-permute-start | bytes 786440 | tf_op jit(solution)/shard_map/ppermute | solution.py:49
  113.6 14.8 %collective-permute-start.29 = (bf16[4,128,256]{2,1,0:T(8,128)(2,1)S(1)}, bf16[4,128,256]{2,1,0:T(8,128)(2,1)S(1)}, u32[]{:S(2)}, u32[]{:S(2)}) collective-permute-start(bf16[4,128,256]{2,1,0:T(8,128)(2,1)S(1)} %get-tuple-element.82.refs_1_), channel_id=1, source_target_pairs={{0,96},{32,0},{64,32},{96,64},{1,97},{33,1},{65,33},{97,65},{2,98}... | collective-permute-start | bytes 786440 | tf_op jit(solution)/shard_map/ppermute | solution.py:49
  115.4 13.0 %collective-permute-start.26 = (bf16[4,128,256]{2,1,0:T(8,128)(2,1)S(1)}, bf16[4,128,256]{2,1,0:T(8,128)(2,1)S(1)}, u32[]{:S(2)}, u32[]{:S(2)}) collective-permute-start(bf16[4,128,256]{2,1,0:T(8,128)(2,1)S(1)} %get-tuple-element.81.refs_0_), channel_id=1, source_target_pairs={{0,8},{8,16},{16,24},{24,0},{1,9},{9,17},{17,25},{25,1},{2,10},{10... | collective-permute-start | bytes 786440 | tf_op jit(solution)/shard_map/ppermute | solution.py:49
  115.8 12.7 %collective-permute-start.28 = (bf16[4,128,256]{2,1,0:T(8,128)(2,1)S(1)}, bf16[4,128,256]{2,1,0:T(8,128)(2,1)S(1)}, u32[]{:S(2)}, u32[]{:S(2)}) collective-permute-start(bf16[4,128,256]{2,1,0:T(8,128)(2,1)S(1)} %get-tuple-element.81.refs_0_), channel_id=1, source_target_pairs={{0,24},{8,0},{16,8},{24,16},{1,25},{9,1},{17,9},{25,17},{2,26},{10... | collective-permute-start | bytes 786440 | tf_op jit(solution)/shard_map/ppermute | solution.py:49
  (10 other events, 135.9 us)

commit v4 on v3

--- a/solution.py
+++ b/solution.py
@@ -89,10 +89,13 @@
 
 def dot3(left, right, dims):
     (lh, ll), (rh, rl) = left, right
+    free = 1 - dims[0][0]
     dot = functools.partial(
         lax.dot_general, dimension_numbers=(dims, ((), ())), preferred_element_type=jnp.float32
     )
-    return dot(lh, rh) + (dot(lh, rl) + dot(ll, rh))
+    both = dot(jnp.concatenate([lh, ll], axis=free), rh)
+    count = lh.shape[free]
+    return both[:count] + (dot(lh, rl) + both[count:])
 
 
 def chunk(turned, x_ref, width, m, by):

time: 132 us -> 132 us (level)
  transfers between devices with their start and end apart: 33 -> 33, of which waited for: 9 -> 9; matrix products, arithmetic and copies ran while one was open for 1% -> 1% of each run, Pallas kernels for 12% -> 11%
where the time goes in v4:
time: 132 us; the launch traced here: 130 us
  starting transfers between devices  66.8 us (51%)
  Pallas kernels  28.3 us (21%)
  waiting for transfers between devices  25.5 us (19%)
  local copies, waits for them, and re-layouts  7.53 us (6%)
    ppermute x24, starting transfers between devices, shift(): lax.ppermute(value, axis, [(i, (i + by) % RING) for i in range(RING)])  40.8 us
    all_to_all x1, starting transfers between devices, on_device(): lax.all_to_all(spread, FS_TP, 0, 0, tiled=True).reshape(everyone, 128)  16.8 us
    ppermute x24, waiting for transfers between devices, shift(): lax.ppermute(value, axis, [(i, (i + by) % RING) for i in range(RING)])  11.3 us
    ppermute x8, waiting for transfers between devices, swap(): lax.ppermute(value, axis, [(i, i ^ 1 if kind == 0 else 3 - i) for i in ra...  10.1 us
    ppermute x8, starting transfers between devices, swap(): lax.ppermute(value, axis, [(i, i ^ 1 if kind == 0 else 3 - i) for i in ra...  9.16 us
    unnamed x18, local copies, waits for them, and re-layouts  6.87 us
    pallas_call x1, Pallas kernels, on_device(): call(functools.partial(first_kernel, rows), [pltpu.VMEM((tokens, features...  5.79 us
    pallas_call x1, Pallas kernels, on_device(): call(functools.partial(near_kernel, rows), [pltpu.VMEM(coded, bf16)] * 4,...  4.4 us
  transfers between devices with their start and end apart: 33, of which 9 were waited for; matrix products, arithmetic and copies ran while one was open for 1% of the time, Pallas kernels for 11%

profile of v4, /device:TPU:1, one launch (start us, length us, event | category | flops | bytes accessed | tf_op | source)
XLA Modules:
  0.0 130.0 jit_solution(15291728373141856307)
XLA Ops:
  0.6 5.8 %shard_map.119 = (bf16[3072,2048]{1,0:T(8,128)(2,1)S(1)}, bf16[256,3072]{1,0:T(8,128)(2,1)S(1)}, bf16[256,3072]{1,0:T(8,128)(2,1)S(1)}, bf16[4,264,128]{2,1,0:T(8,128)(2,1)S(1)}, bf16[4,264,128]{2,1,0:T(8,128)(2,1)S(1)}) custom-call(bf16[3072,2048]{1,0:T(8,128)(2,1)} %x_hbm.1, bf16[3072,256]{1,0:T(8,128)(2,1)} %k_hbm.1, bf16[3072,256]{1,0:T(8,128)(2,1)} %v_hbm.1), custom_call_target="tpu_custom_call" | custom-call | tf_op jit(solution)/shard_map/pallas_call | solution.py:281
  6.4 4.4 %shard_map.121 = (bf16[4,264,128]{2,1,0:T(8,128)(2,1)S(1)}, bf16[4,264,128]{2,1,0:T(8,128)(2,1)S(1)}, bf16[4,264,128]{2,1,0:T(8,128)(2,1)S(1)}, bf16[4,264,128]{2,1,0:T(8,128)(2,1)S(1)}) custom-call(bf16[3072,2048]{1,0:T(8,128)(2,1)S(1)} %get-tuple-element.46.x_ref, bf16[256,3072]{1,0:T(8,128)(2,1)S(1)} %get-tuple-element.47.kt_ref, ...), custom_call_target="tpu_custom_call" | custom-call | tf_op jit(solution)/shard_map/pallas_call | solution.py:299
  10.8 2.5 %collective-permute-start.1 = (bf16[4,264,128]{2,1,0:T(8,128)(2,1)S(1)}, bf16[4,264,128]{2,1,0:T(8,128)(2,1)S(1)}, u32[]{:S(2)}, u32[]{:S(2)}) collective-permute-start(bf16[4,264,128]{2,1,0:T(8,128)(2,1)S(1)} %get-tuple-element.51), channel_id=1, source_target_pairs={{0,32},{32,64},{64,96},{96,0},{1,33},{33,65},{65,97},{97,1},{2,34}... | collective-permute-start | bytes 811016 | tf_op jit(solution)/shard_map/ppermute | solution.py:49
  13.3 2.2 %collective-permute-start.2 = (bf16[4,264,128]{2,1,0:T(8,128)(2,1)S(1)}, bf16[4,264,128]{2,1,0:T(8,128)(2,1)S(1)}, u32[]{:S(2)}, u32[]{:S(2)}) collective-permute-start(bf16[4,264,128]{2,1,0:T(8,128)(2,1)S(1)} %get-tuple-element.52), channel_id=1, source_target_pairs={{0,96},{32,0},{64,32},{96,64},{1,97},{33,1},{65,33},{97,65},{2,98}... | collective-permute-start | bytes 811016 | tf_op jit(solution)/shard_map/ppermute | solution.py:49
  19.5 1.9 %shard_map.120 = (f32[4,256,128]{2,1,0:T(8,128)S(1)}, f32[4,256,128]{2,1,0:T(8,128)S(1)}) custom-call(bf16[3072,2048]{1,0:T(8,128)(2,1)S(1)} %get-tuple-element.46.x_ref, bf16[256,3072]{1,0:T(8,128)(2,1)S(1)} %get-tuple-element.47.kt_ref, bf16[256,3072]{1,0:T(8,128)(2,1)S(1)} %get-tuple-element.48.vt_ref), custom_call_target="tpu_custom_call" | custom-call | tf_op jit(solution)/shard_map/pallas_call | solution.py:304
  21.6 2.8 %collective-permute-start.10 = (bf16[4,264,128]{2,1,0:T(8,128)(2,1)S(1)}, bf16[4,264,128]{2,1,0:T(8,128)(2,1)S(1)}, u32[]{:S(2)}, u32[]{:S(2)}) collective-permute-start(bf16[4,264,128]{2,1,0:T(8,128)(2,1)S(1)} %get-tuple-element.63), channel_id=1, source_target_pairs={{0,16},{8,24},{16,0},{24,8},{1,17},{9,25},{17,1},{25,9},{2,18},{10... | collective-permute-start | bytes 811016 | tf_op jit(solution)/shard_map/ppermute | solution.py:49
  24.4 3.9 %collective-permute-done.a_ref = bf16[4,264,128]{2,1,0:T(8,128)(2,1)S(1)} collective-permute-done((bf16[4,264,128]{2,1,0:T(8,128)(2,1)S(1)}, bf16[4,264,128]{2,1,0:T(8,128)(2,1)S(1)}, u32[]{:S(2)}, u32[]{:S(2)}) %collective-permute-start) | collective-permute-done | bytes 270368 | tf_op jit(solution)/shard_map/ppermute | solution.py:49
  30.5 1.8 %collective-permute-start.4 = (bf16[2,264,128]{2,1,0:T(8,128)(2,1)S(1)}, bf16[2,264,128]{2,1,0:T(8,128)(2,1)S(1)}, u32[]{:S(2)}, u32[]{:S(2)}) collective-permute-start(bf16[2,264,128]{2,1,0:T(8,128)(2,1)S(1)} %get-tuple-element.55), channel_id=1, source_target_pairs={{0,24},{8,16},{16,8},{24,0},{1,25},{9,17},{17,9},{25,1},{2,26},{10... | collective-permute-start | bytes 405512 | tf_op jit(solution)/shard_map/ppermute | solution.py:181
  33.5 2.1 %collective-permute-done.4.b_ref = bf16[2,264,128]{2,1,0:T(8,128)(2,1)S(1)} collective-permute-done((bf16[2,264,128]{2,1,0:T(8,128)(2,1)S(1)}, bf16[2,264,128]{2,1,0:T(8,128)(2,1)S(1)}, u32[]{:S(2)}, u32[]{:S(2)}) %collective-permute-start.4) | collective-permute-done | bytes 135200 | tf_op jit(solution)/shard_map/ppermute | solution.py:181
  36.0 1.9 %collective-permute-start.5 = (bf16[2,264,128]{2,1,0:T(8,128)(2,1)S(1)}, bf16[2,264,128]{2,1,0:T(8,128)(2,1)S(1)}, u32[]{:S(2)}, u32[]{:S(2)}) collective-permute-start(bf16[2,264,128]{2,1,0:T(8,128)(2,1)S(1)} %get-tuple-element.57), channel_id=1, source_target_pairs={{0,24},{8,16},{16,8},{24,0},{1,25},{9,17},{17,9},{25,1},{2,26},{10... | collective-permute-start | bytes 405512 | tf_op jit(solution)/shard_map/ppermute | solution.py:181
  38.9 3.2 %collective-permute-start.13 = (bf16[2,264,128]{2,1,0:T(8,128)(2,1)S(1)}, bf16[2,264,128]{2,1,0:T(8,128)(2,1)S(1)}, u32[]{:S(2)}, u32[]{:S(2)}) collective-permute-start(bf16[2,264,128]{2,1,0:T(8,128)(2,1)S(1)} %get-tuple-element.67), channel_id=1, source_target_pairs={{0,32},{32,0},{64,96},{96,64},{1,33},{33,1},{65,97},{97,65},{2,34}... | collective-permute-start | bytes 405512 | tf_op jit(solution)/shard_map/ppermute | solution.py:181
  42.7 2.6 %collective-permute-start.7 = (bf16[4,264,128]{2,1,0:T(8,128)(2,1)S(1)}, bf16[4,264,128]{2,1,0:T(8,128)(2,1)S(1)}, u32[]{:S(2)}, u32[]{:S(2)}) collective-permute-start(bf16[4,264,128]{2,1,0:T(8,128)(2,1)S(1)} %get-tuple-element.60), channel_id=1, source_target_pairs={{0,64},{32,96},{64,0},{96,32},{1,65},{33,97},{65,1},{97,33},{2,66}... | collective-permute-start | bytes 811016 | tf_op jit(solution)/shard_map/ppermute | solution.py:49
  45.4 2.1 %collective-permute-done.14.b_ref = bf16[2,264,128]{2,1,0:T(8,128)(2,1)S(1)} collective-permute-done((bf16[2,264,128]{2,1,0:T(8,128)(2,1)S(1)}, bf16[2,264,128]{2,1,0:T(8,128)(2,1)S(1)}, u32[]{:S(2)}, u32[]{:S(2)}) %collective-permute-start.14) | collective-permute-done | bytes 135200 | tf_op jit(solution)/shard_map/ppermute | solution.py:181
  48.6 1.5 %collective-permute-start.8 = (bf16[4,264,128]{2,1,0:T(8,128)(2,1)S(1)}, bf16[4,264,128]{2,1,0:T(8,128)(2,1)S(1)}, u32[]{:S(2)}, u32[]{:S(2)}) collective-permute-start(bf16[4,264,128]{2,1,0:T(8,128)(2,1)S(1)} %get-tuple-element.60), channel_id=1, source_target_pairs={{0,32},{32,64},{64,96},{96,0},{1,33},{33,65},{65,97},{97,1},{2,34}... | collective-permute-start | bytes 811016 | tf_op jit(solution)/shard_map/ppermute | solution.py:49
  51.3 4.7 %collective-permute-done.15.a_ref = bf16[2,264,128]{2,1,0:T(8,128)(2,1)S(1)} collective-permute-done((bf16[2,264,128]{2,1,0:T(8,128)(2,1)S(1)}, bf16[2,264,128]{2,1,0:T(8,128)(2,1)S(1)}, u32[]{:S(2)}, u32[]{:S(2)}) %collective-permute-start.15) | collective-permute-done | bytes 135200 | tf_op jit(solution)/shard_map/ppermute | solution.py:181
  56.5 1.9 %collective-permute-start.17 = (bf16[4,264,128]{2,1,0:T(8,128)(2,1)S(1)}, bf16[4,264,128]{2,1,0:T(8,128)(2,1)S(1)}, u32[]{:S(2)}, u32[]{:S(2)}) collective-permute-start(bf16[4,264,128]{2,1,0:T(8,128)(2,1)S(1)} %get-tuple-element.73), channel_id=1, source_target_pairs={{0,16},{8,24},{16,0},{24,8},{1,17},{9,25},{17,1},{25,9},{2,18},{10... | collective-permute-start | bytes 811016 | tf_op jit(solution)/shard_map/ppermute | solution.py:49
  58.4 2.7 %collective-permute-start.19 = (bf16[4,264,128]{2,1,0:T(8,128)(2,1)S(1)}, bf16[4,264,128]{2,1,0:T(8,128)(2,1)S(1)}, u32[]{:S(2)}, u32[]{:S(2)}) collective-permute-start(bf16[4,264,128]{2,1,0:T(8,128)(2,1)S(1)} %get-tuple-element.73), channel_id=1, source_target_pairs={{0,24},{8,0},{16,8},{24,16},{1,25},{9,1},{17,9},{25,17},{2,26},{10... | collective-permute-start | bytes 811016 | tf_op jit(solution)/shard_map/ppermute | solution.py:49
  63.9 2.5 %collective-permute-done.18.b_ref = bf16[4,264,128]{2,1,0:T(8,128)(2,1)S(1)} collective-permute-done((bf16[4,264,128]{2,1,0:T(8,128)(2,1)S(1)}, bf16[4,264,128]{2,1,0:T(8,128)(2,1)S(1)}, u32[]{:S(2)}, u32[]{:S(2)}) %collective-permute-start.18) | collective-permute-done | bytes 270368 | tf_op jit(solution)/shard_map/ppermute | solution.py:49
  66.3 2.0 %shard_map.129 = (f32[2,128,256]{2,1,0:T(8,128)}, f32[1,128]{1,0:T(1,128)S(1)}, bf16[8,2,256,256]{3,2,1,0:T(8,128)(2,1)S(1)}) custom-call(f32[2,128,2048]{2,1,0:T(8,128)S(1)} %bitcast.17, f32[2,256,256]{2,1,0:T(8,128)S(1)} %bitcast.19, f32[1,128]{1,0:T(1,128)S(1)} %get-tuple-element.61.before_ref, f32[2,128,256]{2,1,0:T(8,128)S(1)} %copy-done.7, ...), custom_call_target="tpu_custom_call" | custom-call | tf_op jit(solution)/shard_map/pallas_call | solution.py:329
  69.7 1.8 %collective-permute-start.20 = (f32[2,128,256]{2,1,0:T(8,128)}, f32[2,128,256]{2,1,0:T(8,128)}, u32[]{:S(2)}, u32[]{:S(2)}) collective-permute-start(f32[2,128,256]{2,1,0:T(8,128)} %get-tuple-element.75.refs_0_), channel_id=1, source_target_pairs={{0,8},{8,16},{16,24},{24,0},{1,9},{9,17},{17,25},{25,1},{2,10},{10... | collective-permute-start | bytes 786440 | tf_op jit(solution)/shard_map/ppermute | solution.py:49
  72.1 2.1 %collective-permute-start.22 = (f32[2,128,256]{2,1,0:T(8,128)}, f32[2,128,256]{2,1,0:T(8,128)}, u32[]{:S(2)}, u32[]{:S(2)}) collective-permute-start(f32[2,128,256]{2,1,0:T(8,128)} %get-tuple-element.75.refs_0_), channel_id=1, source_target_pairs={{0,24},{8,0},{16,8},{24,16},{1,25},{9,1},{17,9},{25,17},{2,26},{10... | collective-permute-start | bytes 786440 | tf_op jit(solution)/shard_map/ppermute | solution.py:49
  74.8 16.8 %all-to-all-start = ((f32[128,1,128]{2,1,0:T(1,128)}), f32[128,1,128]{2,1,0:T(1,128)S(1)}, u32[]{:S(2)}, u32[]{:S(2)}) async-start(f32[128,1,128]{2,1,0:T(1,128)} %broadcast_in_dim.19), calls=%async_computation | async-start | bytes 131072 | tf_op jit(solution)/shard_map/all_to_all | solution.py:347
  91.7 1.6 %collective-permute-start.23 = (f32[2,128,256]{2,1,0:T(8,128)S(1)}, f32[2,128,256]{2,1,0:T(8,128)}, u32[]{:S(2)}, u32[]{:S(2)}) collective-permute-start(f32[2,128,256]{2,1,0:T(8,128)S(1)} %get-tuple-element.77.refs_0_), channel_id=1, source_target_pairs={{0,32},{32,64},{64,96},{96,0},{1,33},{33,65},{65,97},{97,1},{2,34}... | collective-permute-start | bytes 786440 | tf_op jit(solution)/shard_map/ppermute | solution.py:49
  93.2 2.9 %collective-permute-start.24 = (f32[2,128,256]{2,1,0:T(8,128)S(1)}, f32[2,128,256]{2,1,0:T(8,128)}, u32[]{:S(2)}, u32[]{:S(2)}) collective-permute-start(f32[2,128,256]{2,1,0:T(8,128)S(1)} %get-tuple-element.77.refs_0_), channel_id=1, source_target_pairs={{0,64},{32,96},{64,0},{96,32},{1,65},{33,97},{65,1},{97,33},{2,66}... | collective-permute-start | bytes 786440 | tf_op jit(solution)/shard_map/ppermute | solution.py:49
  97.1 4.2 %all-to-all-done = f32[128,1,128]{2,1,0:T(1,128)S(1)} async-done(((f32[128,1,128]{2,1,0:T(1,128)}), f32[128,1,128]{2,1,0:T(1,128)S(1)}, u32[]{:S(2)}, u32[]{:S(2)}) %all-to-all-start) | async-done | bytes 65568 | tf_op jit(solution)/shard_map/all_to_all | solution.py:347
  103.9 4.6 %collective-permute-done.24.refs_2_ = f32[2,128,256]{2,1,0:T(8,128)} collective-permute-done((f32[2,128,256]{2,1,0:T(8,128)S(1)}, f32[2,128,256]{2,1,0:T(8,128)}, u32[]{:S(2)}, u32[]{:S(2)}) %collective-permute-start.24) | collective-permute-done | bytes 262176 | tf_op jit(solution)/shard_map/ppermute | solution.py:49
  110.0 2.9 %collective-permute-start.30 = (bf16[4,128,256]{2,1,0:T(8,128)(2,1)S(1)}, bf16[4,128,256]{2,1,0:T(8,128)(2,1)S(1)}, u32[]{:S(2)}, u32[]{:S(2)}) collective-permute-start(bf16[4,128,256]{2,1,0:T(8,128)(2,1)S(1)} %get-tuple-element.81.refs_0_), channel_id=1, source_target_pairs={{0,16},{8,24},{16,0},{24,8},{1,17},{9,25},{17,1},{25,9},{2,18},{10... | collective-permute-start | bytes 786440 | tf_op jit(solution)/shard_map/ppermute | solution.py:49
  113.8 1.8 %collective-permute-start.29 = (bf16[4,128,256]{2,1,0:T(8,128)(2,1)S(1)}, bf16[4,128,256]{2,1,0:T(8,128)(2,1)S(1)}, u32[]{:S(2)}, u32[]{:S(2)}) collective-permute-start(bf16[4,128,256]{2,1,0:T(8,128)(2,1)S(1)} %get-tuple-element.82.refs_1_), channel_id=1, source_target_pairs={{0,96},{32,0},{64,32},{96,64},{1,97},{33,1},{65,33},{97,65},{2,98}... | collective-permute-start | bytes 786440 | tf_op jit(solution)/shard_map/ppermute | solution.py:49
  116.0 2.4 %collective-permute-start.28 = (bf16[4,128,256]{2,1,0:T(8,128)(2,1)S(1)}, bf16[4,128,256]{2,1,0:T(8,128)(2,1)S(1)}, u32[]{:S(2)}, u32[]{:S(2)}) collective-permute-start(bf16[4,128,256]{2,1,0:T(8,128)(2,1)S(1)} %get-tuple-element.81.refs_0_), channel_id=1, source_target_pairs={{0,24},{8,0},{16,8},{24,16},{1,25},{9,1},{17,9},{25,17},{2,26},{10... | collective-permute-start | bytes 786440 | tf_op jit(solution)/shard_map/ppermute | solution.py:49
  118.3 1.6 %copy-done.4 = bf16[8,2,256,256]{3,2,1,0:T(8,128)(2,1)S(1)} copy-done((bf16[8,2,256,256]{3,2,1,0:T(8,128)(2,1)S(1)}, bf16[8,2,256,256]{3,2,1,0:T(8,128)(2,1)}, u32[]{:S(2)}) %copy-start.4) | copy-done | bytes 2097176
  119.9 1.6 %copy-done.6 = bf16[8,2,256,256]{3,2,1,0:T(8,128)(2,1)S(1)} copy-done((bf16[8,2,256,256]{3,2,1,0:T(8,128)(2,1)S(1)}, bf16[8,2,256,256]{3,2,1,0:T(8,128)(2,1)}, u32[]{:S(2)}) %copy-start.6) | copy-done | bytes 2097176
  122.5 4.2 %shard_map.134 = (f32[2,128,2048]{2,1,0:T(8,128)}, f32[2,256,256]{2,1,0:T(8,128)}) custom-call(f32[2,128,2048]{2,1,0:T(8,128)S(1)} %bitcast.20, f32[2,256,256]{2,1,0:T(8,128)S(1)} %bitcast.23, f32[4,256,128]{2,1,0:T(8,128)S(1)} %get-tuple-element.72.line_ref.line_k, f32[4,256,128]{2,1,0:T(8,128)S(1)} %get-tuple-element.59.line_ref.line_v, ...), custom_call_target="tpu_custom_call" | custom-call | tf_op jit(solution)/shard_map/pallas_call | solution.py:361
  (71 shorter events, 28.1 us)
Async XLA Ops:
  10.8 10.8 %collective-permute-start.1 = (bf16[4,264,128]{2,1,0:T(8,128)(2,1)S(1)}, bf16[4,264,128]{2,1,0:T(8,128)(2,1)S(1)}, u32[]{:S(2)}, u32[]{:S(2)}) collective-permute-start(bf16[4,264,128]{2,1,0:T(8,128)(2,1)S(1)} %get-tuple-element.51), channel_id=1, source_target_pairs={{0,32},{32,64},{64,96},{96,0},{1,33},{33,65},{65,97},{97,1},{2,34}... | collective-permute-start | bytes 811016 | tf_op jit(solution)/shard_map/ppermute | solution.py:49
  13.3 11.1 %collective-permute-start.2 = (bf16[4,264,128]{2,1,0:T(8,128)(2,1)S(1)}, bf16[4,264,128]{2,1,0:T(8,128)(2,1)S(1)}, u32[]{:S(2)}, u32[]{:S(2)}) collective-permute-start(bf16[4,264,128]{2,1,0:T(8,128)(2,1)S(1)} %get-tuple-element.52), channel_id=1, source_target_pairs={{0,96},{32,0},{64,32},{96,64},{1,97},{33,1},{65,33},{97,65},{2,98}... | collective-permute-start | bytes 811016 | tf_op jit(solution)/shard_map/ppermute | solution.py:49
  15.5 12.8 %collective-permute-start = (bf16[4,264,128]{2,1,0:T(8,128)(2,1)S(1)}, bf16[4,264,128]{2,1,0:T(8,128)(2,1)S(1)}, u32[]{:S(2)}, u32[]{:S(2)}) collective-permute-start(bf16[4,264,128]{2,1,0:T(8,128)(2,1)S(1)} %get-tuple-element.50), channel_id=1, source_target_pairs={{0,64},{32,96},{64,0},{96,32},{1,65},{33,97},{65,1},{97,33},{2,66}... | collective-permute-start | bytes 811016 | tf_op jit(solution)/shard_map/ppermute | solution.py:49
  16.8 21.2 %collective-permute-start.11 = (bf16[4,264,128]{2,1,0:T(8,128)(2,1)S(1)}, bf16[4,264,128]{2,1,0:T(8,128)(2,1)S(1)}, u32[]{:S(2)}, u32[]{:S(2)}) collective-permute-start(bf16[4,264,128]{2,1,0:T(8,128)(2,1)S(1)} %get-tuple-element.64), channel_id=1, source_target_pairs={{0,8},{8,16},{16,24},{24,0},{1,9},{9,17},{17,25},{25,1},{2,10},{10... | collective-permute-start | bytes 811016 | tf_op jit(solution)/shard_map/ppermute | solution.py:49
  18.0 20.0 %collective-permute-start.12 = (bf16[4,264,128]{2,1,0:T(8,128)(2,1)S(1)}, bf16[4,264,128]{2,1,0:T(8,128)(2,1)S(1)}, u32[]{:S(2)}, u32[]{:S(2)}) collective-permute-start(bf16[4,264,128]{2,1,0:T(8,128)(2,1)S(1)} %get-tuple-element.65), channel_id=1, source_target_pairs={{0,24},{8,0},{16,8},{24,16},{1,25},{9,1},{17,9},{25,17},{2,26},{10... | collective-permute-start | bytes 811016 | tf_op jit(solution)/shard_map/ppermute | solution.py:49
  21.6 16.3 %collective-permute-start.10 = (bf16[4,264,128]{2,1,0:T(8,128)(2,1)S(1)}, bf16[4,264,128]{2,1,0:T(8,128)(2,1)S(1)}, u32[]{:S(2)}, u32[]{:S(2)}) collective-permute-start(bf16[4,264,128]{2,1,0:T(8,128)(2,1)S(1)} %get-tuple-element.63), channel_id=1, source_target_pairs={{0,16},{8,24},{16,0},{24,8},{1,17},{9,25},{17,1},{25,9},{2,18},{10... | collective-permute-start | bytes 811016 | tf_op jit(solution)/shard_map/ppermute | solution.py:49
  30.5 5.1 %collective-permute-start.4 = (bf16[2,264,128]{2,1,0:T(8,128)(2,1)S(1)}, bf16[2,264,128]{2,1,0:T(8,128)(2,1)S(1)}, u32[]{:S(2)}, u32[]{:S(2)}) collective-permute-start(bf16[2,264,128]{2,1,0:T(8,128)(2,1)S(1)} %get-tuple-element.55), channel_id=1, source_target_pairs={{0,24},{8,16},{16,8},{24,0},{1,25},{9,17},{17,9},{25,1},{2,26},{10... | collective-permute-start | bytes 405512 | tf_op jit(solution)/shard_map/ppermute | solution.py:181
  36.0 6.2 %collective-permute-start.5 = (bf16[2,264,128]{2,1,0:T(8,128)(2,1)S(1)}, bf16[2,264,128]{2,1,0:T(8,128)(2,1)S(1)}, u32[]{:S(2)}, u32[]{:S(2)}) collective-permute-start(bf16[2,264,128]{2,1,0:T(8,128)(2,1)S(1)} %get-tuple-element.57), channel_id=1, source_target_pairs={{0,24},{8,16},{16,8},{24,0},{1,25},{9,17},{17,9},{25,1},{2,26},{10... | collective-permute-start | bytes 405512 | tf_op jit(solution)/shard_map/ppermute | solution.py:181
  37.9 4.3 %collective-permute-start.6 = (bf16[2,264,128]{2,1,0:T(8,128)(2,1)S(1)}, bf16[2,264,128]{2,1,0:T(8,128)(2,1)S(1)}, u32[]{:S(2)}, u32[]{:S(2)}) collective-permute-start(bf16[2,264,128]{2,1,0:T(8,128)(2,1)S(1)} %get-tuple-element.58), channel_id=1, source_target_pairs={{0,8},{8,0},{16,24},{24,16},{1,9},{9,1},{17,25},{25,17},{2,10},{10... | collective-permute-start | bytes 405512 | tf_op jit(solution)/shard_map/ppermute | solution.py:181
  38.9 6.5 %collective-permute-start.13 = (bf16[2,264,128]{2,1,0:T(8,128)(2,1)S(1)}, bf16[2,264,128]{2,1,0:T(8,128)(2,1)S(1)}, u32[]{:S(2)}, u32[]{:S(2)}) collective-permute-start(bf16[2,264,128]{2,1,0:T(8,128)(2,1)S(1)} %get-tuple-element.67), channel_id=1, source_target_pairs={{0,32},{32,0},{64,96},{96,64},{1,33},{33,1},{65,97},{97,65},{2,34}... | collective-permute-start | bytes 405512 | tf_op jit(solution)/shard_map/ppermute | solution.py:181
  42.0 5.4 %collective-permute-start.14 = (bf16[2,264,128]{2,1,0:T(8,128)(2,1)S(1)}, bf16[2,264,128]{2,1,0:T(8,128)(2,1)S(1)}, u32[]{:S(2)}, u32[]{:S(2)}) collective-permute-start(bf16[2,264,128]{2,1,0:T(8,128)(2,1)S(1)} %get-tuple-element.68), channel_id=1, source_target_pairs={{0,96},{32,64},{64,32},{96,0},{1,97},{33,65},{65,33},{97,1},{2,98}... | collective-permute-start | bytes 405512 | tf_op jit(solution)/shard_map/ppermute | solution.py:181
  42.7 15.7 %collective-permute-start.7 = (bf16[4,264,128]{2,1,0:T(8,128)(2,1)S(1)}, bf16[4,264,128]{2,1,0:T(8,128)(2,1)S(1)}, u32[]{:S(2)}, u32[]{:S(2)}) collective-permute-start(bf16[4,264,128]{2,1,0:T(8,128)(2,1)S(1)} %get-tuple-element.60), channel_id=1, source_target_pairs={{0,64},{32,96},{64,0},{96,32},{1,65},{33,97},{65,1},{97,33},{2,66}... | collective-permute-start | bytes 811016 | tf_op jit(solution)/shard_map/ppermute | solution.py:49
  47.9 8.1 %collective-permute-start.15 = (bf16[2,264,128]{2,1,0:T(8,128)(2,1)S(1)}, bf16[2,264,128]{2,1,0:T(8,128)(2,1)S(1)}, u32[]{:S(2)}, u32[]{:S(2)}) collective-permute-start(bf16[2,264,128]{2,1,0:T(8,128)(2,1)S(1)} %get-tuple-element.70), channel_id=1, source_target_pairs={{0,96},{32,64},{64,32},{96,0},{1,97},{33,65},{65,33},{97,1},{2,98}... | collective-permute-start | bytes 405512 | tf_op jit(solution)/shard_map/ppermute | solution.py:181
  48.6 7.4 %collective-permute-start.16 = (bf16[2,264,128]{2,1,0:T(8,128)(2,1)S(1)}, bf16[2,264,128]{2,1,0:T(8,128)(2,1)S(1)}, u32[]{:S(2)}, u32[]{:S(2)}) collective-permute-start(bf16[2,264,128]{2,1,0:T(8,128)(2,1)S(1)} %get-tuple-element.71), channel_id=1, source_target_pairs={{0,32},{32,0},{64,96},{96,64},{1,33},{33,1},{65,97},{97,65},{2,34}... | collective-permute-start | bytes 405512 | tf_op jit(solution)/shard_map/ppermute | solution.py:181
  48.6 12.4 %collective-permute-start.8 = (bf16[4,264,128]{2,1,0:T(8,128)(2,1)S(1)}, bf16[4,264,128]{2,1,0:T(8,128)(2,1)S(1)}, u32[]{:S(2)}, u32[]{:S(2)}) collective-permute-start(bf16[4,264,128]{2,1,0:T(8,128)(2,1)S(1)} %get-tuple-element.60), channel_id=1, source_target_pairs={{0,32},{32,64},{64,96},{96,0},{1,33},{33,65},{65,97},{97,1},{2,34}... | collective-permute-start | bytes 811016 | tf_op jit(solution)/shard_map/ppermute | solution.py:49
  50.1 11.0 %collective-permute-start.9 = (bf16[4,264,128]{2,1,0:T(8,128)(2,1)S(1)}, bf16[4,264,128]{2,1,0:T(8,128)(2,1)S(1)}, u32[]{:S(2)}, u32[]{:S(2)}) collective-permute-start(bf16[4,264,128]{2,1,0:T(8,128)(2,1)S(1)} %get-tuple-element.60), channel_id=1, source_target_pairs={{0,96},{32,0},{64,32},{96,64},{1,97},{33,1},{65,33},{97,65},{2,98}... | collective-permute-start | bytes 811016 | tf_op jit(solution)/shard_map/ppermute | solution.py:49
  56.5 7.4 %collective-permute-start.17 = (bf16[4,264,128]{2,1,0:T(8,128)(2,1)S(1)}, bf16[4,264,128]{2,1,0:T(8,128)(2,1)S(1)}, u32[]{:S(2)}, u32[]{:S(2)}) collective-permute-start(bf16[4,264,128]{2,1,0:T(8,128)(2,1)S(1)} %get-tuple-element.73), channel_id=1, source_target_pairs={{0,16},{8,24},{16,0},{24,8},{1,17},{9,25},{17,1},{25,9},{2,18},{10... | collective-permute-start | bytes 811016 | tf_op jit(solution)/shard_map/ppermute | solution.py:49
  58.4 8.0 %collective-permute-start.18 = (bf16[4,264,128]{2,1,0:T(8,128)(2,1)S(1)}, bf16[4,264,128]{2,1,0:T(8,128)(2,1)S(1)}, u32[]{:S(2)}, u32[]{:S(2)}) collective-permute-start(bf16[4,264,128]{2,1,0:T(8,128)(2,1)S(1)} %get-tuple-element.73), channel_id=1, source_target_pairs={{0,8},{8,16},{16,24},{24,0},{1,9},{9,17},{17,25},{25,1},{2,10},{10... | collective-permute-start | bytes 811016 | tf_op jit(solution)/shard_map/ppermute | solution.py:49
  58.4 8.0 %collective-permute-start.19 = (bf16[4,264,128]{2,1,0:T(8,128)(2,1)S(1)}, bf16[4,264,128]{2,1,0:T(8,128)(2,1)S(1)}, u32[]{:S(2)}, u32[]{:S(2)}) collective-permute-start(bf16[4,264,128]{2,1,0:T(8,128)(2,1)S(1)} %get-tuple-element.73), channel_id=1, source_target_pairs={{0,24},{8,0},{16,8},{24,16},{1,25},{9,1},{17,9},{25,17},{2,26},{10... | collective-permute-start | bytes 811016 | tf_op jit(solution)/shard_map/ppermute | solution.py:49
  69.7 26.5 %collective-permute-start.20 = (f32[2,128,256]{2,1,0:T(8,128)}, f32[2,128,256]{2,1,0:T(8,128)}, u32[]{:S(2)}, u32[]{:S(2)}) collective-permute-start(f32[2,128,256]{2,1,0:T(8,128)} %get-tuple-element.75.refs_0_), channel_id=1, source_target_pairs={{0,8},{8,16},{16,24},{24,0},{1,9},{9,17},{17,25},{25,1},{2,10},{10... | collective-permute-start | bytes 786440 | tf_op jit(solution)/shard_map/ppermute | solution.py:49
  71.5 29.7 %collective-permute-start.21 = (f32[2,128,256]{2,1,0:T(8,128)}, f32[2,128,256]{2,1,0:T(8,128)}, u32[]{:S(2)}, u32[]{:S(2)}) collective-permute-start(f32[2,128,256]{2,1,0:T(8,128)} %get-tuple-element.75.refs_0_), channel_id=1, source_target_pairs={{0,16},{8,24},{16,0},{24,8},{1,17},{9,25},{17,1},{25,9},{2,18},{10... | collective-permute-start | bytes 786440 | tf_op jit(solution)/shard_map/ppermute | solution.py:49
  72.1 29.1 %collective-permute-start.22 = (f32[2,128,256]{2,1,0:T(8,128)}, f32[2,128,256]{2,1,0:T(8,128)}, u32[]{:S(2)}, u32[]{:S(2)}) collective-permute-start(f32[2,128,256]{2,1,0:T(8,128)} %get-tuple-element.75.refs_0_), channel_id=1, source_target_pairs={{0,24},{8,0},{16,8},{24,16},{1,25},{9,1},{17,9},{25,17},{2,26},{10... | collective-permute-start | bytes 786440 | tf_op jit(solution)/shard_map/ppermute | solution.py:49
  74.8 26.4 %all-to-all-start = ((f32[128,1,128]{2,1,0:T(1,128)}), f32[128,1,128]{2,1,0:T(1,128)S(1)}, u32[]{:S(2)}, u32[]{:S(2)}) async-start(f32[128,1,128]{2,1,0:T(1,128)} %broadcast_in_dim.19), calls=%async_computation | async-start | bytes 131072 | tf_op jit(solution)/shard_map/all_to_all | solution.py:347
  91.7 12.3 %collective-permute-start.23 = (f32[2,128,256]{2,1,0:T(8,128)S(1)}, f32[2,128,256]{2,1,0:T(8,128)}, u32[]{:S(2)}, u32[]{:S(2)}) collective-permute-start(f32[2,128,256]{2,1,0:T(8,128)S(1)} %get-tuple-element.77.refs_0_), channel_id=1, source_target_pairs={{0,32},{32,64},{64,96},{96,0},{1,33},{33,65},{65,97},{97,1},{2,34}... | collective-permute-start | bytes 786440 | tf_op jit(solution)/shard_map/ppermute | solution.py:49
  93.2 15.3 %collective-permute-start.24 = (f32[2,128,256]{2,1,0:T(8,128)S(1)}, f32[2,128,256]{2,1,0:T(8,128)}, u32[]{:S(2)}, u32[]{:S(2)}) collective-permute-start(f32[2,128,256]{2,1,0:T(8,128)S(1)} %get-tuple-element.77.refs_0_), channel_id=1, source_target_pairs={{0,64},{32,96},{64,0},{96,32},{1,65},{33,97},{65,1},{97,33},{2,66}... | collective-permute-start | bytes 786440 | tf_op jit(solution)/shard_map/ppermute | solution.py:49
  96.1 12.4 %collective-permute-start.25 = (f32[2,128,256]{2,1,0:T(8,128)S(1)}, f32[2,128,256]{2,1,0:T(8,128)}, u32[]{:S(2)}, u32[]{:S(2)}) collective-permute-start(f32[2,128,256]{2,1,0:T(8,128)S(1)} %get-tuple-element.77.refs_0_), channel_id=1, source_target_pairs={{0,96},{32,0},{64,32},{96,64},{1,97},{33,1},{65,33},{97,65},{2,98}... | collective-permute-start | bytes 786440 | tf_op jit(solution)/shard_map/ppermute | solution.py:49
  102.6 13.3 %collective-permute-start.31 = (bf16[4,128,256]{2,1,0:T(8,128)(2,1)S(1)}, bf16[4,128,256]{2,1,0:T(8,128)(2,1)S(1)}, u32[]{:S(2)}, u32[]{:S(2)}) collective-permute-start(bf16[4,128,256]{2,1,0:T(8,128)(2,1)S(1)} %get-tuple-element.82.refs_1_), channel_id=1, source_target_pairs={{0,64},{32,96},{64,0},{96,32},{1,65},{33,97},{65,1},{97,33},{2,66}... | collective-permute-start | bytes 786440 | tf_op jit(solution)/shard_map/ppermute | solution.py:49
  110.0 17.6 %collective-permute-start.30 = (bf16[4,128,256]{2,1,0:T(8,128)(2,1)S(1)}, bf16[4,128,256]{2,1,0:T(8,128)(2,1)S(1)}, u32[]{:S(2)}, u32[]{:S(2)}) collective-permute-start(bf16[4,128,256]{2,1,0:T(8,128)(2,1)S(1)} %get-tuple-element.81.refs_0_), channel_id=1, source_target_pairs={{0,16},{8,24},{16,0},{24,8},{1,17},{9,25},{17,1},{25,9},{2,18},{10... | collective-permute-start | bytes 786440 | tf_op jit(solution)/shard_map/ppermute | solution.py:49
  112.8 15.8 %collective-permute-start.27 = (bf16[4,128,256]{2,1,0:T(8,128)(2,1)S(1)}, bf16[4,128,256]{2,1,0:T(8,128)(2,1)S(1)}, u32[]{:S(2)}, u32[]{:S(2)}) collective-permute-start(bf16[4,128,256]{2,1,0:T(8,128)(2,1)S(1)} %get-tuple-element.82.refs_1_), channel_id=1, source_target_pairs={{0,32},{32,64},{64,96},{96,0},{1,33},{33,65},{65,97},{97,1},{2,34}... | collective-permute-start | bytes 786440 | tf_op jit(solution)/shard_map/ppermute | solution.py:49
  113.8 14.8 %collective-permute-start.29 = (bf16[4,128,256]{2,1,0:T(8,128)(2,1)S(1)}, bf16[4,128,256]{2,1,0:T(8,128)(2,1)S(1)}, u32[]{:S(2)}, u32[]{:S(2)}) collective-permute-start(bf16[4,128,256]{2,1,0:T(8,128)(2,1)S(1)} %get-tuple-element.82.refs_1_), channel_id=1, source_target_pairs={{0,96},{32,0},{64,32},{96,64},{1,97},{33,1},{65,33},{97,65},{2,98}... | collective-permute-start | bytes 786440 | tf_op jit(solution)/shard_map/ppermute | solution.py:49
  115.6 13.0 %collective-permute-start.26 = (bf16[4,128,256]{2,1,0:T(8,128)(2,1)S(1)}, bf16[4,128,256]{2,1,0:T(8,128)(2,1)S(1)}, u32[]{:S(2)}, u32[]{:S(2)}) collective-permute-start(bf16[4,128,256]{2,1,0:T(8,128)(2,1)S(1)} %get-tuple-element.81.refs_0_), channel_id=1, source_target_pairs={{0,8},{8,16},{16,24},{24,0},{1,9},{9,17},{17,25},{25,1},{2,10},{10... | collective-permute-start | bytes 786440 | tf_op jit(solution)/shard_map/ppermute | solution.py:49
  116.0 12.7 %collective-permute-start.28 = (bf16[4,128,256]{2,1,0:T(8,128)(2,1)S(1)}, bf16[4,128,256]{2,1,0:T(8,128)(2,1)S(1)}, u32[]{:S(2)}, u32[]{:S(2)}) collective-permute-start(bf16[4,128,256]{2,1,0:T(8,128)(2,1)S(1)} %get-tuple-element.81.refs_0_), channel_id=1, source_target_pairs={{0,24},{8,0},{16,8},{24,16},{1,25},{9,1},{17,9},{25,17},{2,26},{10... | collective-permute-start | bytes 786440 | tf_op jit(solution)/shard_map/ppermute | solution.py:49
  (10 other events, 136.2 us)
